TPU v7x, 256 devices: a whole 4x4x8 slice. The times are simulated.
256 devices in a mesh: ep: 64 (over z, y, core), tp: 4 (over x).
Axes of the slice: x: 4, y: 4, z: 8, core: 2. Of those that a mesh axis runs over, the one named last changes fastest.
Arguments:
- mixer_channels_raw: bfloat16 [24576, 4096], P('ep', 'tp'), may hold values from -6 to 6
- write_vectors_raw: bfloat16 [24576, 2048], P('ep', 'tp'), may hold values from -6 to 6
- read_vectors_raw: bfloat16 [24576, 2048], P('ep', 'tp'), may hold values from -6 to 6
- gate_logits: bfloat16 [24576, 4096], P('ep', 'tp'), may hold values from -6 to 6
- step_size_raw: bfloat16 [24576, 64], P('ep', 'tp'), may hold values from -4 to 4
- extra_log_decay: float32 [24576, 64], P('ep', 'tp'), may hold values from -2 to 0, as said below
- mixer_conv_taps: float32 [4, 4096], P(None, 'tp'), may hold values from -3 to 3
- write_conv_taps: float32 [4, 2048], P(None, 'tp'), may hold values from -3 to 3
- read_conv_taps: float32 [4, 2048], P(None, 'tp'), may hold values from -3 to 3
- step_size_bias: float32 [64], P('tp'), may hold values from -5 to -3
- log_decay_rate: float32 [64], P('tp'), as said below
- direct_path_weight: float32 [64], P('tp'), may hold values from 0.5 to 3
- mixer_output_weight: bfloat16 [4096, 2048], P('tp'), may hold values from -0.09375 to 0.09375
- mixer_norm_scale: float32 [2048], replicated, may hold values from 0.1 to 1.9
- routed_tokens: bfloat16 [16384, 2048], P('ep'), may hold values from -6 to 6
- expert_norm_scale: float32 [2048], replicated, may hold values from 0.1 to 1.9
- routes: int32 [16384, 2], P('ep'), may hold values from 0 to 63, as said below
- routing_weights: float32 [16384, 2], P('ep'), may hold values from 0.2 to 1
- expert_gate_matrix: bfloat16 [64, 2048, 1024], P('ep', None, 'tp'), may hold values from -0.125 to 0.125
- expert_up_matrix: bfloat16 [64, 2048, 1024], P('ep', None, 'tp'), may hold values from -0.125 to 0.125
- expert_down_matrix: bfloat16 [64, 1024, 2048], P('ep', 'tp'), may hold values from -0.1875 to 0.1875
Outputs:
- mixer_out: bfloat16 [24576, 2048], P(('ep', 'tp'))
- expert_out: bfloat16 [16384, 2048], P('ep', 'tp')
Inputs may be any that keep to these rules, and one draw needn't show every extreme that they name: `routes`: each row names two different experts of one group of 4 consecutive experts. In each aligned block of 256 rows no expert is named by more than 16 rows, and some expert is named by exactly 16 rows in every block. `extra_log_decay`: zero at all but a few positions. `log_decay_rate`: logarithms of positive rates.
All inputs are finite; a program needn't handle non-finite values.
Results may differ from a plain program's by a relative error of at most 0.019.
Values may be sent and summed in bfloat16 or wider, within the bound.
No kernel may reach another device: no remote copies, remote signals or barrier semaphores. Data moves between devices by JAX's collectives and lax.ppermute only.
A program may use at most 128 MiB of HBM per device.

v0:
```python
import jax
import jax.numpy as jnp
from jax import lax
from jax.sharding import Mesh
from jax.sharding import PartitionSpec as P

HEAD_DIM = 64
STATE = 128
BLOCK = 128
EPG = 4
EP = ("ep_0", "ep_1", "ep_2")
EP_TP = ("ep_0", "ep_1", "ep_2", "tp")


eps = 1e-06
highest = lax.Precision.HIGHEST


def nothing_yet(x, identity):
    return jax.tree.map(
        lambda a, e: jnp.broadcast_to(jnp.asarray(e, a.dtype), a.shape), x, identity
    )


def prefix_by_axis(x, axes, combine, identity):
    before = start = nothing_yet(x, identity)
    running = x
    for axis in reversed(axes):
        length, index = (lax.axis_size(axis), lax.axis_index(axis))
        pieces = jax.tree.map(
            lambda part, kind: lax.all_gather(part.astype(kind), axis),
            running,
            (jnp.bfloat16, jnp.bfloat16),
        )
        inside, running = (start, start)
        for k in range(length):
            passed = k < index
            running = combine(
                running, jax.tree.map(lambda part, own: part[k].astype(own.dtype), pieces, x)
            )
            inside = jax.tree.map(lambda new, old: jnp.where(passed, new, old), running, inside)
        before = combine(inside, before)
    return before


def passed_along(value, axis, steps):
    count = lax.axis_size(axis)
    first, last = (max(0, -steps), min(count, count - steps))
    return lax.ppermute(value, axis, [(source, source + steps) for source in range(first, last)])


def split_up(x, dim, length):
    shape = x.shape
    blocks = x.reshape(*shape[:dim], length, shape[dim] // length, *shape[dim + 1 :])
    return jnp.moveaxis(blocks, dim, 0)


def sum_at_owner(x, axis, dim):
    length = lax.axis_size(axis)
    blocks = lax.all_to_all(split_up(x, dim, length), axis, 0, 0, tiled=True)
    return jnp.sum(blocks.astype(jnp.float32), axis=0)


def convolve(values, edge, taps):
    length = values.shape[0]
    joined = jnp.concatenate([edge, values], axis=0).astype(jnp.float32)
    summed = jnp.zeros((length, values.shape[1]), jnp.float32)
    for offset in range(taps.shape[0]):
        summed = summed + taps[offset][None, :] * joined[offset : offset + length]
    return jax.nn.silu(summed)


def normalize(values, gain):
    return (
        values * lax.rsqrt(jnp.mean(values * values, axis=-1, keepdims=True) + eps) * gain[None, :]
    )


def combine_states(earlier, later):
    return (earlier[0] * later[0], later[0][..., None, None] * earlier[1] + later[1])


def local_scan(inner, step_size, decay_factor, write, read):
    length = inner.shape[0]
    nblocks = length // BLOCK
    groups_local = write.shape[1] // STATE
    ratio = step_size.shape[1] // groups_local
    values = inner.reshape(nblocks, BLOCK, groups_local, ratio, HEAD_DIM)
    steps_here = step_size.reshape(nblocks, BLOCK, groups_local, ratio)
    cumul = jnp.cumsum(decay_factor.reshape(nblocks, BLOCK, groups_local, ratio), axis=1)
    writes = write.reshape(nblocks, BLOCK, groups_local, STATE)
    reads = read.reshape(nblocks, BLOCK, groups_local, STATE)
    tail = jnp.exp(cumul[:, -1:] - cumul) * steps_here
    update = jnp.einsum("bsgn,bsgrp->bgrpn", writes, values * tail[..., None], precision=highest)
    block_decay = jnp.exp(cumul[:, -1])
    carry = jnp.zeros(update.shape[1:], jnp.float32)
    entering = []
    for number in range(nblocks):
        entering.append(carry)
        carry = block_decay[number][..., None, None] * carry + update[number]
    device_decay = jnp.prod(block_decay, axis=0)
    identity = (jnp.ones_like(device_decay), jnp.zeros_like(carry))
    causal = jnp.arange(BLOCK)[:, None] >= jnp.arange(BLOCK)[None, :]
    spread = jnp.where(
        causal[None, :, :, None, None], cumul[:, :, None] - cumul[:, None, :], -jnp.inf
    )
    weights = jnp.exp(spread) * steps_here[:, None]
    intersection = jnp.einsum("blgn,bsgn->blsg", reads, writes, precision=highest)
    within = jnp.einsum(
        "blsgr,bsgrp->blgrp", intersection[..., None] * weights, values, precision=highest
    )
    incoming_decay, incoming = prefix_by_axis((device_decay, carry), EP, combine_states, identity)
    starts = jnp.concatenate(
        [jnp.ones_like(block_decay[:1]), jnp.cumprod(block_decay, axis=0)[:-1]], axis=0
    )
    states_in = jnp.stack(entering, axis=0) + starts[..., None, None] * incoming[None]
    carried = (
        jnp.einsum("blgn,bgrpn->blgrp", reads, states_in, precision=highest)
        * jnp.exp(cumul)[..., None]
    )
    return (within + carried).reshape(length, -1)


def per_device(
    mixer_channels_raw,
    write_vectors_raw,
    read_vectors_raw,
    gate_logits,
    step_size_raw,
    extra_log_decay,
    mixer_conv_taps,
    write_conv_taps,
    read_conv_taps,
    step_size_bias,
    log_decay_rate,
    direct_path_weight,
    mixer_output_weight,
    mixer_norm_scale,
    routed_tokens,
    expert_norm_scale,
    routes,
    routing_weights,
    expert_gate_matrix,
    expert_up_matrix,
    expert_down_matrix,
):
    margin = mixer_conv_taps.shape[0] - 1
    edges = passed_along(
        (mixer_channels_raw[-margin:], write_vectors_raw[-margin:], read_vectors_raw[-margin:]),
        EP,
        1,
    )
    inner = convolve(mixer_channels_raw, edges[0], mixer_conv_taps)
    write = convolve(write_vectors_raw, edges[1], write_conv_taps)
    read = convolve(read_vectors_raw, edges[2], read_conv_taps)
    step_size = jax.nn.softplus(step_size_raw.astype(jnp.float32) + step_size_bias[None, :])
    decay_factor = extra_log_decay - step_size * jnp.exp(log_decay_rate)[None, :]
    scanned = (
        local_scan(inner, step_size, decay_factor, write, read)
        + inner * jnp.repeat(direct_path_weight, HEAD_DIM)[None, :]
    )
    gated = (scanned * jax.nn.silu(gate_logits.astype(jnp.float32))).astype(jnp.bfloat16)
    projected = sum_at_owner(
        jnp.dot(gated, mixer_output_weight, preferred_element_type=jnp.float32).astype(
            jnp.bfloat16
        ),
        "tp",
        0,
    )
    mixer_out = normalize(projected, mixer_norm_scale).astype(jnp.bfloat16)
    moe_normed = normalize(routed_tokens.astype(jnp.float32), expert_norm_scale).astype(
        jnp.bfloat16
    )
    experts_total = lax.axis_size(EP)
    token_count = moe_normed.shape[0]
    capacity = token_count * EPG // experts_total
    flat_expert = routes.reshape(-1)
    onehot = (flat_expert[:, None] == jnp.arange(experts_total, dtype=jnp.int32)[None, :]).astype(
        jnp.int32
    )
    rank = jnp.sum(jnp.cumsum(onehot, axis=0) * onehot, axis=1) - 1
    dest = flat_expert * capacity + rank
    token_ids = jnp.repeat(jnp.arange(token_count, dtype=jnp.int32), 2)
    slot_token = (
        jnp.full((experts_total * capacity,), token_count, jnp.int32).at[dest].set(token_ids)
    )
    padded = jnp.concatenate(
        [moe_normed, jnp.zeros((1, moe_normed.shape[1]), jnp.bfloat16)], axis=0
    )
    outgoing = padded[slot_token].reshape(experts_total, capacity, moe_normed.shape[1])
    arrived = lax.all_to_all(outgoing, EP, split_axis=0, concat_axis=0, tiled=True)
    sources = arrived.shape[0]
    items = arrived.shape[1]
    flat_rows = arrived.reshape(sources * items, arrived.shape[2])
    gate_val = jnp.dot(flat_rows, expert_gate_matrix[0], preferred_element_type=jnp.float32)
    up_val = jnp.dot(flat_rows, expert_up_matrix[0], preferred_element_type=jnp.float32)
    hidden = (jax.nn.silu(gate_val) * up_val).astype(jnp.bfloat16)
    partial_terms = jnp.dot(hidden, expert_down_matrix[0], preferred_element_type=jnp.float32)
    own = lax.psum_scatter(
        partial_terms.astype(jnp.bfloat16), "tp", scatter_dimension=1, tiled=True
    )
    returned = lax.all_to_all(
        own.reshape(sources, items, -1), EP, split_axis=0, concat_axis=0, tiled=True
    )
    results = returned.reshape(experts_total * capacity, -1)[dest].astype(jnp.float32)
    results = results.reshape(token_count, 2, -1)
    expert_out = jnp.sum(results * routing_weights[:, :, None], axis=1).astype(jnp.bfloat16)
    return (mixer_out, expert_out)


def solution(mesh):
    split = Mesh(mesh.devices.reshape(8, 4, 2, mesh.shape["tp"]), ("ep_0", "ep_1", "ep_2", "tp"))
    placed = (
        P(EP, "tp"),
        P(EP, "tp"),
        P(EP, "tp"),
        P(EP, "tp"),
        P(EP, "tp"),
        P(EP, "tp"),
        P(None, "tp"),
        P(None, "tp"),
        P(None, "tp"),
        P("tp"),
        P("tp"),
        P("tp"),
        P("tp", None),
        P(),
        P(EP, None),
        P(),
        P(EP, None),
        P(EP, None),
        P(EP, None, "tp"),
        P(EP, None, "tp"),
        P(EP, "tp", None),
    )
    return jax.shard_map(
        per_device,
        mesh=split,
        in_specs=placed,
        out_specs=(P(EP_TP, None), P(EP, "tp")),
        check_vma=False,
    )
```

profile of v0, /device:TPU:1, one launch (start us, length us, event | category | flops | bytes accessed | tf_op | source)
XLA Modules:
  0.0 274.0 jit_solution(18102002715232296363)
XLA Ops:
  8.0 0.9 slice.197
  8.9 0.9 copy.55
  9.8 4.6 %collective-permute-start = (bf16[3,1024]{0,1:T(8,128)(2,1)}, bf16[3,1024]{0,1:T(8,128)(2,1)}, u32[]{:S(2)}, u32[]{:S(2)}) collective-permute-start(bf16[3,1024]{0,1:T(8,128)(2,1)} %copy.55), channel_id=1, source_target_pairs={{0,4},{4,8},{8,12},{12,16},{16,20},{20,24},{24,28},{28,32},{32,36}... | collective-permute-start | bytes 18440 | tf_op jit(solution)/shard_map/ppermute | solution.py:49
  15.1 1.9 collective-permute-start.1
  17.7 0.8 copy.74
  18.8 1.5 fusion.6
  20.6 1.2 reduce-window.6
  22.4 2.4 scatter_custom_fusion
  25.3 6.0 %gather_fusion = bf16[1024,2048]{1,0:T(8,128)(2,1)} fusion(bf16[257,2048]{1,0:T(8,128)(2,1)S(1)} %concatenate.19, s32[1024]{0:T(1024)S(1)} %fusion.66), kind=kCustom, calls=%fused_computation | custom fusion | bytes 8392704 | tf_op jit(solution)/shard_map/gather | solution.py:190
  31.3 12.2 %all-to-all-start.1 = ((bf16[64,16,2048]{2,1,0:T(8,128)(2,1)}), bf16[64,16,2048]{2,1,0:T(8,128)(2,1)}, u32[]{:S(2)}, u32[]{:S(2)}) async-start(bf16[64,16,2048]{2,1,0:T(8,128)(2,1)} %bitcast.183), calls=%async_computation.1 | async-start | bytes 8388608 | tf_op jit(solution)/shard_map/all_to_all | solution.py:191
  44.7 2.0 all-gather.1
  46.7 10.4 %all_gather.25 = bf16[4,4,4]{2,1,0:T(4,128)(2,1)S(1)} all-gather(bf16[1,4,4]{2,1,0:T(4,128)(2,1)S(1)} %fusion.80), channel_id=1, replica_groups=mesh['ep_0'=8,'ep_1'=4,'ep_2'=2,'tp'=4] {'ep_1'}, dimensions={0}, use_global_device_ids=true | all-gather | bytes 160 | tf_op jit(solution)/shard_map/all_gather | solution.py:31
  57.8 1.3 fusion.98
  59.1 1.5 copy.56
  61.6 1.1 reshape.293
  62.8 1.4 maximum_convert_fusion
  64.2 2.9 %divide_multiply_fusion = f32[384,1024]{0,1:T(8,128)} fusion(f32[387,1024]{0,1:T(8,128)S(1)} %maximum_convert_fusion, f32[1024]{0:T(1024)S(1)} %bitcast.191, f32[1024]{0:T(1024)S(1)} %bitcast.192, f32[1024]{0:T(1024)S(1)} %bitcast.190, f32[1024]{0:T(1024)S(1)} %bitcast.189), kind=kLoop, calls=%fused_computation.48 | loop fusion | flops 4325376 | bytes 7880704 | tf_op jit(solution)/shard_map/jit(silu)/mul | solution.py:70
  67.2 2.5 reshape.292
  70.8 1.6 fusion.22
  72.4 1.1 fusion.59
  73.5 3.5 %all_gather.27 = bf16[2,4,4,64,128]{4,3,2,1,0:T(8,128)(2,1)S(1)} all-gather(bf16[1,4,4,64,128]{4,3,2,1,0:T(8,128)(2,1)S(1)} %get-tuple-element.4), channel_id=1, replica_groups=mesh['ep_0'=8,'ep_1'=4,'ep_2'=2,'tp'=4] {'ep_2'}, dimensions={0}, use_global_device_ids=true | all-gather | bytes 786432 | tf_op jit(solution)/shard_map/all_gather | solution.py:31
  77.0 0.8 copy-done.6
  77.8 1.0 fusion.62
  79.0 35.7 %all-gather.5.cloned.1.call-done = bf16[4,4,4,64,128]{4,3,2,1,0:T(8,128)(2,1)} async-done(((bf16[1,4,4,64,128]{4,3,2,1,0:T(8,128)(2,1)}), bf16[4,4,4,64,128]{4,3,2,1,0:T(8,128)(2,1)}) %all-gather.5.cloned.1.call-update) | async-done | bytes 1048592 | tf_op jit(solution)/shard_map/all_gather | solution.py:31
  114.7 2.2 fusion.61
  117.0 22.3 %all-to-all-done.1 = bf16[64,16,2048]{2,1,0:T(8,128)(2,1)} async-done(((bf16[64,16,2048]{2,1,0:T(8,128)(2,1)}), bf16[64,16,2048]{2,1,0:T(8,128)(2,1)}, u32[]{:S(2)}, u32[]{:S(2)}) %all-to-all-start.1) | async-done | bytes 4194336 | tf_op jit(solution)/shard_map/all_to_all | solution.py:191
  139.4 4.7 %fusion.37 = f32[1024,256]{1,0:T(8,128)} fusion(bf16[1024,2048]{1,0:T(8,128)(2,1)} %bitcast.45, bf16[1,2048,256]{2,1,0:T(8,128)(2,1)} %param.39), kind=kOutput, calls=%fused_computation.57 | convolution fusion | flops 1073741824 | bytes 6291456 | tf_op jit(solution)/shard_map/dot_general | solution.py:195
  144.1 9.1 %convolution_convert_fusion = bf16[1024,2048]{1,0:T(8,128)(2,1)} fusion(bf16[1024,2048]{1,0:T(8,128)(2,1)} %bitcast.45, bf16[1,256,2048]{2,1,0:T(8,128)(2,1)S(1)} %copy-done, bf16[1,2048,256]{2,1,0:T(8,128)(2,1)} %param.40, f32[1024,256]{1,0:T(8,128)} %fusion.37), kind=kOutput, calls=%fused_computation.3 | convolution fusion | flops 2151153664 | bytes 11534336 | tf_op jit(solution)/shard_map/dot_general | solution.py:198
  153.3 1.0 copy-done.14
  154.3 5.9 %collective-permute-start.2 = (bf16[3,512]{1,0:T(4,128)(2,1)S(1)}, bf16[3,512]{1,0:T(4,128)(2,1)S(1)}, u32[]{:S(2)}, u32[]{:S(2)}) collective-permute-start(bf16[3,512]{1,0:T(4,128)(2,1)S(1)} %slice.215), channel_id=1, source_target_pairs={{0,4},{4,8},{8,12},{12,16},{16,20},{20,24},{24,28},{28,32},{32,36}... | collective-permute-start | bytes 9224 | tf_op jit(solution)/shard_map/ppermute | solution.py:49
  160.1 11.0 %all_gather.26 = bf16[8,4,4]{2,1,0:T(4,128)(2,1)S(1)} all-gather(bf16[1,4,4]{2,1,0:T(4,128)(2,1)S(1)} %fusion.74), channel_id=1, replica_groups=mesh['ep_0'=8,'ep_1'=4,'ep_2'=2,'tp'=4] {'ep_0'}, dimensions={0}, use_global_device_ids=true | all-gather | bytes 288 | tf_op jit(solution)/shard_map/all_gather | solution.py:31
  171.5 2.4 copy.72
  174.5 1.4 divide_multiply_fusion.1
  175.9 1.4 reshape.294
  177.3 3.8 %convolution_bitcast_fusion = f32[3,128,128,4]{1,2,3,0:T(8,128)} fusion(f32[3,128,4,128]{3,2,1,0:T(4,128)S(1)} %reshape.294, f32[3,128,4,128]{3,2,1,0:T(4,128)} %reshape.293), kind=kOutput, calls=%fused_computation.53 | convolution fusion | flops 301989888 | bytes 2359296 | tf_op jit(solution)/shard_map/blgn,bsgn->blsg/dot_general | solution.py:108
  181.1 2.3 copy.59
  183.4 8.4 %fusion = f32[3,4,4,64,128]{4,3,2,1,0:T(8,128)} fusion(f32[3,128,4,4,64]{1,0,4,3,2:T(4,128)S(1)} %reshape.292, f32[3,128,4,4]{1,3,2,0:T(4,128)S(1)} %copy.63, f32[3,128,4,4]{1,3,2,0:T(4,128)S(1)} %copy.61, f32[3,128,128,4]{2,1,3,0:T(8,128)} %copy.59, pred[128,128]{1,0:T(8,128)(4,1)S(1)} %iota_compare_fusion.2), kind=kOutput, calls=%fused_computation.5 | convolution fusion | flops 607125504 | bytes 3997696 | tf_op jit(solution)/shard_map/blsgr,bsgrp->blgrp/dot_general | solution.py:109
  191.9 4.0 %add_bitcast_fusion = f32[4,4,64,128]{3,2,1,0:T(8,128)S(1)} fusion(bf16[8,4,4,64,128]{4,3,2,1,0:T(8,128)(2,1)} %all-gather.7.cloned.1.call-done, f32[4,4]{1,0:T(4,128)S(1)} %copy-done.27, f32[4,4]{1,0:T(4,128)S(1)} %get-tuple-element.39, f32[4,4]{1,0:T(4,128)S(1)} %fusion.88, f32[4,4]{1,0:T(4,128)S(1)} %get-tuple-element.35, f32[4,4]{1,0:T(4,128)S(1)} %copy-done.23, ...), kind=kLoop, calls=%fused_computation.98 | loop fusion | flops 7471104 | bytes 4195342 | tf_op jit(solution)/shard_map/mul | solution.py:116
  195.9 1.8 fusion.21
  197.8 1.1 copy.71
  199.5 2.2 convolution_convert_fusion.1
  201.6 22.9 %all_to_all.15 = bf16[4,96,2048]{2,1,0:T(8,128)(2,1)} all-to-all(bf16[4,96,2048]{2,1,0:T(8,128)(2,1)S(1)} %bitcast.187), channel_id=1, replica_groups=mesh['ep_0'=8,'ep_1'=4,'ep_2'=2,'tp'=4] {'tp'}, dimensions={0} | all-to-all | bytes 3145728 | tf_op jit(solution)/shard_map/all_to_all | solution.py:60
  224.6 9.1 %all-to-all-start.2 = ((bf16[64,16,512]{2,1,0:T(8,128)(2,1)}), bf16[64,16,512]{2,1,0:T(8,128)(2,1)S(1)}, u32[]{:S(2)}, u32[]{:S(2)}) async-start(bf16[64,16,512]{2,1,0:T(8,128)(2,1)} %bitcast.188), calls=%async_computation.3 | async-start | bytes 2097152 | tf_op jit(solution)/shard_map/all_to_all | solution.py:202
  233.9 1.7 convert_reduce_fusion
  235.8 0.9 multiply_convert_fusion
  236.7 25.2 %all-to-all-done.2 = bf16[64,16,512]{2,1,0:T(8,128)(2,1)S(1)} async-done(((bf16[64,16,512]{2,1,0:T(8,128)(2,1)}), bf16[64,16,512]{2,1,0:T(8,128)(2,1)S(1)}, u32[]{:S(2)}, u32[]{:S(2)}) %all-to-all-start.2) | async-done | bytes 1048608 | tf_op jit(solution)/shard_map/all_to_all | solution.py:202
  261.9 2.0 gather_fusion.1
  264.5 2.1 multiply_reduce_fusion
  (147 shorter events, 9.6 us)
Async XLA Ops:
  8.0 136.1 %copy-start = (bf16[1,256,2048]{2,1,0:T(8,128)(2,1)S(1)}, bf16[1,256,2048]{2,1,0:T(8,128)(2,1)}, u32[]{:S(2)}) copy-start(bf16[1,256,2048]{2,1,0:T(8,128)(2,1)} %param.41) | copy-start | bytes 3145732
  8.0 16.9 %copy-start.7 = (bf16[256,2048]{1,0:T(8,128)(2,1)S(1)}, bf16[256,2048]{1,0:T(8,128)(2,1)}, u32[]{:S(2)}) copy-start(bf16[256,2048]{1,0:T(8,128)(2,1)} %param.35) | copy-start | bytes 3145732
  8.0 16.9 %copy-start.28 = (f32[2048]{0:T(1024)S(1)}, f32[2048]{0:T(1024)}, u32[]{:S(2)}) copy-start(f32[2048]{0:T(1024)} %param.36) | copy-start | bytes 24580
  9.8 53.0 %collective-permute-start = (bf16[3,1024]{0,1:T(8,128)(2,1)}, bf16[3,1024]{0,1:T(8,128)(2,1)}, u32[]{:S(2)}, u32[]{:S(2)}) collective-permute-start(bf16[3,1024]{0,1:T(8,128)(2,1)} %copy.55), channel_id=1, source_target_pairs={{0,4},{4,8},{8,12},{12,16},{16,20},{20,24},{24,28},{28,32},{32,36}... | collective-permute-start | bytes 18440 | tf_op jit(solution)/shard_map/ppermute | solution.py:49
  15.1 45.9 %collective-permute-start.1 = (bf16[3,512]{1,0:T(4,128)(2,1)S(1)}, bf16[3,512]{1,0:T(4,128)(2,1)S(1)}, u32[]{:S(2)}, u32[]{:S(2)}) collective-permute-start(bf16[3,512]{1,0:T(4,128)(2,1)S(1)} %slice.206), channel_id=1, source_target_pairs={{0,4},{4,8},{8,12},{12,16},{16,20},{20,24},{24,28},{28,32},{32,36}... | collective-permute-start | bytes 9224 | tf_op jit(solution)/shard_map/ppermute | solution.py:49
  22.4 2.9 %copy-start.30 = (s32[512,1]{0,1:T(1,128)}, s32[512,1]{0,1:T(1,128)S(1)}, u32[]{:S(2)}) copy-start(s32[512,1]{0,1:T(1,128)S(1)} %compare_select_fusion.1) | copy-start | bytes 6148
  31.3 12.3 %copy-start.38 = (f32[16]{0:T(128)S(1)}, f32[16]{0:T(128)}, u32[]{:S(2)}) copy-start(f32[16]{0:T(128)} %param.31) | copy-start | bytes 196
  31.3 12.3 %copy-start.17 = (f32[384,16]{0,1:T(8,128)S(1)}, f32[384,16]{0,1:T(8,128)}, u32[]{:S(2)}) copy-start(f32[384,16]{0,1:T(8,128)} %param.26) | copy-start | bytes 73732
  31.3 12.3 %copy-start.25 = (bf16[384,16]{0,1:T(8,128)(2,1)S(1)}, bf16[384,16]{0,1:T(8,128)(2,1)}, u32[]{:S(2)}) copy-start(bf16[384,16]{0,1:T(8,128)(2,1)} %param.25) | copy-start | bytes 36868
  31.3 12.3 %copy-start.35 = (f32[16]{0:T(128)S(1)}, f32[16]{0:T(128)}, u32[]{:S(2)}) copy-start(f32[16]{0:T(128)} %param.30) | copy-start | bytes 196
  31.3 108.0 %all-to-all-start.1 = ((bf16[64,16,2048]{2,1,0:T(8,128)(2,1)}), bf16[64,16,2048]{2,1,0:T(8,128)(2,1)}, u32[]{:S(2)}, u32[]{:S(2)}) async-start(bf16[64,16,2048]{2,1,0:T(8,128)(2,1)} %bitcast.183), calls=%async_computation.1 | async-start | bytes 8388608 | tf_op jit(solution)/shard_map/all_to_all | solution.py:191
  43.5 71.2 %all-gather.5.cloned.1.call-start = ((), (), s32[]{:S(2)}) async-start(), calls=%async_computation.4 | async-start | bytes 1310720 | tf_op jit(solution)/shard_map/all_gather | solution.py:31
  43.7 0.9 copy-start.15
  43.8 14.0 %copy-start.32 = (f32[4,512]{1,0:T(4,128)S(1)}, f32[4,512]{1,0:T(4,128)}, u32[]{:S(2)}) copy-start(f32[4,512]{1,0:T(4,128)} %param.28) | copy-start | bytes 24580
  43.8 14.0 %copy-start.24 = (f32[4,1024]{1,0:T(4,128)S(1)}, f32[4,1024]{1,0:T(4,128)}, u32[]{:S(2)}) copy-start(f32[4,1024]{1,0:T(4,128)} %param.27) | copy-start | bytes 49156
  44.3 14.8 %copy-start.2 = (f32[3,128,4,4]{3,2,1,0:T(4,128)}, f32[3,128,4,4]{3,2,1,0:T(4,128)S(1)}, u32[]{:S(2)}) copy-start(f32[3,128,4,4]{3,2,1,0:T(4,128)S(1)} %fusion.102) | copy-start | bytes 73732
  59.1 1.9 copy-start.13
  69.7 1.1 copy-start.4
  77.0 0.8 copy-start.6
  78.8 113.1 %all-gather.7.cloned.1.call-start = ((), (), s32[]{:S(2)}) async-start(), calls=%async_computation.5 | async-start | bytes 2359296 | tf_op jit(solution)/shard_map/all_gather | solution.py:31
  79.0 65.1 %copy-start.18 = (f32[4,4]{1,0:T(4,128)}, f32[4,4]{1,0:T(4,128)S(1)}, u32[]{:S(2)}) copy-start(f32[4,4]{1,0:T(4,128)S(1)} %get-tuple-element.36) | copy-start | bytes 196
  79.0 65.1 %copy-start.20 = (f32[4,4]{1,0:T(4,128)}, f32[4,4]{1,0:T(4,128)S(1)}, u32[]{:S(2)}) copy-start(f32[4,4]{1,0:T(4,128)S(1)} %get-tuple-element.37) | copy-start | bytes 196
  79.0 65.1 %copy-start.22 = (f32[4,4]{1,0:T(4,128)}, f32[4,4]{1,0:T(4,128)S(1)}, u32[]{:S(2)}) copy-start(f32[4,4]{1,0:T(4,128)S(1)} %get-tuple-element.38) | copy-start | bytes 196
  117.0 107.6 %reduce-scatter.2.cloned.1.call-start = ((), (), s32[]{:S(2)}) async-start(), calls=%async_computation.6 | async-start | bytes 5242880 | tf_op jit(solution)/shard_map/reduce_scatter | solution.py:199
  153.2 1.0 copy-start.14
  153.3 17.9 %copy-start.3 = (f32[3,128,4,4]{3,2,1,0:T(4,128)S(1)}, f32[3,128,4,4]{3,2,1,0:T(4,128)}, u32[]{:S(2)}) copy-start(f32[3,128,4,4]{3,2,1,0:T(4,128)} %copy-done.2) | copy-start | bytes 73732
  153.3 17.9 %copy-start.33 = (f32[4,512]{1,0:T(4,128)S(1)}, f32[4,512]{1,0:T(4,128)}, u32[]{:S(2)}) copy-start(f32[4,512]{1,0:T(4,128)} %param.29) | copy-start | bytes 24580
  153.3 18.0 %copy-start.16 = (f32[3,128,4,4]{1,0,3,2:T(4,128)S(1)}, f32[3,128,4,4]{1,0,3,2:T(4,128)}, u32[]{:S(2)}) copy-start(f32[3,128,4,4]{1,0,3,2:T(4,128)} %copy-done.15) | copy-start | bytes 73732
  154.3 20.1 %collective-permute-start.2 = (bf16[3,512]{1,0:T(4,128)(2,1)S(1)}, bf16[3,512]{1,0:T(4,128)(2,1)S(1)}, u32[]{:S(2)}, u32[]{:S(2)}) collective-permute-start(bf16[3,512]{1,0:T(4,128)(2,1)S(1)} %slice.215), channel_id=1, source_target_pairs={{0,4},{4,8},{8,12},{12,16},{16,20},{20,24},{24,28},{28,32},{32,36}... | collective-permute-start | bytes 9224 | tf_op jit(solution)/shard_map/ppermute | solution.py:49
  171.3 2.9 %copy-start.36 = (f32[16]{0:T(128)S(1)}, f32[16]{0:T(128)}, u32[]{:S(2)}) copy-start(f32[16]{0:T(128)} %param.32) | copy-start | bytes 196
  171.5 2.4 copy-start.8
  183.4 8.5 %copy-start.19 = (f32[4,4]{1,0:T(4,128)S(1)}, f32[4,4]{1,0:T(4,128)}, u32[]{:S(2)}) copy-start(f32[4,4]{1,0:T(4,128)} %copy-done.18) | copy-start | bytes 196
  183.4 8.5 %copy-start.21 = (f32[4,4]{1,0:T(4,128)S(1)}, f32[4,4]{1,0:T(4,128)}, u32[]{:S(2)}) copy-start(f32[4,4]{1,0:T(4,128)} %copy-done.20) | copy-start | bytes 196
  183.4 8.5 %copy-start.23 = (f32[4,4]{1,0:T(4,128)S(1)}, f32[4,4]{1,0:T(4,128)}, u32[]{:S(2)}) copy-start(f32[4,4]{1,0:T(4,128)} %copy-done.22) | copy-start | bytes 196
  183.4 8.5 %copy-start.26 = (f32[4,4]{1,0:T(4,128)S(1)}, f32[4,4]{1,0:T(4,128)}, u32[]{:S(2)}) copy-start(f32[4,4]{1,0:T(4,128)} %get-tuple-element.2) | copy-start | bytes 196
  183.4 8.5 %copy-start.27 = (f32[4,4]{1,0:T(4,128)S(1)}, f32[4,4]{1,0:T(4,128)}, u32[]{:S(2)}) copy-start(f32[4,4]{1,0:T(4,128)} %get-tuple-element.3) | copy-start | bytes 196
  191.8 4.1 %copy-start.9 = (f32[1,4,4,64,128]{4,3,2,1,0:T(8,128)S(1)}, f32[1,4,4,64,128]{4,3,2,1,0:T(8,128)}, u32[]{:S(2)}) copy-start(f32[1,4,4,64,128]{4,3,2,1,0:T(8,128)} %get-tuple-element.5) | copy-start | bytes 1572868
  191.9 4.1 %copy-start.10 = (f32[1,4,4,64,128]{4,3,2,1,0:T(8,128)S(1)}, f32[1,4,4,64,128]{4,3,2,1,0:T(8,128)}, u32[]{:S(2)}) copy-start(f32[1,4,4,64,128]{4,3,2,1,0:T(8,128)} %get-tuple-element.6) | copy-start | bytes 1572868
  191.9 4.1 %copy-start.11 = (f32[3,4,4,64,128]{4,3,2,1,0:T(8,128)S(1)}, f32[3,4,4,64,128]{4,3,2,1,0:T(8,128)}, u32[]{:S(2)}) copy-start(f32[3,4,4,64,128]{4,3,2,1,0:T(8,128)} %fusion) | copy-start | bytes 4718596
  195.9 2.9 %copy-start.37 = (bf16[1024,2048]{1,0:T(8,128)(2,1)S(1)}, bf16[1024,2048]{1,0:T(8,128)(2,1)}, u32[]{:S(2)}) copy-start(bf16[1024,2048]{1,0:T(8,128)(2,1)} %param.33) | copy-start | bytes 12582916
  197.8 1.5 copy-start.5
  197.8 1.7 copy-start.12
  224.6 9.2 %copy-start.34 = (f32[256,2]{0,1:T(2,128)S(1)}, f32[256,2]{0,1:T(2,128)}, u32[]{:S(2)}) copy-start(f32[256,2]{0,1:T(2,128)} %param.38) | copy-start | bytes 6148
  224.6 9.3 %copy-start.31 = (s32[512,1]{0,1:T(1,128)S(1)}, s32[512,1]{0,1:T(1,128)}, u32[]{:S(2)}) copy-start(s32[512,1]{0,1:T(1,128)} %copy-done.30) | copy-start | bytes 6148
  224.6 37.3 %all-to-all-start.2 = ((bf16[64,16,512]{2,1,0:T(8,128)(2,1)}), bf16[64,16,512]{2,1,0:T(8,128)(2,1)S(1)}, u32[]{:S(2)}, u32[]{:S(2)}) async-start(bf16[64,16,512]{2,1,0:T(8,128)(2,1)} %bitcast.188), calls=%async_computation.3 | async-start | bytes 2097152 | tf_op jit(solution)/shard_map/all_to_all | solution.py:202
  233.9 1.9 copy-start.29
  261.9 4.7 %copy-start.1 = (bf16[1,256,2048]{2,1,0:T(8,128)(2,1)S(1)}, bf16[1,256,2048]{2,1,0:T(8,128)(2,1)}, u32[]{:S(2)}) copy-start(bf16[1,256,2048]{2,1,0:T(8,128)(2,1)} %param.41) | copy-start | bytes 3145732
Sparse Core Ops, SparseCore 0:
  78.9 35.8 all-gather.4
  117.1 41.7 all-gather.6
Sparse Core Ops, SparseCore 1:
  153.4 48.4 reduce-scatter.1
where the time goes:
time: 275 us; the launch traced here: 274 us
  waiting for transfers between devices  83.3 us (30%)
  blocking collectives  49.9 us (18%)
  starting transfers between devices  34 us (12%)
  local copies, waits for them, and re-layouts  32.9 us (12%)
  matrix products  31.6 us (11%)
  other arithmetic  26.1 us (9%)
  between operations  16.3 us (6%)
    all_gather x2, waiting for transfers between devices, prefix_by_axis(): lax.all_gather(part.astype(kind), axis)  35.7 us
    all_gather x4, blocking collectives, prefix_by_axis(): lax.all_gather(part.astype(kind), axis)  27 us
    all_to_all x1, waiting for transfers between devices, per_device(): lax.all_to_all(own.reshape(sources, items, -1), EP, split_axis=0, concat_...  25.2 us
    all_to_all x1, blocking collectives, sum_at_owner(): blocks = lax.all_to_all(split_up(x, dim, length), axis, 0, 0, tiled=True)  22.9 us
    all_to_all x1, waiting for transfers between devices, per_device(): lax.all_to_all(outgoing, EP, split_axis=0, concat_axis=0, tiled=True)  22.3 us
    ppermute x3, starting transfers between devices, passed_along(): lax.ppermute(value, axis, [(source, source + steps) for source in range(f...  12.3 us
    all_to_all x1, starting transfers between devices, per_device(): lax.all_to_all(outgoing, EP, split_axis=0, concat_axis=0, tiled=True)  12.2 us
    all_to_all x1, starting transfers between devices, per_device(): lax.all_to_all(own.reshape(sources, items, -1), EP, split_axis=0, concat_...  9.14 us
  transfers between devices with their start and end apart: 8, of which 3 were waited for; matrix products, arithmetic and copies ran while one was open for 30% of the time, Pallas kernels for 0%

commit v1 on v0

v1 whole, which is shorter than its diff:
```python
import jax
import jax.numpy as jnp
from jax import lax
from jax.experimental import pallas as pl
from jax.experimental.pallas import tpu as pltpu
from jax.sharding import Mesh
from jax.sharding import PartitionSpec as P


HEAD_DIM = 64
STATE = 128
CAP = 16
EP = ("ep_0", "ep_1", "ep_2")
PLANE = ("ep_1", "ep_2")
EP_TP = ("ep_0", "ep_1", "ep_2", "tp")
EPS = 1e-06
HI = lax.Precision.HIGHEST
F32 = jnp.float32
BF16 = jnp.bfloat16
MIB = 1024 * 1024


def vmem(count):
    return [pl.BlockSpec(memory_space=pltpu.VMEM)] * count


def params(mib):
    return pltpu.CompilerParams(vmem_limit_bytes=mib * MIB)


def cost(flops, nbytes):
    return pl.CostEstimate(flops=flops, bytes_accessed=nbytes, transcendentals=0)


def iota(shape, dim):
    return lax.broadcasted_iota(jnp.int32, shape, dim)


def spread_heads(group, heads, width):
    per = width // HEAD_DIM
    return (iota((heads, width), 0) == group * per + iota((heads, width), 1) // HEAD_DIM).astype(F32)


def dot(a, b, precision=None):
    return jnp.dot(a, b, preferred_element_type=F32, precision=precision)


def dot_tn(a, b):
    return lax.dot_general(a, b, (((0,), (0,)), ((), ())), preferred_element_type=F32)


def dot_nt(a, b):
    return lax.dot_general(a, b, (((1,), (1,)), ((), ())), preferred_element_type=F32)


def silu(x):
    return x / (1.0 + jnp.exp(-x))


def conv_kernel(
    ch_ref, wr_ref, rd_ref, edge_ref, ct_ref, wt_ref, rt_ref, sraw_ref, extra_ref, bias_ref, rate_ref,
    x_ref, w_ref, r_ref, pay_ref, cum_ref, step_ref,
):
    length, heads = sraw_ref.shape
    tile = 128

    def conv(src, taps, dst, first):
        def body(i, carry):
            lanes = pl.ds(pl.multiple_of(i * tile, tile), tile)
            edges = edge_ref[:, pl.ds(pl.multiple_of(first + i * tile, tile), tile)].astype(F32)
            joined = jnp.concatenate([edges[8:16], src[:, lanes].astype(F32)], axis=0)
            t = taps[:, lanes]
            total = t[0:1] * joined[5 : 5 + length]
            for k in range(1, t.shape[0]):
                total = total + t[k : k + 1] * joined[5 + k : 5 + k + length]
            dst[:, lanes] = silu(total).astype(BF16)
            return carry

        lax.fori_loop(0, src.shape[1] // tile, body, 0)

    nch, nw = ch_ref.shape[1], wr_ref.shape[1]
    conv(ch_ref, ct_ref, x_ref, 0)
    conv(wr_ref, wt_ref, w_ref, nch)
    conv(rd_ref, rt_ref, r_ref, nch + nw)

    raw = sraw_ref[...].astype(F32) + bias_ref[...]
    step = jnp.maximum(raw, 0.0) + jnp.log1p(jnp.exp(-jnp.abs(raw)))
    decay = extra_ref[...] - step * jnp.exp(rate_ref[...])
    below = (iota((length, length), 0) >= iota((length, length), 1)).astype(F32)
    cum = dot(below, decay, HI)
    cum_ref[...] = cum
    step_ref[...] = step
    last = cum[length - 1 : length]
    tail = jnp.exp(last - cum) * step
    groups = nw // STATE
    width = nch // groups
    parts = pay_ref.shape[0]
    rows = STATE // parts
    his, los = [], []
    for g in range(groups):
        spread = spread_heads(g, heads, width)
        xt = (x_ref[:, g * width : (g + 1) * width].astype(F32) * dot(tail, spread, HI)).astype(BF16)
        state = dot_tn(w_ref[:, g * STATE : (g + 1) * STATE], xt).astype(BF16)
        pay_ref[:, g * rows : (g + 1) * rows, :] = state.reshape(parts, rows, width)
        total = dot(last, spread, HI)
        high = total.astype(BF16).astype(F32)
        his.append(high)
        los.append(total - high)
    extra_rows = jnp.concatenate(his + los + [jnp.zeros((16 - 2 * groups, width), F32)], axis=0).astype(BF16)
    for p in range(parts):
        pay_ref[p, groups * rows :, :] = extra_rows


def within_kernel(x_ref, w_ref, r_ref, cum_ref, step_ref, direct_ref, y_ref):
    g = pl.program_id(0)
    length, heads = cum_ref.shape
    width = x_ref.shape[1]
    per = width // HEAD_DIM
    block = 128
    pick = (iota((heads, 128), 0) == g * per + iota((heads, 128), 1)).astype(F32)
    cols = dot(cum_ref[...], pick, HI)
    rows = cols.T
    x = x_ref[...].astype(F32)
    xs = (x * dot(step_ref[...], spread_heads(g, heads, width), HI)).astype(BF16)
    first_half = iota((block, 128), 1) < HEAD_DIM
    for i in range(length // block):
        here = slice(i * block, (i + 1) * block)
        seen = (i + 1) * block
        gram = dot_nt(r_ref[here, :], w_ref[0:seen, :])
        causal = i * block + iota((block, seen), 0) >= iota((block, seen), 1)
        outs = []
        for j in range(per):
            gap = cols[here, j : j + 1] - rows[j : j + 1, 0:seen]
            m = (gram * jnp.exp(jnp.where(causal, gap, -1e30))).astype(BF16)
            pair = (j // 2) * 128
            outs.append(dot(m, xs[0:seen, pair : pair + 128]))
        for q in range(per // 2):
            lanes = slice(q * 128, (q + 1) * 128)
            y_ref[here, lanes] = (
                jnp.where(first_half, outs[2 * q], outs[2 * q + 1]) + direct_ref[:, lanes] * x[here, lanes]
            )


def plane_kernel(z_ref, before_ref, total_ref):
    parts, height, width = z_ref.shape
    groups = 4
    rows = (height - 16) // groups
    base = groups * rows
    his, los = [], []
    for g in range(groups):
        run = jnp.zeros((rows, width), F32)
        log = jnp.zeros((1, width), F32)
        here = slice(g * rows, (g + 1) * rows)
        for p in range(parts):
            before_ref[p, here, :] = run
            before_ref[p, base + g : base + g + 1, :] = log
            pad = z_ref[p, base : base + 16, :].astype(F32)
            own = pad[g : g + 1] + pad[groups + g : groups + g + 1]
            run = jnp.exp(own) * run + z_ref[p, here, :].astype(F32)
            log = log + own
        total_ref[here, :] = run.astype(BF16)
        high = log.astype(BF16).astype(F32)
        his.append(high)
        los.append(log - high)
    total_ref[base:, :] = jnp.concatenate(
        his + los + [jnp.zeros((16 - 2 * groups, width), F32)], axis=0
    ).astype(BF16)


def enter_kernel(zi_ref, before_ref, planes_ref, out_ref):
    count, height, width = planes_ref.shape
    parts = before_ref.shape[0]
    groups = 4
    rows = (height - 16) // groups
    base = groups * rows
    mine = zi_ref[0]
    for g in range(groups):
        here = slice(g * rows, (g + 1) * rows)
        state = jnp.zeros((rows, width), F32)
        for k in range(count):
            pad = planes_ref[k, base : base + 16, :].astype(F32)
            own = pad[g : g + 1] + pad[groups + g : groups + g + 1]
            new = jnp.exp(own) * state + planes_ref[k, here, :].astype(F32)
            state = jnp.where(k < mine, new, state)
        for p in range(parts):
            log = before_ref[p, base + g : base + g + 1, :]
            out_ref[p, here, :] = (before_ref[p, here, :] + jnp.exp(log) * state).astype(BF16)


def project_kernel(
    me_ref, y_ref, r_ref, s_ref, cum_ref, gate_ref, wo_ref,
    own_ref, up_ref, down_ref, opa_ref, opb_ref, gated_ref,
):
    length, heads = cum_ref.shape
    n = 4
    part = length // n
    groups = r_ref.shape[1] // STATE
    width = y_ref.shape[1] // groups

    @pl.when(pl.program_id(0) == 0)
    def _():
        me = me_ref[0]
        states = [
            s_ref[:, g * 16 : (g + 1) * 16, :].reshape(STATE, width) for g in range(groups)
        ]
        for k in range(n):
            rows = pl.ds(pl.multiple_of(lax.rem(me + k, n) * part, part), part)
            grown = jnp.exp(cum_ref[rows, :])
            for g in range(groups):
                lanes = slice(g * width, (g + 1) * width)
                carried = dot(r_ref[rows, g * STATE : (g + 1) * STATE], states[g])
                y = y_ref[rows, lanes] + dot(grown, spread_heads(g, heads, width), HI) * carried
                gate = gate_ref[rows, lanes].astype(F32)
                gated_ref[k * part : (k + 1) * part, lanes] = (y * silu(gate)).astype(BF16)

    out = dot(gated_ref[...], wo_ref[...]).astype(BF16)
    own_ref[...] = out[0:part]
    up_ref[...] = out[part : 2 * part]
    opa_ref[...] = out[2 * part : 2 * part + part // 2]
    opb_ref[...] = out[2 * part + part // 2 : 3 * part]
    down_ref[...] = out[3 * part : 4 * part]


def norm_kernel(own_ref, u_ref, d_ref, gain_ref, out_ref):
    total = own_ref[...].astype(F32) + u_ref[...].astype(F32) + d_ref[...].astype(F32)
    mean = jnp.mean(total * total, axis=-1, keepdims=True)
    out_ref[...] = (total * lax.rsqrt(mean + EPS) * gain_ref[...]).astype(BF16)


def dispatch_kernel(me_ref, tok_ref, gain_ref, routes_ref, out_ref, dest_ref, normed_ref):
    count = tok_ref.shape[0]
    slots, quarter = out_ref.shape
    experts = slots // CAP
    v = tok_ref[...].astype(F32)
    mean = jnp.mean(v * v, axis=-1, keepdims=True)
    normed_ref[...] = (v * lax.rsqrt(mean + EPS) * gain_ref[...]).astype(BF16)
    first, second = routes_ref[:, 0:1], routes_ref[:, 1:2]
    ids = iota((count, experts), 1)
    is_first, is_second = ids == first, ids == second
    named = jnp.where(is_first | is_second, 1.0, 0.0).astype(BF16)
    before = jnp.where(iota((count, count), 0) > iota((count, count), 1), 1.0, 0.0).astype(BF16)
    rank = dot(before, named)
    place = rank + (ids * CAP).astype(F32)
    dest0 = jnp.sum(jnp.where(is_first, place, 0.0), axis=1, keepdims=True).astype(jnp.int32)
    dest1 = jnp.sum(jnp.where(is_second, place, 0.0), axis=1, keepdims=True).astype(jnp.int32)
    dest_ref[:, 0:1] = dest0
    dest_ref[:, 1:2] = dest1
    slot = iota((count, slots), 1)
    chosen = jnp.where((slot == dest0) | (slot == dest1), 1.0, 0.0).astype(BF16)
    lanes = pl.ds(pl.multiple_of(me_ref[0] * quarter, quarter), quarter)
    out_ref[...] = dot_tn(chosen, normed_ref[:, lanes]).astype(BF16)


def combine_kernel(back_ref, dest_ref, weight_ref, out_ref):
    count = dest_ref.shape[0]
    slot = iota((count, back_ref.shape[0]), 1)
    mix = jnp.where(slot == dest_ref[:, 0:1], weight_ref[:, 0:1], 0.0) + jnp.where(
        slot == dest_ref[:, 1:2], weight_ref[:, 1:2], 0.0
    )
    high = mix.astype(BF16)
    low = (mix - high.astype(F32)).astype(BF16)
    back = back_ref[...]
    out_ref[...] = (dot(high, back) + dot(low, back)).astype(BF16)


def ring_dot(me, pieces, weights):
    own, left, right, op0, op1 = pieces
    size = own.shape[1]
    half = size // 2

    def rows(shift, offset, count):
        start = lax.rem(me + shift, 4) * size + offset
        return pl.ds(pl.multiple_of(start, half), count)

    out = []
    for w in weights:
        total = dot(own[...], w[rows(0, 0, size), :])
        total = total + dot(left[...], w[rows(3, 0, size), :])
        total = total + dot(right[...], w[rows(1, 0, size), :])
        total = total + dot(op0[...], w[rows(2, 0, half), :])
        total = total + dot(op1[...], w[rows(2, half, half), :])
        out.append(total)
    return out


def hidden_kernel(me_ref, own, left, right, op0, op1, gate_ref, up_ref, out_ref):
    gate, up = ring_dot(me_ref[0], (own, left, right, op0, op1), (gate_ref, up_ref))
    out_ref[...] = (silu(gate) * up).astype(BF16)


def result_kernel(me_ref, own, left, right, op0, op1, down_ref, out_ref):
    (total,) = ring_dot(me_ref[0], (own, left, right, op0, op1), (down_ref,))
    out_ref[...] = total.astype(BF16)


def ring_pieces(x, axis):
    n = lax.axis_size(axis)
    plus = [(i, (i + 1) % n) for i in range(n)]
    minus = [(i, (i - 1) % n) for i in range(n)]
    half = x.shape[1] // 2
    left = lax.ppermute(x, axis, plus)
    right = lax.ppermute(x, axis, minus)
    op0 = lax.ppermute(left[:, :half], axis, plus)
    op1 = lax.ppermute(right[:, half:], axis, minus)
    return x, left, right, op0, op1


def ring_call(kernel, me, pieces, weights, columns, tile):
    rows = pieces[0].shape[0]
    smem = pl.BlockSpec(memory_space=pltpu.SMEM)
    specs = [smem]
    specs += [pl.BlockSpec((tile, p.shape[1]), lambda i: (i, 0)) for p in pieces]
    specs += [pl.BlockSpec(w.shape, lambda i: (0, 0)) for w in weights]
    depth = weights[0].shape[0]
    return pl.pallas_call(
        kernel,
        grid=(rows // tile,),
        in_specs=specs,
        out_specs=pl.BlockSpec((tile, columns), lambda i: (i, 0)),
        out_shape=jax.ShapeDtypeStruct((rows, columns), BF16),
        compiler_params=params(32),
        cost_estimate=cost(2 * rows * depth * columns * len(weights), rows * depth * 2),
    )(me, *pieces, *weights)


def per_device(
    mixer_channels_raw,
    write_vectors_raw,
    read_vectors_raw,
    gate_logits,
    step_size_raw,
    extra_log_decay,
    mixer_conv_taps,
    write_conv_taps,
    read_conv_taps,
    step_size_bias,
    log_decay_rate,
    direct_path_weight,
    mixer_output_weight,
    mixer_norm_scale,
    routed_tokens,
    expert_norm_scale,
    routes,
    routing_weights,
    expert_gate_matrix,
    expert_up_matrix,
    expert_down_matrix,
):
    sds = jax.ShapeDtypeStruct
    smem = pl.BlockSpec(memory_space=pltpu.SMEM)
    tp = lax.axis_index("tp")
    me = tp.reshape(1).astype(jnp.int32)
    tps = lax.axis_size("tp")
    plus = [(i, (i + 1) % tps) for i in range(tps)]
    minus = [(i, (i - 1) % tps) for i in range(tps)]
    cross = [(i, (i + 2) % tps) for i in range(tps)]

    tokens, model = routed_tokens.shape
    experts = lax.axis_size(EP)
    slots = experts * CAP
    quarter = model // tps
    outgoing, dest = pl.pallas_call(
        dispatch_kernel,
        in_specs=[smem] + vmem(3),
        out_specs=vmem(2),
        out_shape=(sds((slots, quarter), BF16), sds((tokens, 2), jnp.int32)),
        scratch_shapes=[pltpu.VMEM((tokens, model), BF16)],
        compiler_params=params(24),
        cost_estimate=cost(2 * slots * tokens * quarter, 4 * MIB),
        name="dispatch",
    )(me, routed_tokens, expert_norm_scale[None, :], routes)
    arrived = lax.all_to_all(
        outgoing.reshape(experts, CAP, quarter), EP, split_axis=0, concat_axis=0, tiled=True
    )
    arrived = arrived.reshape(slots, quarter)

    ff = expert_down_matrix.shape[1]
    down = expert_down_matrix[0]

    def feature_block(shift):
        return lax.dynamic_slice(down, (0, lax.rem(tp + shift, tps) * quarter), (ff, quarter))

    d_own = feature_block(0)
    d_left = lax.ppermute(feature_block(1), "tp", plus)
    d_right = lax.ppermute(feature_block(3), "tp", minus)
    d_cross = lax.ppermute(feature_block(2), "tp", cross)

    length, channels = mixer_channels_raw.shape
    heads = step_size_raw.shape[1]
    nw = write_vectors_raw.shape[1]
    groups = nw // STATE
    width = channels // groups
    edge = jnp.concatenate(
        [mixer_channels_raw[-16:], write_vectors_raw[-16:], read_vectors_raw[-16:]], axis=1
    )
    edge = lax.ppermute(edge, EP, [(i, i + 1) for i in range(experts - 1)])
    parts = lax.axis_size(PLANE)
    height = groups * (STATE // parts) + 16
    x, w, r, payload, cum, step = pl.pallas_call(
        conv_kernel,
        in_specs=vmem(11),
        out_specs=vmem(6),
        out_shape=(
            sds((length, channels), BF16),
            sds((length, nw), BF16),
            sds((length, nw), BF16),
            sds((parts, height, width), BF16),
            sds((length, heads), F32),
            sds((length, heads), F32),
        ),
        compiler_params=params(24),
        cost_estimate=cost(2 * length * STATE * channels * 8, 4 * MIB),
        name="conv",
    )(
        mixer_channels_raw,
        write_vectors_raw,
        read_vectors_raw,
        edge,
        mixer_conv_taps,
        write_conv_taps,
        read_conv_taps,
        step_size_raw,
        extra_log_decay,
        step_size_bias[None, :],
        log_decay_rate[None, :],
    )
    gathered = lax.all_to_all(payload, PLANE, 0, 0, tiled=True)
    before, total = pl.pallas_call(
        plane_kernel,
        in_specs=vmem(1),
        out_specs=vmem(2),
        out_shape=(sds((parts, height, width), F32), sds((height, width), BF16)),
        compiler_params=params(8),
        cost_estimate=cost(1000000, MIB),
        name="plane",
    )(gathered)
    zs = lax.axis_size("ep_0")
    planes = lax.all_to_all(
        jnp.broadcast_to(total[None], (zs, height, width)), "ep_0", 0, 0, tiled=True
    )
    entering = pl.pallas_call(
        enter_kernel,
        in_specs=[smem] + vmem(2),
        out_specs=vmem(1)[0],
        out_shape=sds((parts, height - 16, width), BF16),
        compiler_params=params(8),
        cost_estimate=cost(1000000, MIB),
        name="enter",
    )(lax.axis_index("ep_0").reshape(1).astype(jnp.int32), before, planes)
    entering = lax.all_to_all(entering, PLANE, 0, 0, tiled=True)

    y = pl.pallas_call(
        within_kernel,
        grid=(groups,),
        in_specs=[
            pl.BlockSpec((length, width), lambda g: (0, g)),
            pl.BlockSpec((length, STATE), lambda g: (0, g)),
            pl.BlockSpec((length, STATE), lambda g: (0, g)),
            pl.BlockSpec((length, heads), lambda g: (0, 0)),
            pl.BlockSpec((length, heads), lambda g: (0, 0)),
            pl.BlockSpec((1, width), lambda g: (0, g)),
        ],
        out_specs=pl.BlockSpec((length, width), lambda g: (0, g)),
        out_shape=sds((length, channels), F32),
        compiler_params=params(24),
        cost_estimate=cost(4 * length * length * channels, 4 * MIB),
        name="within",
    )(x, w, r, cum, step, jnp.repeat(direct_path_weight, HEAD_DIM)[None, :])

    out_dim = mixer_output_weight.shape[1]
    part = length // tps
    tile = 512
    row_block = lambda rows: pl.BlockSpec((rows, tile), lambda j: (0, j))
    whole = lambda a: pl.BlockSpec(a.shape, lambda j: (0,) * a.ndim)
    own, up, dn, opa, opb = pl.pallas_call(
        project_kernel,
        grid=(out_dim // tile,),
        in_specs=[smem]
        + [whole(a) for a in (y, r, entering, cum, gate_logits)]
        + [pl.BlockSpec((channels, tile), lambda j: (0, j))],
        out_specs=(row_block(part), row_block(part), row_block(part), row_block(part // 2), row_block(part // 2)),
        out_shape=(
            sds((part, out_dim), BF16),
            sds((part, out_dim), BF16),
            sds((part, out_dim), BF16),
            sds((part // 2, out_dim), BF16),
            sds((part // 2, out_dim), BF16),
        ),
        scratch_shapes=[pltpu.VMEM((length, channels), BF16)],
        compiler_params=params(24),
        cost_estimate=cost(2 * length * channels * out_dim, 6 * MIB),
        name="project",
    )(me, y, r, entering, cum, gate_logits, mixer_output_weight)
    opa = lax.ppermute(opa, "tp", plus)
    opb = lax.ppermute(opb, "tp", minus)
    half = part // 2
    up = jnp.concatenate([(up[:half].astype(F32) + opa.astype(F32)).astype(BF16), up[half:]], axis=0)
    dn = jnp.concatenate([dn[:half], (dn[half:].astype(F32) + opb.astype(F32)).astype(BF16)], axis=0)
    up = lax.ppermute(up, "tp", plus)
    dn = lax.ppermute(dn, "tp", minus)
    mixer_out = pl.pallas_call(
        norm_kernel,
        in_specs=vmem(4),
        out_specs=vmem(1)[0],
        out_shape=sds((part, out_dim), BF16),
        compiler_params=params(8),
        cost_estimate=cost(1000000, 2 * MIB),
        name="norm",
    )(own, up, dn, mixer_norm_scale[None, :])

    pieces = ring_pieces(arrived, "tp")
    hidden = ring_call(
        hidden_kernel, me, pieces, (expert_gate_matrix[0], expert_up_matrix[0]), ff, 256
    )
    stacked = jnp.zeros((tps, ff, quarter), BF16)
    for shift, block in ((0, d_own), (3, d_left), (1, d_right), (2, d_cross)):
        stacked = lax.dynamic_update_slice(stacked, block[None], (lax.rem(tp + shift, tps), 0, 0))
    pieces = ring_pieces(hidden, "tp")
    result = ring_call(
        result_kernel, me, pieces, (stacked.reshape(tps * ff, quarter),), quarter, 256
    )
    returned = lax.all_to_all(
        result.reshape(experts, CAP, quarter), EP, split_axis=0, concat_axis=0, tiled=True
    )
    returned = returned.reshape(slots, quarter)
    expert_out = pl.pallas_call(
        combine_kernel,
        in_specs=vmem(3),
        out_specs=vmem(1)[0],
        out_shape=sds((tokens, quarter), BF16),
        compiler_params=params(16),
        cost_estimate=cost(4 * slots * tokens * quarter, 2 * MIB),
        name="combine",
    )(returned, dest, routing_weights)
    return (mixer_out, expert_out)


def solution(mesh):
    split = Mesh(mesh.devices.reshape(8, 4, 2, mesh.shape["tp"]), EP_TP)
    placed = (
        P(EP, "tp"),
        P(EP, "tp"),
        P(EP, "tp"),
        P(EP, "tp"),
        P(EP, "tp"),
        P(EP, "tp"),
        P(None, "tp"),
        P(None, "tp"),
        P(None, "tp"),
        P("tp"),
        P("tp"),
        P("tp"),
        P("tp", None),
        P(),
        P(EP, None),
        P(),
        P(EP, None),
        P(EP, None),
        P(EP, None, "tp"),
        P(EP, None, "tp"),
        P(EP, "tp", None),
    )

    return jax.shard_map(
        per_device,
        mesh=split,
        in_specs=placed,
        out_specs=(P(EP_TP, None), P(EP, "tp")),
        check_vma=False,
    )
```

time: 275 us -> 200 us (0.73)
  waiting for transfers between devices: 83.3 us -> 38.9 us
  Pallas kernels: 0 us -> 33.1 us
  matrix products: 31.6 us -> 0 us
  other arithmetic: 26.1 us -> 0.16 us
  starting transfers between devices: 34 us -> 50.3 us
  between operations: 16.3 us -> 1.16 us
  blocking collectives: 49.9 us -> 41.1 us
    all_to_all x2 -> x4, waiting for transfers between devices: 47.5 us -> 1.04 us  [the longest x1 1.04 us: per_device(): entering = lax.all_to_all(entering, PLANE, 0, 0, tiled=True)]
    ppermute x3 -> x16, waiting for transfers between devices: 0.01 us -> 37.9 us  [the longest x2 22.1 us: ring_pieces(): left = lax.ppermute(x, axis, plus)]
    all_gather x2 -> x0, waiting for transfers between devices: 35.7 us -> none  [prefix_by_axis(): lax.all_gather(part.astype(kind), axis)]
    pallas_call x0 -> x10, Pallas kernels: none -> 33.1 us  [the longest x2 9.52 us: ring_call(): pl.pallas_call(kernel, grid=(rows // tile,), in_specs=specs, out_specs=pl...]
    dot_general x7 -> x0, matrix products: 31.6 us -> none  [the longest x1 9.13 us: per_device(): jnp.dot(hidden, expert_down_matrix[0], preferred_element_type=jnp.float32)]
    all_gather x4 -> x0, blocking collectives: 27 us -> none  [prefix_by_axis(): lax.all_gather(part.astype(kind), axis)]
    all_to_all x1, blocking collectives: 22.9 us -> 41.1 us  [per_device(): lax.all_to_all(outgoing.reshape(experts, CAP, quarter), EP, split_axis=0,...]
    unnamed x82 -> x74, local copies, waits for them, and re-layouts: 8.07 us -> 22.7 us
  transfers between devices with their start and end apart: 8 -> 20, of which waited for: 3 -> 6; matrix products, arithmetic and copies ran while one was open for 30% -> 5% of each run, Pallas kernels for 0% -> 15%
where the time goes in v1:
time: 200 us; the launch traced here: 197 us
  starting transfers between devices  50.3 us (25%)
  blocking collectives  41.1 us (21%)
  waiting for transfers between devices  38.9 us (19%)
  Pallas kernels  33.1 us (17%)
  local copies, waits for them, and re-layouts  32.5 us (16%)
    all_to_all x1, blocking collectives, per_device(): lax.all_to_all(outgoing.reshape(experts, CAP, quarter), EP, split_axis=0,...  41.1 us
    unnamed x74, local copies, waits for them, and re-layouts  22.7 us
    ppermute x2, waiting for transfers between devices, ring_pieces(): left = lax.ppermute(x, axis, plus)  22.1 us
    pallas_call x2, Pallas kernels, ring_call(): pl.pallas_call(kernel, grid=(rows // tile,), in_specs=specs, out_specs=pl...  9.52 us
    all_to_all x1, starting transfers between devices, per_device(): lax.all_to_all(result.reshape(experts, CAP, quarter), EP, split_axis=0, c...  8.89 us
    pallas_call x1, Pallas kernels, per_device(): pl.pallas_call(conv_kernel, in_specs=vmem(11), out_specs=vmem(6), out_sha...  7.95 us
    ppermute x1, waiting for transfers between devices, per_device(): up = lax.ppermute(up, 'tp', plus)  7.58 us
    all_to_all x1, starting transfers between devices, per_device(): lax.all_to_all(jnp.broadcast_to(total[None], (zs, height, width)), 'ep_0'...  6.1 us
  transfers between devices with their start and end apart: 20, of which 6 were waited for; matrix products, arithmetic and copies ran while one was open for 5% of the time, Pallas kernels for 15%

profile of v1, /device:TPU:1, one launch (start us, length us, event | category | flops | bytes accessed | tf_op | source)
XLA Modules:
  0.0 197.3 jit_solution(15344408052319861892)
XLA Ops:
  1.6 1.2 copy-done.1
  3.5 1.4 dispatch.1
  4.9 41.1 %all_to_all.25 = bf16[64,16,512]{2,1,0:T(8,128)(2,1)S(1)} all-to-all(bf16[64,16,512]{2,1,0:T(8,128)(2,1)S(1)} %bitcast.30), channel_id=1, replica_groups=mesh['ep_0'=8,'ep_1'=4,'ep_2'=2,'tp'=4] {'ep_0','ep_1','ep_2'}, dimensions={0} | all-to-all | bytes 2097152 | tf_op jit(solution)/shard_map/all_to_all | solution.py:372
  46.0 1.2 collective-permute-start.5
  47.2 1.5 collective-permute-start.6
  48.7 22.1 %collective-permute-done.5.left = bf16[1024,512]{1,0:T(8,128)(2,1)S(1)} collective-permute-done((bf16[1024,512]{1,0:T(8,128)(2,1)S(1)}, bf16[1024,512]{1,0:T(8,128)(2,1)S(1)}, u32[]{:S(2)}, u32[]{:S(2)}) %collective-permute-start.5) | collective-permute-done | bytes 1048608 | tf_op jit(solution)/shard_map/ppermute | solution.py:301
  72.5 1.0 copy-done.12
  73.5 2.7 %collective-permute-start.8 = (bf16[1024,256]{1,0:T(8,128)(2,1)}, bf16[1024,256]{1,0:T(8,128)(2,1)}, u32[]{:S(2)}, u32[]{:S(2)}) collective-permute-start(bf16[1024,256]{1,0:T(8,128)(2,1)} %slice.45), channel_id=1, source_target_pairs={{0,3},{1,0},{2,1},{3,2},{4,7},{5,4},{6,5},{7,6},{8,11},{9,8},{10,9... | collective-permute-start | bytes 1572872 | tf_op jit(solution)/shard_map/ppermute | solution.py:304
  76.2 5.1 %collective-permute-start = (bf16[16,2048]{1,0:T(8,128)(2,1)S(1)}, bf16[16,2048]{1,0:T(8,128)(2,1)S(1)}, u32[]{:S(2)}, u32[]{:S(2)}) collective-permute-start(bf16[16,2048]{1,0:T(8,128)(2,1)S(1)} %pad_maximum_fusion.2), channel_id=1, source_target_pairs={{0,4},{4,8},{8,12},{12,16},{16,20},{20,24},{24,28},{28,32},{32,36}... | collective-permute-start | bytes 196616 | tf_op jit(solution)/shard_map/ppermute | solution.py:396
  81.6 1.0 collective-permute-done.edge_ref
  82.6 1.1 copy-done.18
  83.7 1.0 copy-done.19
  84.7 1.0 copy-done.20
  85.7 7.9 %conv.1 = (bf16[384,1024]{1,0:T(8,128)(2,1)S(1)}, bf16[384,512]{1,0:T(8,128)(2,1)S(1)}, bf16[384,512]{1,0:T(8,128)(2,1)S(1)}, bf16[8,80,256]{2,1,0:T(8,128)(2,1)...) custom-call(bf16[384,1024]{1,0:T(8,128)(2,1)S(1)} %copy-done.18, bf16[384,512]{1,0:T(8,128)(2,1)S(1)} %copy-done.19, ...), custom_call_target="tpu_custom_call" | custom-call | flops 805306368 | bytes 4194304 | tf_op jit(solution)/shard_map/conv/pallas_call | solution.py:399
  95.3 5.4 %all-to-all-start = ((bf16[8,80,256]{2,1,0:T(8,128)(2,1)}), bf16[8,80,256]{2,1,0:T(8,128)(2,1)S(1)}, u32[]{:S(2)}, u32[]{:S(2)}) async-start(bf16[8,80,256]{2,1,0:T(8,128)(2,1)} %get-tuple-element.22), calls=%async_computation | async-start | bytes 655360 | tf_op jit(solution)/shard_map/all_to_all | solution.py:427
  100.7 1.2 copy-done.13
  102.0 1.2 copy-done.21
  103.2 1.2 copy-done.22
  104.4 5.0 %shard_map.212.own = bf16[1024,256]{1,0:T(8,128)(2,1)} custom-call(s32[1]{0:T(128)} %bitcast.me_ref, bf16[1024,512]{1,0:T(8,128)(2,1)S(1)} %bitcast.28, bf16[1024,512]{1,0:T(8,128)(2,1)S(1)} %collective-permute-done.5.left, bf16[1024,512]{1,0:T(8,128)(2,1)S(1)} %copy-done.13, bf16[1024,256]{1,0:T(8,128)(2,1)} %collective-permute-done.7.op0, ...), custom_call_target="tpu_custom_call" | custom-call | flops 2147483648 | bytes 4194304 | tf_op jit(solution)/shard_map/pallas_call | solution.py:315
  109.4 2.7 %collective-permute-start.10 = (bf16[1024,256]{1,0:T(8,128)(2,1)}, bf16[1024,256]{1,0:T(8,128)(2,1)}, u32[]{:S(2)}, u32[]{:S(2)}) collective-permute-start(bf16[1024,256]{1,0:T(8,128)(2,1)} %shard_map.212.own), channel_id=1, source_target_pairs={{0,3},{1,0},{2,1},{3,2},{4,7},{5,4},{6,5},{7,6},{8,11},{9,8},{10,9... | collective-permute-start | bytes 1572872 | tf_op jit(solution)/shard_map/ppermute | solution.py:302
  114.8 6.1 %all-to-all-start.1 = ((bf16[8,80,256]{2,1,0:T(8,128)(2,1)}), bf16[8,80,256]{2,1,0:T(8,128)(2,1)S(1)}, u32[]{:S(2)}, u32[]{:S(2)}) async-start(bf16[8,80,256]{2,1,0:T(8,128)(2,1)} %broadcast_in_dim.37), calls=%async_computation.1 | async-start | bytes 655360 | tf_op jit(solution)/shard_map/all_to_all | solution.py:438
  120.9 2.7 %collective-permute-start.14 = (bf16[256,512]{1,0:T(8,128)(2,1)}, bf16[256,512]{1,0:T(8,128)(2,1)}, u32[]{:S(2)}, u32[]{:S(2)}) collective-permute-start(bf16[256,512]{1,0:T(8,128)(2,1)} %get-tuple-element.35), channel_id=1, source_target_pairs={{0,3},{1,0},{2,1},{3,2},{4,7},{5,4},{6,5},{7,6},{8,11},{9,8},{10,9... | collective-permute-start | bytes 786440 | tf_op jit(solution)/shard_map/ppermute | solution.py:385
  123.8 1.1 copy-done.4
  124.9 1.0 copy-done.11
  125.9 0.9 copy-done.15
  126.8 6.0 %within.1.y_ref = f32[384,1024]{1,0:T(8,128)S(1)} custom-call(bf16[384,1024]{1,0:T(8,128)(2,1)S(1)} %copy-done.4, bf16[384,512]{1,0:T(8,128)(2,1)S(1)} %copy-done.11, bf16[384,512]{1,0:T(8,128)(2,1)S(1)} %get-tuple-element.19.r_ref, f32[384,16]{1,0:T(8,128)S(1)} %get-tuple-element.20.cum_ref, f32[384,16]{1,0:T(8,128)S(1)} %copy-done.15, ...), custom_call_target="tpu_custom_call" | custom-call | flops 603979776 | bytes 4194304 | tf_op jit(solution)/shard_map/within/pallas_call | solution.py:452
  132.9 2.8 %collective-permute-done.13 = bf16[256,512]{1,0:T(8,128)(2,1)} collective-permute-done((bf16[256,512]{1,0:T(8,128)(2,1)}, bf16[256,512]{1,0:T(8,128)(2,1)}, u32[]{:S(2)}, u32[]{:S(2)}) %collective-permute-start.13) | collective-permute-done | bytes 262176 | tf_op jit(solution)/shard_map/ppermute | solution.py:384
  135.6 1.0 bitcast_dynamic-update-slice_fusion.2
  136.6 1.7 slice.46
  138.3 1.7 slice.47
  139.9 2.7 %collective-permute-start.12 = (bf16[1024,128]{1,0:T(8,128)(2,1)}, bf16[1024,128]{1,0:T(8,128)(2,1)}, u32[]{:S(2)}, u32[]{:S(2)}) collective-permute-start(bf16[1024,128]{1,0:T(8,128)(2,1)} %slice.47), channel_id=1, source_target_pairs={{0,3},{1,0},{2,1},{3,2},{4,7},{5,4},{6,5},{7,6},{8,11},{9,8},{10,9... | collective-permute-start | bytes 786440 | tf_op jit(solution)/shard_map/ppermute | solution.py:304
  142.6 1.0 bitcast_dynamic-update-slice_fusion.1
  143.6 1.1 copy-done.7
  145.6 5.8 %all-to-all-start.2 = ((bf16[8,64,256]{2,1,0:T(8,128)(2,1)}), bf16[8,64,256]{2,1,0:T(8,128)(2,1)}, u32[]{:S(2)}, u32[]{:S(2)}) async-start(bf16[8,64,256]{2,1,0:T(8,128)(2,1)} %copy-done.2), calls=%async_computation.2 | async-start | bytes 524288 | tf_op jit(solution)/shard_map/all_to_all | solution.py:450
  151.4 1.0 bitcast_dynamic-update-slice_fusion
  152.4 4.5 %shard_map.213 = bf16[1024,512]{1,0:T(8,128)(2,1)} custom-call(s32[1]{0:T(128)} %bitcast.me_ref, bf16[1024,256]{1,0:T(8,128)(2,1)} %shard_map.212.own, bf16[1024,256]{1,0:T(8,128)(2,1)} %collective-permute-done.9.left, bf16[1024,256]{1,0:T(8,128)(2,1)} %collective-permute-done.10.right, bf16[1024,128]{1,0:T(8,128)(2,1)} %collective-permute-done.11.op0, ...), custom_call_target="tpu_custom_call" | custom-call | flops 1073741824 | bytes 2097152 | tf_op jit(solution)/shard_map/pallas_call | solution.py:315
  156.9 1.0 all-to-all-done.2.s_ref
  158.0 8.9 %all-to-all-start.4 = ((bf16[64,16,512]{2,1,0:T(8,128)(2,1)}), bf16[64,16,512]{2,1,0:T(8,128)(2,1)S(1)}, u32[]{:S(2)}, u32[]{:S(2)}) async-start(bf16[64,16,512]{2,1,0:T(8,128)(2,1)} %bitcast.17), calls=%async_computation.4 | async-start | bytes 2097152 | tf_op jit(solution)/shard_map/all_to_all | solution.py:522
  166.9 2.2 %copy-done = bf16[1024,2048]{1,0:T(8,128)(2,1)S(1)} copy-done((bf16[1024,2048]{1,0:T(8,128)(2,1)S(1)}, bf16[1024,2048]{1,0:T(8,128)(2,1)}, u32[]{:S(2)}) %copy-start) | copy-done | bytes 4194328
  169.1 1.1 copy-done.5
  170.2 5.3 %project.1 = (bf16[96,2048]{1,0:T(8,128)(2,1)S(1)}, bf16[96,2048]{1,0:T(8,128)(2,1)S(1)}, bf16[96,2048]{1,0:T(8,128)(2,1)S(1)}, bf16[48,2048]{1,0:T(8,128)(2,1)S(1)}, bf16[48,2048]{1,0:T(8,128)(2,1)S(1)}) custom-call(s32[1]{0:T(128)} %bitcast.me_ref, f32[384,1024]{1,0:T(8,128)S(1)} %within.1.y_ref, bf16[384,512]{1,0:T(8,128)(2,1)S(1)} %get-tuple-element.19.r_ref, ...), custom_call_target="tpu_custom_call" | custom-call | flops 1610612736 | bytes 6291456 | tf_op jit(solution)/shard_map/project/pallas_call | solution.py:475
  175.6 2.7 %collective-permute-start.3 = (bf16[48,2048]{1,0:T(8,128)(2,1)S(1)}, bf16[48,2048]{1,0:T(8,128)(2,1)S(1)}, u32[]{:S(2)}, u32[]{:S(2)}) collective-permute-start(bf16[48,2048]{1,0:T(8,128)(2,1)S(1)} %get-tuple-element.29), channel_id=1, source_target_pairs={{0,3},{1,0},{2,1},{3,2},{4,7},{5,4},{6,5},{7,6},{8,11},{9,8},{10,9... | collective-permute-start | bytes 589832 | tf_op jit(solution)/shard_map/ppermute | solution.py:495
  178.4 4.4 %collective-permute-done.1 = bf16[48,2048]{1,0:T(8,128)(2,1)S(1)} collective-permute-done((bf16[48,2048]{1,0:T(8,128)(2,1)S(1)}, bf16[48,2048]{1,0:T(8,128)(2,1)S(1)}, u32[]{:S(2)}, u32[]{:S(2)}) %collective-permute-start.1) | collective-permute-done | bytes 196640 | tf_op jit(solution)/shard_map/ppermute | solution.py:494
  183.1 2.7 %collective-permute-start.4 = (bf16[96,2048]{1,0:T(8,128)(2,1)S(1)}, bf16[96,2048]{1,0:T(8,128)(2,1)S(1)}, u32[]{:S(2)}, u32[]{:S(2)}) collective-permute-start(bf16[96,2048]{1,0:T(8,128)(2,1)S(1)} %pad_maximum_fusion.1), channel_id=1, source_target_pairs={{0,3},{1,0},{2,1},{3,2},{4,7},{5,4},{6,5},{7,6},{8,11},{9,8},{10,9... | collective-permute-start | bytes 1179656 | tf_op jit(solution)/shard_map/ppermute | solution.py:500
  186.0 7.6 %collective-permute-done.2.u_ref = bf16[96,2048]{1,0:T(8,128)(2,1)S(1)} collective-permute-done((bf16[96,2048]{1,0:T(8,128)(2,1)S(1)}, bf16[96,2048]{1,0:T(8,128)(2,1)S(1)}, u32[]{:S(2)}, u32[]{:S(2)}) %collective-permute-start.2) | collective-permute-done | bytes 393248 | tf_op jit(solution)/shard_map/ppermute | solution.py:499
  193.5 1.0 copy-done.9
  194.5 1.0 norm.1
  195.6 1.7 combine.1
  (102 shorter events, 9.5 us)
Async XLA Ops:
  0.6 75.5 %slice-start.2 = ((bf16[384,512]{1,0:T(8,128)(2,1)}), bf16[16,512]{1,0:T(8,128)(2,1)S(1)}, s32[]{:S(2)}) async-start(bf16[384,512]{1,0:T(8,128)(2,1)} %rd_ref.1), calls=%async_computation.7 | async-start | bytes 32768 | tf_op jit(solution)/shard_map/slice | solution.py:394
  0.6 75.5 %slice-start.1 = ((bf16[384,512]{1,0:T(8,128)(2,1)}), bf16[16,512]{1,0:T(8,128)(2,1)S(1)}, s32[]{:S(2)}) async-start(bf16[384,512]{1,0:T(8,128)(2,1)} %wr_ref.1), calls=%async_computation.6 | async-start | bytes 32768 | tf_op jit(solution)/shard_map/slice | solution.py:394
  0.7 75.5 %slice-start = ((bf16[384,1024]{1,0:T(8,128)(2,1)}), bf16[16,1024]{1,0:T(8,128)(2,1)S(1)}, s32[]{:S(2)}) async-start(bf16[384,1024]{1,0:T(8,128)(2,1)} %ch_ref.1), calls=%async_computation.5 | async-start | bytes 65536 | tf_op jit(solution)/shard_map/slice | solution.py:394
  0.7 80.6 %copy-start.32 = (bf16[384,16]{0,1:T(8,128)(2,1)S(1)}, bf16[384,16]{0,1:T(8,128)(2,1)}, u32[]{:S(2)}) copy-start(bf16[384,16]{0,1:T(8,128)(2,1)} %param.25) | copy-start | bytes 36868
  0.7 80.8 %copy-start.31 = (f32[384,16]{0,1:T(8,128)S(1)}, f32[384,16]{0,1:T(8,128)}, u32[]{:S(2)}) copy-start(f32[384,16]{0,1:T(8,128)} %param.26) | copy-start | bytes 73732
  0.7 81.9 %copy-start.25 = (f32[4,1024]{1,0:T(4,128)S(1)}, f32[4,1024]{1,0:T(4,128)}, u32[]{:S(2)}) copy-start(f32[4,1024]{1,0:T(4,128)} %ct_ref.1) | copy-start | bytes 49156
  0.7 81.9 %copy-start.26 = (f32[4,512]{1,0:T(4,128)S(1)}, f32[4,512]{1,0:T(4,128)}, u32[]{:S(2)}) copy-start(f32[4,512]{1,0:T(4,128)} %wt_ref.1) | copy-start | bytes 24580
  0.7 81.9 %copy-start.27 = (f32[4,512]{1,0:T(4,128)S(1)}, f32[4,512]{1,0:T(4,128)}, u32[]{:S(2)}) copy-start(f32[4,512]{1,0:T(4,128)} %rt_ref.1) | copy-start | bytes 24580
  0.7 81.9 %copy-start.28 = (f32[16]{0:T(128)S(1)}, f32[16]{0:T(128)}, u32[]{:S(2)}) copy-start(f32[16]{0:T(128)} %param.30) | copy-start | bytes 196
  0.7 81.9 %copy-start.29 = (f32[16]{0:T(128)S(1)}, f32[16]{0:T(128)}, u32[]{:S(2)}) copy-start(f32[16]{0:T(128)} %param.31) | copy-start | bytes 196
  1.6 1.2 copy-start.1
  4.9 71.3 %copy-start.23 = (s32[256,2]{1,0:T(8,128)}, s32[256,2]{1,0:T(8,128)S(1)}, u32[]{:S(2)}) copy-start(s32[256,2]{1,0:T(8,128)S(1)} %get-tuple-element.31.dest_ref) | copy-start | bytes 6148
  46.0 24.8 %collective-permute-start.5 = (bf16[1024,512]{1,0:T(8,128)(2,1)S(1)}, bf16[1024,512]{1,0:T(8,128)(2,1)S(1)}, u32[]{:S(2)}, u32[]{:S(2)}) collective-permute-start(bf16[1024,512]{1,0:T(8,128)(2,1)S(1)} %bitcast.26), channel_id=1, source_target_pairs={{0,1},{1,2},{2,3},{3,0},{4,5},{5,6},{6,7},{7,4},{8,9},{9,10},{10,1... | collective-permute-start | bytes 3145736 | tf_op jit(solution)/shard_map/ppermute | solution.py:301
  47.2 24.4 %collective-permute-start.6 = (bf16[1024,512]{1,0:T(8,128)(2,1)S(1)}, bf16[1024,512]{1,0:T(8,128)(2,1)S(1)}, u32[]{:S(2)}, u32[]{:S(2)}) collective-permute-start(bf16[1024,512]{1,0:T(8,128)(2,1)S(1)} %bitcast.27), channel_id=1, source_target_pairs={{0,3},{1,0},{2,1},{3,2},{4,7},{5,4},{6,5},{7,6},{8,11},{9,8},{10,9... | collective-permute-start | bytes 3145736 | tf_op jit(solution)/shard_map/ppermute | solution.py:302
  71.6 29.1 %collective-permute-start.7 = (bf16[1024,256]{1,0:T(8,128)(2,1)}, bf16[1024,256]{1,0:T(8,128)(2,1)}, u32[]{:S(2)}, u32[]{:S(2)}) collective-permute-start(bf16[1024,256]{1,0:T(8,128)(2,1)} %slice.44), channel_id=1, source_target_pairs={{0,1},{1,2},{2,3},{3,0},{4,5},{5,6},{6,7},{7,4},{8,9},{9,10},{10,1... | collective-permute-start | bytes 1572872 | tf_op jit(solution)/shard_map/ppermute | solution.py:303
  72.5 1.0 copy-start.12
  73.5 27.2 %collective-permute-start.8 = (bf16[1024,256]{1,0:T(8,128)(2,1)}, bf16[1024,256]{1,0:T(8,128)(2,1)}, u32[]{:S(2)}, u32[]{:S(2)}) collective-permute-start(bf16[1024,256]{1,0:T(8,128)(2,1)} %slice.45), channel_id=1, source_target_pairs={{0,3},{1,0},{2,1},{3,2},{4,7},{5,4},{6,5},{7,6},{8,11},{9,8},{10,9... | collective-permute-start | bytes 1572872 | tf_op jit(solution)/shard_map/ppermute | solution.py:304
  76.2 6.4 %collective-permute-start = (bf16[16,2048]{1,0:T(8,128)(2,1)S(1)}, bf16[16,2048]{1,0:T(8,128)(2,1)S(1)}, u32[]{:S(2)}, u32[]{:S(2)}) collective-permute-start(bf16[16,2048]{1,0:T(8,128)(2,1)S(1)} %pad_maximum_fusion.2), channel_id=1, source_target_pairs={{0,4},{4,8},{8,12},{12,16},{16,20},{20,24},{24,28},{28,32},{32,36}... | collective-permute-start | bytes 196616 | tf_op jit(solution)/shard_map/ppermute | solution.py:396
  82.6 1.1 copy-start.18
  95.3 14.1 %copy-start.14 = (f32[384,16]{1,0:T(8,128)}, f32[384,16]{1,0:T(8,128)S(1)}, u32[]{:S(2)}) copy-start(f32[384,16]{1,0:T(8,128)S(1)} %get-tuple-element.21.step_ref) | copy-start | bytes 73732
  95.3 17.8 %all-to-all-start = ((bf16[8,80,256]{2,1,0:T(8,128)(2,1)}), bf16[8,80,256]{2,1,0:T(8,128)(2,1)S(1)}, u32[]{:S(2)}, u32[]{:S(2)}) async-start(bf16[8,80,256]{2,1,0:T(8,128)(2,1)} %get-tuple-element.22), calls=%async_computation | async-start | bytes 655360 | tf_op jit(solution)/shard_map/all_to_all | solution.py:427
  100.7 1.2 copy-start.13
  102.0 1.2 copy-start.21
  103.2 1.2 copy-start.22
  104.4 7.8 %copy-start.30 = (bf16[1,256,2048]{2,1,0:T(8,128)(2,1)S(1)}, bf16[1,256,2048]{2,1,0:T(8,128)(2,1)}, u32[]{:S(2)}) copy-start(bf16[1,256,2048]{2,1,0:T(8,128)(2,1)} %param.41) | copy-start | bytes 3145732
  109.4 14.2 %copy-start.34 = (f32[16]{0:T(128)S(1)}, f32[16]{0:T(128)}, u32[]{:S(2)}) copy-start(f32[16]{0:T(128)} %param.32) | copy-start | bytes 196
  109.4 27.2 %collective-permute-start.9 = (bf16[1024,256]{1,0:T(8,128)(2,1)}, bf16[1024,256]{1,0:T(8,128)(2,1)}, u32[]{:S(2)}, u32[]{:S(2)}) collective-permute-start(bf16[1024,256]{1,0:T(8,128)(2,1)} %shard_map.212.own), channel_id=1, source_target_pairs={{0,1},{1,2},{2,3},{3,0},{4,5},{5,6},{6,7},{7,4},{8,9},{9,10},{10,1... | collective-permute-start | bytes 1572872 | tf_op jit(solution)/shard_map/ppermute | solution.py:301
  109.4 28.9 %collective-permute-start.10 = (bf16[1024,256]{1,0:T(8,128)(2,1)}, bf16[1024,256]{1,0:T(8,128)(2,1)}, u32[]{:S(2)}, u32[]{:S(2)}) collective-permute-start(bf16[1024,256]{1,0:T(8,128)(2,1)} %shard_map.212.own), channel_id=1, source_target_pairs={{0,3},{1,0},{2,1},{3,2},{4,7},{5,4},{6,5},{7,6},{8,11},{9,8},{10,9... | collective-permute-start | bytes 1572872 | tf_op jit(solution)/shard_map/ppermute | solution.py:302
  113.1 22.5 %collective-permute-start.13 = (bf16[256,512]{1,0:T(8,128)(2,1)}, bf16[256,512]{1,0:T(8,128)(2,1)}, u32[]{:S(2)}, u32[]{:S(2)}) collective-permute-start(bf16[256,512]{1,0:T(8,128)(2,1)} %get-tuple-element.33), channel_id=1, source_target_pairs={{0,1},{1,2},{2,3},{3,0},{4,5},{5,6},{6,7},{7,4},{8,9},{9,10},{10,1... | collective-permute-start | bytes 786440 | tf_op jit(solution)/shard_map/ppermute | solution.py:384
  114.8 28.8 %all-to-all-start.1 = ((bf16[8,80,256]{2,1,0:T(8,128)(2,1)}), bf16[8,80,256]{2,1,0:T(8,128)(2,1)S(1)}, u32[]{:S(2)}, u32[]{:S(2)}) async-start(bf16[8,80,256]{2,1,0:T(8,128)(2,1)} %broadcast_in_dim.37), calls=%async_computation.1 | async-start | bytes 655360 | tf_op jit(solution)/shard_map/all_to_all | solution.py:438
  120.9 21.7 %collective-permute-start.14 = (bf16[256,512]{1,0:T(8,128)(2,1)}, bf16[256,512]{1,0:T(8,128)(2,1)}, u32[]{:S(2)}, u32[]{:S(2)}) collective-permute-start(bf16[256,512]{1,0:T(8,128)(2,1)} %get-tuple-element.35), channel_id=1, source_target_pairs={{0,3},{1,0},{2,1},{3,2},{4,7},{5,4},{6,5},{7,6},{8,11},{9,8},{10,9... | collective-permute-start | bytes 786440 | tf_op jit(solution)/shard_map/ppermute | solution.py:385
  123.6 27.8 %collective-permute-start.15 = (bf16[256,512]{1,0:T(8,128)(2,1)}, bf16[256,512]{1,0:T(8,128)(2,1)}, u32[]{:S(2)}, u32[]{:S(2)}) collective-permute-start(bf16[256,512]{1,0:T(8,128)(2,1)} %get-tuple-element.32), channel_id=1, source_target_pairs={{0,2},{1,3},{2,0},{3,1},{4,6},{5,7},{6,4},{7,5},{8,10},{9,11},{10,... | collective-permute-start | bytes 786440 | tf_op jit(solution)/shard_map/ppermute | solution.py:386
  123.8 1.1 copy-start.4
  138.3 14.1 %collective-permute-start.11 = (bf16[1024,128]{1,0:T(8,128)(2,1)}, bf16[1024,128]{1,0:T(8,128)(2,1)}, u32[]{:S(2)}, u32[]{:S(2)}) collective-permute-start(bf16[1024,128]{1,0:T(8,128)(2,1)} %slice.46), channel_id=1, source_target_pairs={{0,1},{1,2},{2,3},{3,0},{4,5},{5,6},{6,7},{7,4},{8,9},{9,10},{10,1... | collective-permute-start | bytes 786440 | tf_op jit(solution)/shard_map/ppermute | solution.py:303
  139.9 12.5 %collective-permute-start.12 = (bf16[1024,128]{1,0:T(8,128)(2,1)}, bf16[1024,128]{1,0:T(8,128)(2,1)}, u32[]{:S(2)}, u32[]{:S(2)}) collective-permute-start(bf16[1024,128]{1,0:T(8,128)(2,1)} %slice.47), channel_id=1, source_target_pairs={{0,3},{1,0},{2,1},{3,2},{4,7},{5,4},{6,5},{7,6},{8,11},{9,8},{10,9... | collective-permute-start | bytes 786440 | tf_op jit(solution)/shard_map/ppermute | solution.py:304
  143.6 1.1 copy-start.7
  145.6 12.4 %all-to-all-start.2 = ((bf16[8,64,256]{2,1,0:T(8,128)(2,1)}), bf16[8,64,256]{2,1,0:T(8,128)(2,1)}, u32[]{:S(2)}, u32[]{:S(2)}) async-start(bf16[8,64,256]{2,1,0:T(8,128)(2,1)} %copy-done.2), calls=%async_computation.2 | async-start | bytes 524288 | tf_op jit(solution)/shard_map/all_to_all | solution.py:450
  158.0 37.6 %all-to-all-start.4 = ((bf16[64,16,512]{2,1,0:T(8,128)(2,1)}), bf16[64,16,512]{2,1,0:T(8,128)(2,1)S(1)}, u32[]{:S(2)}, u32[]{:S(2)}) async-start(bf16[64,16,512]{2,1,0:T(8,128)(2,1)} %bitcast.17), calls=%async_computation.4 | async-start | bytes 2097152 | tf_op jit(solution)/shard_map/all_to_all | solution.py:522
  166.9 2.2 %copy-start = (bf16[1024,2048]{1,0:T(8,128)(2,1)S(1)}, bf16[1024,2048]{1,0:T(8,128)(2,1)}, u32[]{:S(2)}) copy-start(bf16[1024,2048]{1,0:T(8,128)(2,1)} %wo_ref.1) | copy-start | bytes 12582916
  169.1 1.1 copy-start.5
  170.2 15.6 %copy-start.33 = (f32[256,2]{0,1:T(2,128)S(1)}, f32[256,2]{0,1:T(2,128)}, u32[]{:S(2)}) copy-start(f32[256,2]{0,1:T(2,128)} %param.38) | copy-start | bytes 6148
  170.2 23.3 %copy-start.17 = (f32[2048]{0:T(1024)S(1)}, f32[2048]{0:T(1024)}, u32[]{:S(2)}) copy-start(f32[2048]{0:T(1024)} %param.34) | copy-start | bytes 24580
  175.5 7.6 %copy-start.8 = (bf16[96,2048]{1,0:T(8,128)(2,1)}, bf16[96,2048]{1,0:T(8,128)(2,1)S(1)}, u32[]{:S(2)}) copy-start(bf16[96,2048]{1,0:T(8,128)(2,1)S(1)} %get-tuple-element.25.own_ref) | copy-start | bytes 1179652
  175.5 20.1 %copy-start.24 = (s32[256,2]{1,0:T(8,128)S(1)}, s32[256,2]{1,0:T(8,128)}, u32[]{:S(2)}) copy-start(s32[256,2]{1,0:T(8,128)} %copy-done.23) | copy-start | bytes 6148
  175.5 7.3 %collective-permute-start.1 = (bf16[48,2048]{1,0:T(8,128)(2,1)S(1)}, bf16[48,2048]{1,0:T(8,128)(2,1)S(1)}, u32[]{:S(2)}, u32[]{:S(2)}) collective-permute-start(bf16[48,2048]{1,0:T(8,128)(2,1)S(1)} %get-tuple-element.27), channel_id=1, source_target_pairs={{0,1},{1,2},{2,3},{3,0},{4,5},{5,6},{6,7},{7,4},{8,9},{9,10},{10,1... | collective-permute-start | bytes 589832 | tf_op jit(solution)/shard_map/ppermute | solution.py:494
  175.6 7.4 %collective-permute-start.3 = (bf16[48,2048]{1,0:T(8,128)(2,1)S(1)}, bf16[48,2048]{1,0:T(8,128)(2,1)S(1)}, u32[]{:S(2)}, u32[]{:S(2)}) collective-permute-start(bf16[48,2048]{1,0:T(8,128)(2,1)S(1)} %get-tuple-element.29), channel_id=1, source_target_pairs={{0,3},{1,0},{2,1},{3,2},{4,7},{5,4},{6,5},{7,6},{8,11},{9,8},{10,9... | collective-permute-start | bytes 589832 | tf_op jit(solution)/shard_map/ppermute | solution.py:495
  182.9 10.7 %collective-permute-start.2 = (bf16[96,2048]{1,0:T(8,128)(2,1)S(1)}, bf16[96,2048]{1,0:T(8,128)(2,1)S(1)}, u32[]{:S(2)}, u32[]{:S(2)}) collective-permute-start(bf16[96,2048]{1,0:T(8,128)(2,1)S(1)} %pad_maximum_fusion), channel_id=1, source_target_pairs={{0,1},{1,2},{2,3},{3,0},{4,5},{5,6},{6,7},{7,4},{8,9},{9,10},{10,1... | collective-permute-start | bytes 1179656 | tf_op jit(solution)/shard_map/ppermute | solution.py:499
  183.1 10.4 %collective-permute-start.4 = (bf16[96,2048]{1,0:T(8,128)(2,1)S(1)}, bf16[96,2048]{1,0:T(8,128)(2,1)S(1)}, u32[]{:S(2)}, u32[]{:S(2)}) collective-permute-start(bf16[96,2048]{1,0:T(8,128)(2,1)S(1)} %pad_maximum_fusion.1), channel_id=1, source_target_pairs={{0,3},{1,0},{2,1},{3,2},{4,7},{5,4},{6,5},{7,6},{8,11},{9,8},{10,9... | collective-permute-start | bytes 1179656 | tf_op jit(solution)/shard_map/ppermute | solution.py:500
  (10 other events, 8.8 us)

commit v2 on v1

v2 whole, which is shorter than its diff:
```python
import jax
import jax.numpy as jnp
from jax import lax
from jax.experimental import pallas as pl
from jax.experimental.pallas import tpu as pltpu
from jax.sharding import Mesh
from jax.sharding import PartitionSpec as P


HEAD_DIM = 64
STATE = 128
CAP = 16
EP = ("ep_0", "ep_1", "ep_2")
PLANE = ("ep_1", "ep_2")
EP_TP = ("ep_0", "ep_1", "ep_2", "tp")
EPS = 1e-06
F32 = jnp.float32
BF16 = jnp.bfloat16
MIB = 1024 * 1024
BIG = 56
MID = 24


def vmem(count):
    return [pl.BlockSpec(memory_space=pltpu.VMEM)] * count


def params(mib):
    return pltpu.CompilerParams(vmem_limit_bytes=mib * MIB)


def cost(flops, nbytes):
    return pl.CostEstimate(flops=flops, bytes_accessed=nbytes, transcendentals=0)


def iota(shape, dim):
    return lax.broadcasted_iota(jnp.int32, shape, dim)


def spread_heads(group, heads, width):
    per = width // HEAD_DIM
    return (iota((heads, width), 0) == group * per + iota((heads, width), 1) // HEAD_DIM).astype(F32)


def dot(a, b, precision=None):
    return jnp.dot(a, b, preferred_element_type=F32, precision=precision)


def dot_tn(a, b):
    return lax.dot_general(a, b, (((0,), (0,)), ((), ())), preferred_element_type=F32)


def dot_nt(a, b):
    return lax.dot_general(a, b, (((1,), (1,)), ((), ())), preferred_element_type=F32)


def silu(x):
    return 0.5 * x * (1.0 + jnp.tanh(0.5 * x))


def split3(x):
    high = x.astype(BF16)
    rest = x - high.astype(F32)
    middle = rest.astype(BF16)
    low = (rest - middle.astype(F32)).astype(BF16)
    return jnp.concatenate([high, middle, low], axis=0)


def to_lanes(terms, mask):
    return dot_tn(terms, jnp.concatenate([mask.astype(BF16)] * 3, axis=0))


def to_column(row):
    n = row.shape[1]
    return jnp.sum(jnp.where(iota((n, n), 0) == iota((n, n), 1), row, 0.0), axis=1, keepdims=True)


def conv_kernel(
    place_ref, ch_ref, wr_ref, rd_ref, edge_ref, ct_ref, wt_ref, rt_ref, sraw_ref, extra_ref, bias_ref, rate_ref,
    x_ref, w_ref, r_ref, cum_ref, step_ref, *rest,
):
    *block_refs, pay_ref = rest
    heads, length = sraw_ref.shape
    tile = 128

    def conv(src, taps, dst, first):
        def body(i, carry):
            lanes = pl.ds(pl.multiple_of(i * tile, tile), tile)
            edges = edge_ref[:, pl.ds(pl.multiple_of(first + i * tile, tile), tile)].astype(F32)
            joined = jnp.concatenate([edges[8:16], src[:, lanes].astype(F32)], axis=0)
            t = taps[:, lanes]
            total = t[0:1] * joined[5 : 5 + length]
            for k in range(1, t.shape[0]):
                total = total + t[k : k + 1] * joined[5 + k : 5 + k + length]
            dst[:, lanes] = silu(total).astype(BF16)
            return carry

        lax.fori_loop(0, src.shape[1] // tile, body, 0)

    nch, nw = ch_ref.shape[1], wr_ref.shape[1]
    conv(ch_ref, ct_ref, x_ref, 0)
    conv(wr_ref, wt_ref, w_ref, nch)
    conv(rd_ref, rt_ref, r_ref, nch + nw)

    raw = sraw_ref[...].astype(F32) + to_column(bias_ref[...])
    step = jnp.maximum(raw, 0.0) + jnp.log1p(jnp.exp(-jnp.abs(raw)))
    decay = extra_ref[...] - step * to_column(jnp.exp(rate_ref[...]))
    upto = jnp.where(iota((length, length), 0) <= iota((length, length), 1), 1.0, 0.0).astype(BF16)
    sums = dot(split3(decay), upto)
    cum = sums[0:heads] + sums[heads : 2 * heads] + sums[2 * heads :]
    cum_ref[...] = cum
    step_ref[...] = step
    last = cum[:, length - 1 : length]
    tail = split3(jnp.exp(last - cum) * step)
    last = split3(jnp.broadcast_to(last, (heads, 128)))
    groups = nw // STATE
    width = nch // groups
    parts = pay_ref.shape[0]
    rows = STATE // parts
    his, los = [], []
    for g in range(groups):
        spread = spread_heads(g, heads, width)
        xt = (x_ref[:, g * width : (g + 1) * width].astype(F32) * to_lanes(tail, spread)).astype(BF16)
        state = dot_tn(w_ref[:, g * STATE : (g + 1) * STATE], xt).astype(BF16)
        pay_ref[:, g * rows : (g + 1) * rows, :] = state.reshape(parts, rows, width)
        total = to_lanes(last, spread)[0:1]
        high = total.astype(BF16).astype(F32)
        his.append(high)
        los.append(total - high)
    extra_rows = jnp.concatenate(his + los + [jnp.zeros((16 - 2 * groups, width), F32)], axis=0).astype(BF16)
    for p in range(parts):
        pay_ref[p, groups * rows :, :] = extra_rows
    for d in range(parts):
        block_refs[d][...] = pay_ref[jnp.bitwise_xor(place_ref[0], d)]


def within_kernel(x_ref, w_ref, r_ref, cum_ref, step_ref, direct_ref, y_ref):
    g = pl.program_id(0)
    heads, length = cum_ref.shape
    width = x_ref.shape[1]
    per = width // HEAD_DIM
    block = 128
    pick = iota((heads, 128), 0) == g * per + iota((heads, 128), 1)
    cols = to_lanes(split3(cum_ref[...]), pick.astype(F32))
    spread = spread_heads(g, heads, width)
    x = x_ref[...].astype(F32)
    xs = (x * to_lanes(split3(step_ref[...]), spread)).astype(BF16)
    direct = to_lanes(split3(jnp.broadcast_to(to_column(direct_ref[...]), (heads, 128))), spread)[0:1]
    first_half = iota((block, 128), 1) < HEAD_DIM
    causal = iota((block, block), 0) >= iota((block, block), 1)
    rows = [cum_ref[pl.ds(g * per + j, 1), :] for j in range(per)]
    for i in range(length // block):
        here = slice(i * block, (i + 1) * block)
        seen = (i + 1) * block
        gram = dot_nt(r_ref[here, :], w_ref[0:seen, :])
        outs = []
        for j in range(per):
            gap = cols[here, j : j + 1] - rows[j][:, 0:seen]
            edge = jnp.where(causal, gap[:, i * block :], -1e30)
            if i:
                gap = jnp.concatenate([gap[:, : i * block], edge], axis=1)
            else:
                gap = edge
            m = (gram * jnp.exp(gap)).astype(BF16)
            pair = (j // 2) * 128
            outs.append(dot(m, xs[0:seen, pair : pair + 128]))
        for q in range(per // 2):
            lanes = slice(q * 128, (q + 1) * 128)
            y_ref[here, lanes] = (
                jnp.where(first_half, outs[2 * q], outs[2 * q + 1]) + direct[:, lanes] * x[here, lanes]
            )


def plane_kernel(place_ref, *refs):
    *block_refs, before_ref, total_ref, z_ref = refs
    parts, height, width = z_ref.shape
    for d in range(parts):
        z_ref[jnp.bitwise_xor(place_ref[0], d)] = block_refs[d][...]
    groups = 4
    rows = (height - 16) // groups
    base = groups * rows
    his, los = [], []
    for g in range(groups):
        run = jnp.zeros((rows, width), F32)
        log = jnp.zeros((1, width), F32)
        here = slice(g * rows, (g + 1) * rows)
        for p in range(parts):
            before_ref[p, here, :] = run
            before_ref[p, base + g : base + g + 1, :] = log
            pad = z_ref[p, base : base + 16, :].astype(F32)
            own = pad[g : g + 1] + pad[groups + g : groups + g + 1]
            run = jnp.exp(own) * run + z_ref[p, here, :].astype(F32)
            log = log + own
        total_ref[here, :] = run.astype(BF16)
        high = log.astype(BF16).astype(F32)
        his.append(high)
        los.append(log - high)
    total_ref[base:, :] = jnp.concatenate(
        his + los + [jnp.zeros((16 - 2 * groups, width), F32)], axis=0
    ).astype(BF16)


def unpack_logs(ref, groups, base):
    pad = ref[base : base + 16, :].astype(F32)
    return pad[0:groups] + pad[groups : 2 * groups]


def double_kernel(later_ref, earlier_ref, out_ref):
    height, width = out_ref.shape
    groups = 4
    rows = (height - 16) // groups
    base = groups * rows
    later = unpack_logs(later_ref, groups, base)
    for g in range(groups):
        here = slice(g * rows, (g + 1) * rows)
        grown = jnp.exp(later[g : g + 1]) * earlier_ref[here, :].astype(F32)
        out_ref[here, :] = (grown + later_ref[here, :].astype(F32)).astype(BF16)
    total = later + unpack_logs(earlier_ref, groups, base)
    high = total.astype(BF16).astype(F32)
    out_ref[base:, :] = jnp.concatenate(
        [high, total - high, jnp.zeros((16 - 2 * groups, width), F32)], axis=0
    ).astype(BF16)


def enter_kernel(before_ref, later_ref, earlier_ref, out_ref):
    height, _ = later_ref.shape
    parts = before_ref.shape[0]
    groups = 4
    rows = (height - 16) // groups
    base = groups * rows
    later = unpack_logs(later_ref, groups, base)
    for g in range(groups):
        here = slice(g * rows, (g + 1) * rows)
        grown = jnp.exp(later[g : g + 1]) * earlier_ref[here, :].astype(F32)
        state = grown + later_ref[here, :].astype(F32)
        for p in range(parts):
            log = before_ref[p, base + g : base + g + 1, :]
            out_ref[p, here, :] = (before_ref[p, here, :] + jnp.exp(log) * state).astype(BF16)


def project_kernel(
    me_ref, y_ref, r_ref, s_ref, cum_ref, gate_ref, wo_ref,
    own_ref, up_ref, down_ref, opa_ref, opb_ref, natural_ref, gated_ref,
):
    heads, length = cum_ref.shape
    n = 4
    part = length // n
    groups = r_ref.shape[1] // STATE
    width = y_ref.shape[1] // groups

    @pl.when(pl.program_id(0) == 0)
    def _():
        me = me_ref[0]
        grown = split3(jnp.exp(cum_ref[...]))
        for g in range(groups):
            lanes = slice(g * width, (g + 1) * width)
            state = s_ref[:, g * 16 : (g + 1) * 16, :].reshape(STATE, width)
            carried = dot(r_ref[:, g * STATE : (g + 1) * STATE], state)
            y = y_ref[:, lanes] + to_lanes(grown, spread_heads(g, heads, width)) * carried
            natural_ref[:, lanes] = (y * silu(gate_ref[:, lanes].astype(F32))).astype(BF16)
        for k in range(n):
            rows = pl.ds(pl.multiple_of(lax.rem(me + k, n) * part, part), part)
            gated_ref[k * part : (k + 1) * part, :] = natural_ref[rows, :]

    out = dot(gated_ref[...], wo_ref[...]).astype(BF16)
    own_ref[...] = out[0:part]
    up_ref[...] = out[part : 2 * part]
    opa_ref[...] = out[2 * part : 2 * part + part // 2]
    opb_ref[...] = out[2 * part + part // 2 : 3 * part]
    down_ref[...] = out[3 * part : 4 * part]


def norm_kernel(own_ref, u_ref, d_ref, gain_ref, out_ref):
    total = own_ref[...].astype(F32) + u_ref[...].astype(F32) + d_ref[...].astype(F32)
    mean = jnp.mean(total * total, axis=-1, keepdims=True)
    out_ref[...] = (total * lax.rsqrt(mean + EPS) * gain_ref[...]).astype(BF16)


def dispatch_kernel(
    me_ref, tok_ref, gain_ref, routes_ref, ch_ref, wr_ref, rd_ref, out_ref, dest_ref, edge_ref, normed_ref
):
    count = tok_ref.shape[0]
    slots, quarter = out_ref.shape
    experts = slots // CAP
    nch, nw = ch_ref.shape[1], wr_ref.shape[1]
    edge_ref[:, 0:nch] = ch_ref[...]
    edge_ref[:, nch : nch + nw] = wr_ref[...]
    edge_ref[:, nch + nw :] = rd_ref[...]
    v = tok_ref[...].astype(F32)
    mean = jnp.mean(v * v, axis=-1, keepdims=True)
    normed_ref[...] = (v * lax.rsqrt(mean + EPS) * gain_ref[...]).astype(BF16)
    ids = iota((experts, count), 0)
    is_first, is_second = ids == routes_ref[0:1, :], ids == routes_ref[1:2, :]
    named = jnp.where(is_first | is_second, 1.0, 0.0).astype(BF16)
    before = jnp.where(iota((count, count), 0) < iota((count, count), 1), 1.0, 0.0).astype(BF16)
    place = dot(named, before) + (ids * CAP).astype(F32)
    dest0 = jnp.sum(jnp.where(is_first, place, 0.0), axis=0, keepdims=True).astype(jnp.int32)
    dest1 = jnp.sum(jnp.where(is_second, place, 0.0), axis=0, keepdims=True).astype(jnp.int32)
    dest_ref[0:1, :] = dest0
    dest_ref[1:2, :] = dest1
    slot = iota((slots, count), 0)
    chosen = jnp.where((slot == dest0) | (slot == dest1), 1.0, 0.0).astype(BF16)
    lanes = pl.ds(pl.multiple_of(me_ref[0] * quarter, quarter), quarter)
    out_ref[...] = dot(chosen, normed_ref[:, lanes]).astype(BF16)


def combine_kernel(back_ref, dest_ref, weight_ref, out_ref):
    count = dest_ref.shape[1]
    slot = iota((back_ref.shape[0], count), 0)
    mix = jnp.where(slot == dest_ref[0:1, :], weight_ref[0:1, :], 0.0) + jnp.where(
        slot == dest_ref[1:2, :], weight_ref[1:2, :], 0.0
    )
    high = mix.astype(BF16)
    low = (mix - high.astype(F32)).astype(BF16)
    back = back_ref[...]
    out_ref[...] = (dot_tn(high, back) + dot_tn(low, back)).astype(BF16)


def hidden_kernel(me_ref, own, left, right, op0, op1, gate_ref, up_ref, out_ref):
    me = me_ref[0]
    size = own.shape[1]
    opposite = jnp.where(pl.program_id(0) < pl.num_programs(0) // 2, op0[...], op1[...])

    def product(w):
        def rows(shift):
            return pl.ds(pl.multiple_of(lax.rem(me + shift, 4) * size, size), size)

        total = dot(own[...], w[rows(0), :]) + dot(left[...], w[rows(3), :])
        return total + dot(right[...], w[rows(1), :]) + dot(opposite, w[rows(2), :])

    out_ref[...] = (silu(product(gate_ref)) * product(up_ref)).astype(BF16)


def result_kernel(me_ref, own, left, right, op0, op1, down_own, down_left, down_right, down_cross, out_ref):
    opposite = jnp.where(pl.program_id(0) < pl.num_programs(0) // 2, op0[...], op1[...])
    total = dot(own[...], down_own[...]) + dot(left[...], down_left[...])
    total = total + dot(right[...], down_right[...]) + dot(opposite, down_cross[...])
    out_ref[...] = total.astype(BF16)


def ring_pieces(x, axis):
    n = lax.axis_size(axis)
    plus = [(i, (i + 1) % n) for i in range(n)]
    minus = [(i, (i - 1) % n) for i in range(n)]
    half = x.shape[0] // 2
    left = lax.ppermute(x, axis, plus)
    right = lax.ppermute(x, axis, minus)
    op0 = lax.ppermute(left[:half], axis, plus)
    op1 = lax.ppermute(right[half:], axis, minus)
    return x, left, right, op0, op1


def ring_call(kernel, me, pieces, weights, columns, tile):
    rows = pieces[0].shape[0]
    steps = rows // tile
    smem = pl.BlockSpec(memory_space=pltpu.SMEM)
    specs = [smem]
    specs += [pl.BlockSpec((tile, p.shape[1]), lambda i: (i, 0)) for p in pieces[:3]]
    specs.append(pl.BlockSpec((tile, pieces[3].shape[1]), lambda i: (jnp.minimum(i, steps // 2 - 1), 0)))
    specs.append(pl.BlockSpec((tile, pieces[4].shape[1]), lambda i: (jnp.maximum(i - steps // 2, 0), 0)))
    specs += [pl.BlockSpec(w.shape, lambda i: (0, 0)) for w in weights]
    depth = sum(w.shape[0] for w in weights)
    return pl.pallas_call(
        kernel,
        grid=(steps,),
        in_specs=specs,
        out_specs=pl.BlockSpec((tile, columns), lambda i: (i, 0)),
        out_shape=jax.ShapeDtypeStruct((rows, columns), BF16),
        compiler_params=params(MID),
        cost_estimate=cost(2 * rows * depth * columns, rows * depth * 2),
    )(me, *pieces, *weights)


def per_device(
    mixer_channels_raw,
    write_vectors_raw,
    read_vectors_raw,
    gate_logits,
    step_size_raw,
    extra_log_decay,
    mixer_conv_taps,
    write_conv_taps,
    read_conv_taps,
    step_size_bias,
    log_decay_rate,
    direct_path_weight,
    mixer_output_weight,
    mixer_norm_scale,
    routed_tokens,
    expert_norm_scale,
    routes,
    routing_weights,
    expert_gate_matrix,
    expert_up_matrix,
    expert_down_matrix,
):
    sds = jax.ShapeDtypeStruct
    smem = pl.BlockSpec(memory_space=pltpu.SMEM)
    tp = lax.axis_index("tp")
    me = tp.reshape(1).astype(jnp.int32)
    tps = lax.axis_size("tp")
    plus = [(i, (i + 1) % tps) for i in range(tps)]
    minus = [(i, (i - 1) % tps) for i in range(tps)]
    cross = [(i, (i + 2) % tps) for i in range(tps)]

    tokens, model = routed_tokens.shape
    experts = lax.axis_size(EP)
    slots = experts * CAP
    quarter = model // tps
    length, channels = mixer_channels_raw.shape
    nw = write_vectors_raw.shape[1]
    last_rows = lambda a: pl.BlockSpec((16, a.shape[1]), lambda i: (a.shape[0] // 16 - 1, 0))
    entire = lambda shape: pl.BlockSpec(shape, lambda i: (0,) * len(shape))
    outgoing, dest, edge = pl.pallas_call(
        dispatch_kernel,
        grid=(1,),
        in_specs=[smem, entire((tokens, model)), entire((1, model)), entire((2, tokens))]
        + [last_rows(a) for a in (mixer_channels_raw, write_vectors_raw, read_vectors_raw)],
        out_specs=[entire((slots, quarter)), entire((2, tokens)), entire((16, channels + 2 * nw))],
        out_shape=(
            sds((slots, quarter), BF16),
            sds((2, tokens), jnp.int32),
            sds((16, channels + 2 * nw), BF16),
        ),
        scratch_shapes=[pltpu.VMEM((tokens, model), BF16)],
        compiler_params=params(BIG),
        cost_estimate=cost(2 * slots * tokens * quarter, 4 * MIB),
        name="dispatch",
    )(
        me,
        routed_tokens,
        expert_norm_scale[None, :],
        routes.T,
        mixer_channels_raw,
        write_vectors_raw,
        read_vectors_raw,
    )
    arrived = lax.all_to_all(
        outgoing.reshape(experts, CAP, quarter), EP, split_axis=0, concat_axis=0, tiled=True
    )
    arrived = arrived.reshape(slots, quarter)

    ff = expert_down_matrix.shape[1]
    down = expert_down_matrix[0]

    def feature_block(shift):
        return lax.dynamic_slice(down, (0, lax.rem(tp + shift, tps) * quarter), (ff, quarter))

    d_own = feature_block(0)
    d_left = lax.ppermute(feature_block(1), "tp", plus)
    d_right = lax.ppermute(feature_block(3), "tp", minus)
    d_cross = lax.ppermute(feature_block(2), "tp", cross)

    heads = step_size_raw.shape[1]
    groups = nw // STATE
    width = channels // groups
    edge = lax.ppermute(edge, EP, [(i, i + 1) for i in range(experts - 1)])
    place = lax.axis_index(PLANE).reshape(1).astype(jnp.int32)
    parts = lax.axis_size(PLANE)
    height = groups * (STATE // parts) + 16
    x, w, r, cum, step, *blocks = pl.pallas_call(
        conv_kernel,
        in_specs=[smem] + vmem(11),
        out_specs=vmem(5 + parts),
        out_shape=(
            sds((length, channels), BF16),
            sds((length, nw), BF16),
            sds((length, nw), BF16),
            sds((heads, length), F32),
            sds((heads, length), F32),
        )
        + (sds((height, width), BF16),) * parts,
        scratch_shapes=[pltpu.VMEM((parts, height, width), BF16)],
        compiler_params=params(BIG),
        cost_estimate=cost(2 * length * STATE * channels * 8, 4 * MIB),
        name="conv",
    )(
        place,
        mixer_channels_raw,
        write_vectors_raw,
        read_vectors_raw,
        edge,
        mixer_conv_taps,
        write_conv_taps,
        read_conv_taps,
        step_size_raw.T,
        extra_log_decay.T,
        step_size_bias[None, :],
        log_decay_rate[None, :],
    )
    for d in range(1, parts):
        blocks[d] = lax.ppermute(blocks[d], PLANE, [(i, i ^ d) for i in range(parts)])
    before, total = pl.pallas_call(
        plane_kernel,
        in_specs=[smem] + vmem(parts),
        out_specs=vmem(2),
        out_shape=(sds((parts, height, width), F32), sds((height, width), BF16)),
        scratch_shapes=[pltpu.VMEM((parts, height, width), BF16)],
        compiler_params=params(MID),
        cost_estimate=cost(1000000, MIB),
        name="plane",
    )(place, *blocks)
    planes = lax.axis_size("ep_0")

    def from_below(value, shift):
        return lax.ppermute(value, "ep_0", [(i, i + shift) for i in range(planes - shift)])

    later = from_below(total, 1)
    shift = 1
    while 2 * shift < planes:
        earlier = from_below(later, shift)
        later = pl.pallas_call(
            double_kernel,
            in_specs=vmem(2),
            out_specs=vmem(1)[0],
            out_shape=sds((height, width), BF16),
            compiler_params=params(MID),
            cost_estimate=cost(200000, MIB // 8),
            name="double",
        )(later, earlier)
        shift *= 2
    earlier = from_below(later, shift)
    entering = pl.pallas_call(
        enter_kernel,
        in_specs=vmem(3),
        out_specs=vmem(1)[0],
        out_shape=sds((parts, height - 16, width), BF16),
        compiler_params=params(MID),
        cost_estimate=cost(1000000, MIB),
        name="enter",
    )(before, later, earlier)
    entering = lax.all_to_all(entering, PLANE, 0, 0, tiled=True)

    y = pl.pallas_call(
        within_kernel,
        grid=(groups,),
        in_specs=[
            pl.BlockSpec((length, width), lambda g: (0, g)),
            pl.BlockSpec((length, STATE), lambda g: (0, g)),
            pl.BlockSpec((length, STATE), lambda g: (0, g)),
            pl.BlockSpec((heads, length), lambda g: (0, 0)),
            pl.BlockSpec((heads, length), lambda g: (0, 0)),
            pl.BlockSpec((1, heads), lambda g: (0, 0)),
        ],
        out_specs=pl.BlockSpec((length, width), lambda g: (0, g)),
        out_shape=sds((length, channels), F32),
        compiler_params=params(BIG),
        cost_estimate=cost(4 * length * length * channels, 4 * MIB),
        name="within",
    )(x, w, r, cum, step, direct_path_weight[None, :])

    out_dim = mixer_output_weight.shape[1]
    part = length // tps
    tile = 512
    row_block = lambda rows: pl.BlockSpec((rows, tile), lambda j: (0, j))
    whole = lambda a: pl.BlockSpec(a.shape, lambda j: (0,) * a.ndim)
    own, up, dn, opa, opb = pl.pallas_call(
        project_kernel,
        grid=(out_dim // tile,),
        in_specs=[smem]
        + [whole(a) for a in (y, r, entering, cum, gate_logits)]
        + [pl.BlockSpec((channels, tile), lambda j: (0, j))],
        out_specs=(row_block(part), row_block(part), row_block(part), row_block(part // 2), row_block(part // 2)),
        out_shape=(
            sds((part, out_dim), BF16),
            sds((part, out_dim), BF16),
            sds((part, out_dim), BF16),
            sds((part // 2, out_dim), BF16),
            sds((part // 2, out_dim), BF16),
        ),
        scratch_shapes=[pltpu.VMEM((length, channels), BF16)] * 2,
        compiler_params=params(MID),
        cost_estimate=cost(2 * length * channels * out_dim, 6 * MIB),
        name="project",
    )(me, y, r, entering, cum, gate_logits, mixer_output_weight)
    opa = lax.ppermute(opa, "tp", plus)
    opb = lax.ppermute(opb, "tp", minus)
    half = part // 2
    up = jnp.concatenate([(up[:half].astype(F32) + opa.astype(F32)).astype(BF16), up[half:]], axis=0)
    dn = jnp.concatenate([dn[:half], (dn[half:].astype(F32) + opb.astype(F32)).astype(BF16)], axis=0)
    up = lax.ppermute(up, "tp", plus)
    dn = lax.ppermute(dn, "tp", minus)
    mixer_out = pl.pallas_call(
        norm_kernel,
        in_specs=vmem(4),
        out_specs=vmem(1)[0],
        out_shape=sds((part, out_dim), BF16),
        compiler_params=params(MID),
        cost_estimate=cost(1000000, 2 * MIB),
        name="norm",
    )(own, up, dn, mixer_norm_scale[None, :])

    pieces = ring_pieces(arrived, "tp")
    hidden = ring_call(hidden_kernel, me, pieces, (expert_gate_matrix[0], expert_up_matrix[0]), ff, 512)
    pieces = ring_pieces(hidden, "tp")
    result = ring_call(result_kernel, me, pieces, (d_own, d_left, d_right, d_cross), quarter, 512)
    returned = lax.all_to_all(
        result.reshape(experts, CAP, quarter), EP, split_axis=0, concat_axis=0, tiled=True
    )
    returned = returned.reshape(slots, quarter)
    expert_out = pl.pallas_call(
        combine_kernel,
        in_specs=vmem(3),
        out_specs=vmem(1)[0],
        out_shape=sds((tokens, quarter), BF16),
        compiler_params=params(MID),
        cost_estimate=cost(4 * slots * tokens * quarter, 2 * MIB),
        name="combine",
    )(returned, dest, routing_weights.T)
    return (mixer_out, expert_out)


def solution(mesh):
    split = Mesh(mesh.devices.reshape(8, 4, 2, mesh.shape["tp"]), EP_TP)
    placed = (
        P(EP, "tp"),
        P(EP, "tp"),
        P(EP, "tp"),
        P(EP, "tp"),
        P(EP, "tp"),
        P(EP, "tp"),
        P(None, "tp"),
        P(None, "tp"),
        P(None, "tp"),
        P("tp"),
        P("tp"),
        P("tp"),
        P("tp", None),
        P(),
        P(EP, None),
        P(),
        P(EP, None),
        P(EP, None),
        P(EP, None, "tp"),
        P(EP, None, "tp"),
        P(EP, "tp", None),
    )

    return jax.shard_map(
        per_device,
        mesh=split,
        in_specs=placed,
        out_specs=(P(EP_TP, None), P(EP, "tp")),
        check_vma=False,
    )
```

time: 200 us -> 201 us (level)
  local copies, waits for them, and re-layouts: 32.5 us -> 10.3 us
  starting transfers between devices: 50.3 us -> 69.8 us
  waiting for transfers between devices: 38.9 us -> 47.8 us
  Pallas kernels: 33.1 us -> 29.3 us
    ppermute x4 -> x15, starting transfers between devices: 5.35 us -> 38.6 us  [the longest x4 21.4 us: from_below(): lax.ppermute(value, 'ep_0', [(i, i + shift) for i in range(planes - shift)])]
    unnamed x74 -> x30, local copies, waits for them, and re-layouts: 22.7 us -> 6.64 us
    ppermute x4 -> x15, waiting for transfers between devices: 0.01 us -> 12.1 us  [the longest x2 4.83 us: ring_pieces(): op0 = lax.ppermute(left[:half], axis, plus)]
    all_to_all x2 -> x0, starting transfers between devices: 11.5 us -> none  [the longest x1 6.1 us: per_device(): lax.all_to_all(jnp.broadcast_to(total[None], (zs, height, width)), 'ep_0'...]
    slice x10 -> x4, local copies, waits for them, and re-layouts: 5.02 us -> 1.51 us  [the longest x2 0.76 us: ring_pieces(): op1 = lax.ppermute(right[half:], axis, minus)]
    all_to_all x1, starting transfers between devices: 8.89 us -> 5.38 us  [per_device(): lax.all_to_all(result.reshape(experts, CAP, quarter), EP, split_axis=0, c...]
    dynamic_update_slice x3 -> x0, local copies, waits for them, and re-layouts: 2.9 us -> none  [per_device(): lax.dynamic_update_slice(stacked, block[None], (lax.rem(tp + shift, tps),...]
    ppermute x1, waiting for transfers between devices: 2.75 us -> 0.01 us  [per_device(): d_left = lax.ppermute(feature_block(1), 'tp', plus)]
  transfers between devices with their start and end apart: 20 -> 29, of which waited for: 6 -> 11; matrix products, arithmetic and copies ran while one was open for 5% -> 2% of each run, Pallas kernels for 15% -> 12%
where the time goes in v2:
time: 201 us; the launch traced here: 200 us
  starting transfers between devices  69.8 us (35%)
  waiting for transfers between devices  47.8 us (24%)
  blocking collectives  41.4 us (21%)
  Pallas kernels  29.3 us (15%)
  local copies, waits for them, and re-layouts  10.3 us (5%)
    all_to_all x1, blocking collectives, per_device(): lax.all_to_all(outgoing.reshape(experts, CAP, quarter), EP, split_axis=0,...  41.4 us
    ppermute x2, waiting for transfers between devices, ring_pieces(): left = lax.ppermute(x, axis, plus)  22.1 us
    ppermute x4, starting transfers between devices, from_below(): lax.ppermute(value, 'ep_0', [(i, i + shift) for i in range(planes - shift)])  21.4 us
    ppermute x7, starting transfers between devices, per_device(): lax.ppermute(blocks[d], PLANE, [(i, i ^ d) for i in range(parts)])  11.7 us
    ppermute x1, waiting for transfers between devices, per_device(): up = lax.ppermute(up, 'tp', plus)  7.73 us
    all_to_all x1, starting transfers between devices, per_device(): entering = lax.all_to_all(entering, PLANE, 0, 0, tiled=True)  7.06 us
    unnamed x30, local copies, waits for them, and re-layouts  6.64 us
    pallas_call x1, Pallas kernels, per_device(): pl.pallas_call(conv_kernel, in_specs=[smem] + vmem(11), out_specs=vmem(5...  6.36 us
  transfers between devices with their start and end apart: 29, of which 11 were waited for; matrix products, arithmetic and copies ran while one was open for 2% of the time, Pallas kernels for 12%

profile of v2, /device:TPU:1, one launch (start us, length us, event | category | flops | bytes accessed | tf_op | source)
XLA Modules:
  0.0 199.8 jit_solution(8654467582352623160)
XLA Ops:
  0.7 3.5 %dispatch.1 = (bf16[1024,512]{1,0:T(8,128)(2,1)}, s32[2,256]{1,0:T(2,128)}, bf16[16,2048]{1,0:T(8,128)(2,1)}) custom-call(s32[1]{0:T(128)} %bitcast.me_ref, bf16[256,2048]{1,0:T(8,128)(2,1)} %tok_ref.1, f32[1,2048]{1,0:T(1,128)} %bitcast.34, s32[2,256]{1,0:T(2,128)} %bitcast.35, bf16[384,1024]{1,0:T(8,128)(2,1)} %ch_ref.3, bf16[384,512]{1,0:T(8,128)(2,1)} %wr_ref.3, ...), custom_call_target="tpu_custom_call" | custom-call | flops 268435456 | bytes 4194304 | tf_op jit(solution)/shard_map/dispatch/pallas_call | solution.py:414
  4.1 41.4 %all_to_all.15 = bf16[64,16,512]{2,1,0:T(8,128)(2,1)S(1)} all-to-all(bf16[64,16,512]{2,1,0:T(8,128)(2,1)} %bitcast.33), channel_id=1, replica_groups=mesh['ep_0'=8,'ep_1'=4,'ep_2'=2,'tp'=4] {'ep_0','ep_1','ep_2'}, dimensions={0} | all-to-all | bytes 2097152 | tf_op jit(solution)/shard_map/all_to_all | solution.py:438
  45.6 1.2 collective-permute-start.16
  46.8 1.5 collective-permute-start.17
  48.3 22.1 %collective-permute-done.16.left = bf16[1024,512]{1,0:T(8,128)(2,1)S(1)} collective-permute-done((bf16[1024,512]{1,0:T(8,128)(2,1)S(1)}, bf16[1024,512]{1,0:T(8,128)(2,1)S(1)}, u32[]{:S(2)}, u32[]{:S(2)}) %collective-permute-start.16) | collective-permute-done | bytes 1048608 | tf_op jit(solution)/shard_map/ppermute | solution.py:346
  70.5 2.7 %collective-permute-start.19 = (bf16[512,512]{1,0:T(8,128)(2,1)S(1)}, bf16[512,512]{1,0:T(8,128)(2,1)S(1)}, u32[]{:S(2)}, u32[]{:S(2)}) collective-permute-start(bf16[512,512]{1,0:T(8,128)(2,1)S(1)} %slice.33), channel_id=1, source_target_pairs={{0,3},{1,0},{2,1},{3,2},{4,7},{5,4},{6,5},{7,6},{8,11},{9,8},{10,9... | collective-permute-start | bytes 1572872 | tf_op jit(solution)/shard_map/ppermute | solution.py:349
  73.3 5.1 %collective-permute-start = (bf16[16,2048]{1,0:T(8,128)(2,1)S(1)}, bf16[16,2048]{1,0:T(8,128)(2,1)S(1)}, u32[]{:S(2)}, u32[]{:S(2)}) collective-permute-start(bf16[16,2048]{1,0:T(8,128)(2,1)S(1)} %copy-done.13), channel_id=1, source_target_pairs={{0,4},{4,8},{8,12},{12,16},{16,20},{20,24},{24,28},{28,32},{32,36}... | collective-permute-start | bytes 196616 | tf_op jit(solution)/shard_map/ppermute | solution.py:457
  78.3 4.8 %collective-permute-done.18.op0 = bf16[512,512]{1,0:T(8,128)(2,1)S(1)} collective-permute-done((bf16[512,512]{1,0:T(8,128)(2,1)S(1)}, bf16[512,512]{1,0:T(8,128)(2,1)S(1)}, u32[]{:S(2)}, u32[]{:S(2)}) %collective-permute-start.18) | collective-permute-done | bytes 524320 | tf_op jit(solution)/shard_map/ppermute | solution.py:348
  83.2 2.6 %shard_map.212.own = bf16[1024,256]{1,0:T(8,128)(2,1)S(1)} custom-call(s32[1]{0:T(128)} %bitcast.me_ref, bf16[1024,512]{1,0:T(8,128)(2,1)S(1)} %bitcast.28, bf16[1024,512]{1,0:T(8,128)(2,1)S(1)} %collective-permute-done.16.left, bf16[1024,512]{1,0:T(8,128)(2,1)S(1)} %collective-permute-done.17.right, bf16[512,512]{1,0:T(8,128)(2,1)S(1)} %collective-permute-done.18.op0, ...), custom_call_target="tpu_custom_call" | custom-call | flops 2147483648 | bytes 8388608 | tf_op jit(solution)/shard_map/pallas_call | solution.py:363
  85.8 2.7 %collective-permute-start.21 = (bf16[1024,256]{1,0:T(8,128)(2,1)S(1)}, bf16[1024,256]{1,0:T(8,128)(2,1)S(1)}, u32[]{:S(2)}, u32[]{:S(2)}) collective-permute-start(bf16[1024,256]{1,0:T(8,128)(2,1)S(1)} %shard_map.212.own), channel_id=1, source_target_pairs={{0,3},{1,0},{2,1},{3,2},{4,7},{5,4},{6,5},{7,6},{8,11},{9,8},{10,9... | collective-permute-start | bytes 1572872 | tf_op jit(solution)/shard_map/ppermute | solution.py:347
  89.1 6.4 %conv.1 = (bf16[384,1024]{1,0:T(8,128)(2,1)}, bf16[384,512]{1,0:T(8,128)(2,1)}, bf16[384,512]{1,0:T(8,128)(2,1)}, f32[16,384]{1,0:T(8,128)}, f32[16,384]{1,0:T(8...) custom-call(s32[1]{0:T(128)} %bitcast.1.place_ref, ...), custom_call_target="tpu_custom_call" | custom-call | flops 805306368 | bytes 4194304 | tf_op jit(solution)/shard_map/conv/pallas_call | solution.py:461
  95.5 3.5 %collective-permute-start.1 = (bf16[80,256]{1,0:T(8,128)(2,1)}, bf16[80,256]{1,0:T(8,128)(2,1)S(1)}, u32[]{:S(2)}, u32[]{:S(2)}) collective-permute-start(bf16[80,256]{1,0:T(8,128)(2,1)} %get-tuple-element.32), channel_id=1, source_target_pairs={{0,4},{4,0},{8,12},{12,8},{16,20},{20,16},{24,28},{28,24},{1,5},{5... | collective-permute-start | bytes 122888 | tf_op jit(solution)/shard_map/ppermute | solution.py:492
  99.2 1.5 collective-permute-start.3
  100.7 1.4 collective-permute-start.4
  102.2 2.8 %collective-permute-start.5 = (bf16[80,256]{1,0:T(8,128)(2,1)}, bf16[80,256]{1,0:T(8,128)(2,1)S(1)}, u32[]{:S(2)}, u32[]{:S(2)}) collective-permute-start(bf16[80,256]{1,0:T(8,128)(2,1)} %get-tuple-element.36), channel_id=1, source_target_pairs={{0,20},{4,16},{8,28},{12,24},{16,4},{20,0},{24,12},{28,8},{1,21},{... | collective-permute-start | bytes 122888 | tf_op jit(solution)/shard_map/ppermute | solution.py:492
  105.0 0.8 collective-permute-start.6
  105.8 1.5 collective-permute-start.7
  107.3 2.0 collective-permute-done.6.refs_6_
  109.3 2.0 %collective-permute-done.7.refs_7_ = bf16[80,256]{1,0:T(8,128)(2,1)S(1)} collective-permute-done((bf16[80,256]{1,0:T(8,128)(2,1)}, bf16[80,256]{1,0:T(8,128)(2,1)S(1)}, u32[]{:S(2)}, u32[]{:S(2)}) %collective-permute-start.7) | collective-permute-done | bytes 40992 | tf_op jit(solution)/shard_map/ppermute | solution.py:492
  111.3 0.8 copy-done.7
  112.2 3.4 %collective-permute-start.8 = (bf16[80,256]{1,0:T(8,128)(2,1)S(1)}, bf16[80,256]{1,0:T(8,128)(2,1)S(1)}, u32[]{:S(2)}, u32[]{:S(2)}) collective-permute-start(bf16[80,256]{1,0:T(8,128)(2,1)S(1)} %get-tuple-element.40), channel_id=1, source_target_pairs={{0,32},{32,64},{64,96},{96,128},{128,160},{160,192},{192,224},{1,3... | collective-permute-start | bytes 122888 | tf_op jit(solution)/shard_map/ppermute | solution.py:506
  115.6 1.1 collective-permute-done.8.later_ref
  116.7 3.6 %collective-permute-start.9 = (bf16[80,256]{1,0:T(8,128)(2,1)S(1)}, bf16[80,256]{1,0:T(8,128)(2,1)S(1)}, u32[]{:S(2)}, u32[]{:S(2)}) collective-permute-start(bf16[80,256]{1,0:T(8,128)(2,1)S(1)} %collective-permute-done.8.later_ref), channel_id=1, source_target_pairs={{0,32},{32,64},{64,96},{96,128},{128,160},{160,192},{192,224},{1,3... | collective-permute-start | bytes 122888 | tf_op jit(solution)/shard_map/ppermute | solution.py:506
  120.3 1.1 collective-permute-done.9.earlier_ref
  121.4 5.0 %collective-permute-start.10 = (bf16[80,256]{1,0:T(8,128)(2,1)S(1)}, bf16[80,256]{1,0:T(8,128)(2,1)S(1)}, u32[]{:S(2)}, u32[]{:S(2)}) collective-permute-start(bf16[80,256]{1,0:T(8,128)(2,1)S(1)} %double.2.later_ref), channel_id=1, source_target_pairs={{0,64},{32,96},{64,128},{96,160},{128,192},{160,224},{1,65},{33,97... | collective-permute-start | bytes 122888 | tf_op jit(solution)/shard_map/ppermute | solution.py:506
  126.5 1.1 collective-permute-done.10.earlier_ref
  127.5 9.3 %collective-permute-start.11 = (bf16[80,256]{1,0:T(8,128)(2,1)S(1)}, bf16[80,256]{1,0:T(8,128)(2,1)S(1)}, u32[]{:S(2)}, u32[]{:S(2)}) collective-permute-start(bf16[80,256]{1,0:T(8,128)(2,1)S(1)} %double.3.later_ref), channel_id=1, source_target_pairs={{0,128},{32,160},{64,192},{96,224},{1,129},{33,161},{65,193},{97,2... | collective-permute-start | bytes 122888 | tf_op jit(solution)/shard_map/ppermute | solution.py:506
  136.9 2.1 %dynamic-slice_bitcast_fusion = (bf16[256,512]{1,0:T(8,128)(2,1)}, bf16[256,512]{1,0:T(8,128)(2,1)}, bf16[256,512]{1,0:T(8,128)(2,1)S(1)}, bf16[256,512]{1,0:T(8,128)(2,1)}) fusion(bf16[1,256,2048]{2,1,0:T(8,128)(2,1)} %param.41, s32[]{:T(128)S(6)} %select_n.15, s32[]{:T(128)S(6)} %select_n.13, s32[]{:T(128)S(6)} %select_n.12, s32[]{:T(128)S(6)} %select_n.14), kind=kLoop, calls=%fused_computation.4 | loop fusion | bytes 2097168 | tf_op jit(solution)/shard_map/dynamic_slice | solution.py:447
  139.0 2.7 %collective-permute-start.25 = (bf16[256,512]{1,0:T(8,128)(2,1)}, bf16[256,512]{1,0:T(8,128)(2,1)}, u32[]{:S(2)}, u32[]{:S(2)}) collective-permute-start(bf16[256,512]{1,0:T(8,128)(2,1)} %get-tuple-element.51), channel_id=1, source_target_pairs={{0,3},{1,0},{2,1},{3,2},{4,7},{5,4},{6,5},{7,6},{8,11},{9,8},{10,9... | collective-permute-start | bytes 786440 | tf_op jit(solution)/shard_map/ppermute | solution.py:451
  143.0 0.7 slice.35
  143.7 2.1 %collective-permute-start.23 = (bf16[512,256]{1,0:T(8,128)(2,1)}, bf16[512,256]{1,0:T(8,128)(2,1)}, u32[]{:S(2)}, u32[]{:S(2)}) collective-permute-start(bf16[512,256]{1,0:T(8,128)(2,1)} %slice.35), channel_id=1, source_target_pairs={{0,3},{1,0},{2,1},{3,2},{4,7},{5,4},{6,5},{7,6},{8,11},{9,8},{10,9... | collective-permute-start | bytes 786440 | tf_op jit(solution)/shard_map/ppermute | solution.py:349
  145.8 0.8 enter.1
  146.6 7.1 %all-to-all-start = ((bf16[8,64,256]{2,1,0:T(8,128)(2,1)}), bf16[8,64,256]{2,1,0:T(8,128)(2,1)S(1)}, u32[]{:S(2)}, u32[]{:S(2)}) async-start(bf16[8,64,256]{2,1,0:T(8,128)(2,1)} %enter.1), calls=%async_computation | async-start | bytes 524288 | tf_op jit(solution)/shard_map/all_to_all | solution.py:532
  153.7 6.3 %within.1.y_ref = f32[384,1024]{1,0:T(8,128)} custom-call(bf16[384,1024]{1,0:T(8,128)(2,1)} %get-tuple-element.26.x_ref, bf16[384,512]{1,0:T(8,128)(2,1)} %get-tuple-element.27.w_ref, bf16[384,512]{1,0:T(8,128)(2,1)} %get-tuple-element.28.r_ref, f32[16,384]{1,0:T(8,128)} %get-tuple-element.29.cum_ref, f32[16,384]{1,0:T(8,128)} %get-tuple-element.30.step_ref, ...), custom_call_target="tpu_custom_call" | custom-call | flops 603979776 | bytes 4194304 | tf_op jit(solution)/shard_map/within/pallas_call | solution.py:534
  160.0 1.1 copy-done.5
  161.2 3.5 %shard_map.213 = bf16[1024,512]{1,0:T(8,128)(2,1)} custom-call(s32[1]{0:T(128)} %bitcast.me_ref, bf16[1024,256]{1,0:T(8,128)(2,1)S(1)} %copy-done.5, bf16[1024,256]{1,0:T(8,128)(2,1)S(1)} %collective-permute-done.20.left, bf16[1024,256]{1,0:T(8,128)(2,1)S(1)} %collective-permute-done.21.right, bf16[512,256]{1,0:T(8,128)(2,1)} %collective-permute-done.22.op0, ...), custom_call_target="tpu_custom_call" | custom-call | flops 1073741824 | bytes 2097152 | tf_op jit(solution)/shard_map/pallas_call | solution.py:363
  164.7 5.4 %all-to-all-start.2 = ((bf16[64,16,512]{2,1,0:T(8,128)(2,1)}), bf16[64,16,512]{2,1,0:T(8,128)(2,1)S(1)}, u32[]{:S(2)}, u32[]{:S(2)}) async-start(bf16[64,16,512]{2,1,0:T(8,128)(2,1)} %bitcast.18), calls=%async_computation.2 | async-start | bytes 2097152 | tf_op jit(solution)/shard_map/all_to_all | solution.py:597
  170.1 2.2 %copy-done.1 = bf16[1024,2048]{1,0:T(8,128)(2,1)S(1)} copy-done((bf16[1024,2048]{1,0:T(8,128)(2,1)S(1)}, bf16[1024,2048]{1,0:T(8,128)(2,1)}, u32[]{:S(2)}) %copy-start.1) | copy-done | bytes 4194328
  172.3 1.1 copy-done.3
  173.4 0.7 copy-done.6
  174.2 3.6 %project.1 = (bf16[96,2048]{1,0:T(8,128)(2,1)S(1)}, bf16[96,2048]{1,0:T(8,128)(2,1)S(1)}, bf16[96,2048]{1,0:T(8,128)(2,1)S(1)}, bf16[48,2048]{1,0:T(8,128)(2,1)S(1)}, bf16[48,2048]{1,0:T(8,128)(2,1)S(1)}) custom-call(s32[1]{0:T(128)} %bitcast.me_ref, f32[384,1024]{1,0:T(8,128)S(1)} %copy-done, bf16[384,512]{1,0:T(8,128)(2,1)S(1)} %copy-done.2, ...), custom_call_target="tpu_custom_call" | custom-call | flops 1610612736 | bytes 6291456 | tf_op jit(solution)/shard_map/project/pallas_call | solution.py:557
  177.9 2.7 %collective-permute-start.14 = (bf16[48,2048]{1,0:T(8,128)(2,1)S(1)}, bf16[48,2048]{1,0:T(8,128)(2,1)S(1)}, u32[]{:S(2)}, u32[]{:S(2)}) collective-permute-start(bf16[48,2048]{1,0:T(8,128)(2,1)S(1)} %get-tuple-element.45), channel_id=1, source_target_pairs={{0,3},{1,0},{2,1},{3,2},{4,7},{5,4},{6,5},{7,6},{8,11},{9,8},{10,9... | collective-permute-start | bytes 589832 | tf_op jit(solution)/shard_map/ppermute | solution.py:577
  180.6 4.4 %collective-permute-done.12 = bf16[48,2048]{1,0:T(8,128)(2,1)S(1)} collective-permute-done((bf16[48,2048]{1,0:T(8,128)(2,1)S(1)}, bf16[48,2048]{1,0:T(8,128)(2,1)S(1)}, u32[]{:S(2)}, u32[]{:S(2)}) %collective-permute-start.12) | collective-permute-done | bytes 196640 | tf_op jit(solution)/shard_map/ppermute | solution.py:576
  185.3 2.7 %collective-permute-start.15 = (bf16[96,2048]{1,0:T(8,128)(2,1)S(1)}, bf16[96,2048]{1,0:T(8,128)(2,1)S(1)}, u32[]{:S(2)}, u32[]{:S(2)}) collective-permute-start(bf16[96,2048]{1,0:T(8,128)(2,1)S(1)} %pad_maximum_fusion.1), channel_id=1, source_target_pairs={{0,3},{1,0},{2,1},{3,2},{4,7},{5,4},{6,5},{7,6},{8,11},{9,8},{10,9... | collective-permute-start | bytes 1179656 | tf_op jit(solution)/shard_map/ppermute | solution.py:582
  188.1 7.7 %collective-permute-done.13.u_ref = bf16[96,2048]{1,0:T(8,128)(2,1)S(1)} collective-permute-done((bf16[96,2048]{1,0:T(8,128)(2,1)S(1)}, bf16[96,2048]{1,0:T(8,128)(2,1)S(1)}, u32[]{:S(2)}, u32[]{:S(2)}) %collective-permute-start.13) | collective-permute-done | bytes 393248 | tf_op jit(solution)/shard_map/ppermute | solution.py:581
  195.8 1.1 norm.1
  196.9 1.4 all-to-all-done.2
  198.3 1.5 combine.1
  (64 shorter events, 3.0 us)
Async XLA Ops:
  0.6 82.5 %copy-start.9 = (bf16[1,2048,256]{2,1,0:T(8,128)(2,1)S(1)}, bf16[1,2048,256]{2,1,0:T(8,128)(2,1)}, u32[]{:S(2)}) copy-start(bf16[1,2048,256]{2,1,0:T(8,128)(2,1)} %param.39) | copy-start | bytes 3145732
  0.6 82.5 %copy-start.10 = (bf16[1,2048,256]{2,1,0:T(8,128)(2,1)S(1)}, bf16[1,2048,256]{2,1,0:T(8,128)(2,1)}, u32[]{:S(2)}) copy-start(bf16[1,2048,256]{2,1,0:T(8,128)(2,1)} %param.40) | copy-start | bytes 3145732
  4.1 69.1 %copy-start.13 = (bf16[16,2048]{1,0:T(8,128)(2,1)S(1)}, bf16[16,2048]{1,0:T(8,128)(2,1)}, u32[]{:S(2)}) copy-start(bf16[16,2048]{1,0:T(8,128)(2,1)} %get-tuple-element.25) | copy-start | bytes 196612
  45.6 24.8 %collective-permute-start.16 = (bf16[1024,512]{1,0:T(8,128)(2,1)S(1)}, bf16[1024,512]{1,0:T(8,128)(2,1)S(1)}, u32[]{:S(2)}, u32[]{:S(2)}) collective-permute-start(bf16[1024,512]{1,0:T(8,128)(2,1)S(1)} %bitcast.26), channel_id=1, source_target_pairs={{0,1},{1,2},{2,3},{3,0},{4,5},{5,6},{6,7},{7,4},{8,9},{9,10},{10,1... | collective-permute-start | bytes 3145736 | tf_op jit(solution)/shard_map/ppermute | solution.py:346
  46.8 23.7 %collective-permute-start.17 = (bf16[1024,512]{1,0:T(8,128)(2,1)S(1)}, bf16[1024,512]{1,0:T(8,128)(2,1)S(1)}, u32[]{:S(2)}, u32[]{:S(2)}) collective-permute-start(bf16[1024,512]{1,0:T(8,128)(2,1)S(1)} %bitcast.27), channel_id=1, source_target_pairs={{0,3},{1,0},{2,1},{3,2},{4,7},{5,4},{6,5},{7,6},{8,11},{9,8},{10,9... | collective-permute-start | bytes 3145736 | tf_op jit(solution)/shard_map/ppermute | solution.py:347
  70.4 12.8 %collective-permute-start.18 = (bf16[512,512]{1,0:T(8,128)(2,1)S(1)}, bf16[512,512]{1,0:T(8,128)(2,1)S(1)}, u32[]{:S(2)}, u32[]{:S(2)}) collective-permute-start(bf16[512,512]{1,0:T(8,128)(2,1)S(1)} %slice.32), channel_id=1, source_target_pairs={{0,1},{1,2},{2,3},{3,0},{4,5},{5,6},{6,7},{7,4},{8,9},{9,10},{10,1... | collective-permute-start | bytes 1572872 | tf_op jit(solution)/shard_map/ppermute | solution.py:348
  70.5 12.6 %collective-permute-start.19 = (bf16[512,512]{1,0:T(8,128)(2,1)S(1)}, bf16[512,512]{1,0:T(8,128)(2,1)S(1)}, u32[]{:S(2)}, u32[]{:S(2)}) collective-permute-start(bf16[512,512]{1,0:T(8,128)(2,1)S(1)} %slice.33), channel_id=1, source_target_pairs={{0,3},{1,0},{2,1},{3,2},{4,7},{5,4},{6,5},{7,6},{8,11},{9,8},{10,9... | collective-permute-start | bytes 1572872 | tf_op jit(solution)/shard_map/ppermute | solution.py:349
  73.3 15.2 %collective-permute-start = (bf16[16,2048]{1,0:T(8,128)(2,1)S(1)}, bf16[16,2048]{1,0:T(8,128)(2,1)S(1)}, u32[]{:S(2)}, u32[]{:S(2)}) collective-permute-start(bf16[16,2048]{1,0:T(8,128)(2,1)S(1)} %copy-done.13), channel_id=1, source_target_pairs={{0,4},{4,8},{8,12},{12,16},{16,20},{20,24},{24,28},{28,32},{32,36}... | collective-permute-start | bytes 196616 | tf_op jit(solution)/shard_map/ppermute | solution.py:457
  85.7 67.9 %copy-start.4 = (bf16[1024,256]{1,0:T(8,128)(2,1)}, bf16[1024,256]{1,0:T(8,128)(2,1)S(1)}, u32[]{:S(2)}) copy-start(bf16[1024,256]{1,0:T(8,128)(2,1)S(1)} %shard_map.212.own) | copy-start | bytes 1572868
  85.7 56.0 %collective-permute-start.20 = (bf16[1024,256]{1,0:T(8,128)(2,1)S(1)}, bf16[1024,256]{1,0:T(8,128)(2,1)S(1)}, u32[]{:S(2)}, u32[]{:S(2)}) collective-permute-start(bf16[1024,256]{1,0:T(8,128)(2,1)S(1)} %shard_map.212.own), channel_id=1, source_target_pairs={{0,1},{1,2},{2,3},{3,0},{4,5},{5,6},{6,7},{7,4},{8,9},{9,10},{10,1... | collective-permute-start | bytes 1572872 | tf_op jit(solution)/shard_map/ppermute | solution.py:346
  85.8 56.6 %collective-permute-start.21 = (bf16[1024,256]{1,0:T(8,128)(2,1)S(1)}, bf16[1024,256]{1,0:T(8,128)(2,1)S(1)}, u32[]{:S(2)}, u32[]{:S(2)}) collective-permute-start(bf16[1024,256]{1,0:T(8,128)(2,1)S(1)} %shard_map.212.own), channel_id=1, source_target_pairs={{0,3},{1,0},{2,1},{3,2},{4,7},{5,4},{6,5},{7,6},{8,11},{9,8},{10,9... | collective-permute-start | bytes 1572872 | tf_op jit(solution)/shard_map/ppermute | solution.py:347
  88.5 0.6 copy-start.14
  95.5 5.2 %collective-permute-start.1 = (bf16[80,256]{1,0:T(8,128)(2,1)}, bf16[80,256]{1,0:T(8,128)(2,1)S(1)}, u32[]{:S(2)}, u32[]{:S(2)}) collective-permute-start(bf16[80,256]{1,0:T(8,128)(2,1)} %get-tuple-element.32), channel_id=1, source_target_pairs={{0,4},{4,0},{8,12},{12,8},{16,20},{20,16},{24,28},{28,24},{1,5},{5... | collective-permute-start | bytes 122888 | tf_op jit(solution)/shard_map/ppermute | solution.py:492
  99.0 3.2 %collective-permute-start.2 = (bf16[80,256]{1,0:T(8,128)(2,1)}, bf16[80,256]{1,0:T(8,128)(2,1)S(1)}, u32[]{:S(2)}, u32[]{:S(2)}) collective-permute-start(bf16[80,256]{1,0:T(8,128)(2,1)} %get-tuple-element.33), channel_id=1, source_target_pairs={{0,8},{4,12},{8,0},{12,4},{16,24},{20,28},{24,16},{28,20},{1,9},{5... | collective-permute-start | bytes 122888 | tf_op jit(solution)/shard_map/ppermute | solution.py:492
  99.2 5.8 %collective-permute-start.3 = (bf16[80,256]{1,0:T(8,128)(2,1)}, bf16[80,256]{1,0:T(8,128)(2,1)S(1)}, u32[]{:S(2)}, u32[]{:S(2)}) collective-permute-start(bf16[80,256]{1,0:T(8,128)(2,1)} %get-tuple-element.34), channel_id=1, source_target_pairs={{0,12},{4,8},{8,4},{12,0},{16,28},{20,24},{24,20},{28,16},{1,13},{... | collective-permute-start | bytes 122888 | tf_op jit(solution)/shard_map/ppermute | solution.py:492
  100.7 5.1 %collective-permute-start.4 = (bf16[80,256]{1,0:T(8,128)(2,1)}, bf16[80,256]{1,0:T(8,128)(2,1)S(1)}, u32[]{:S(2)}, u32[]{:S(2)}) collective-permute-start(bf16[80,256]{1,0:T(8,128)(2,1)} %get-tuple-element.35), channel_id=1, source_target_pairs={{0,16},{4,20},{8,24},{12,28},{16,0},{20,4},{24,8},{28,12},{1,17},{... | collective-permute-start | bytes 122888 | tf_op jit(solution)/shard_map/ppermute | solution.py:492
  102.2 5.1 %collective-permute-start.5 = (bf16[80,256]{1,0:T(8,128)(2,1)}, bf16[80,256]{1,0:T(8,128)(2,1)S(1)}, u32[]{:S(2)}, u32[]{:S(2)}) collective-permute-start(bf16[80,256]{1,0:T(8,128)(2,1)} %get-tuple-element.36), channel_id=1, source_target_pairs={{0,20},{4,16},{8,28},{12,24},{16,4},{20,0},{24,12},{28,8},{1,21},{... | collective-permute-start | bytes 122888 | tf_op jit(solution)/shard_map/ppermute | solution.py:492
  105.0 4.3 %collective-permute-start.6 = (bf16[80,256]{1,0:T(8,128)(2,1)}, bf16[80,256]{1,0:T(8,128)(2,1)S(1)}, u32[]{:S(2)}, u32[]{:S(2)}) collective-permute-start(bf16[80,256]{1,0:T(8,128)(2,1)} %get-tuple-element.37), channel_id=1, source_target_pairs={{0,24},{4,28},{8,16},{12,20},{16,8},{20,12},{24,0},{28,4},{1,25},{... | collective-permute-start | bytes 122888 | tf_op jit(solution)/shard_map/ppermute | solution.py:492
  105.8 5.5 %collective-permute-start.7 = (bf16[80,256]{1,0:T(8,128)(2,1)}, bf16[80,256]{1,0:T(8,128)(2,1)S(1)}, u32[]{:S(2)}, u32[]{:S(2)}) collective-permute-start(bf16[80,256]{1,0:T(8,128)(2,1)} %get-tuple-element.38), channel_id=1, source_target_pairs={{0,28},{4,24},{8,20},{12,16},{16,12},{20,8},{24,4},{28,0},{1,29},{... | collective-permute-start | bytes 122888 | tf_op jit(solution)/shard_map/ppermute | solution.py:492
  111.3 0.8 copy-start.7
  112.2 4.5 %collective-permute-start.8 = (bf16[80,256]{1,0:T(8,128)(2,1)S(1)}, bf16[80,256]{1,0:T(8,128)(2,1)S(1)}, u32[]{:S(2)}, u32[]{:S(2)}) collective-permute-start(bf16[80,256]{1,0:T(8,128)(2,1)S(1)} %get-tuple-element.40), channel_id=1, source_target_pairs={{0,32},{32,64},{64,96},{96,128},{128,160},{160,192},{192,224},{1,3... | collective-permute-start | bytes 122888 | tf_op jit(solution)/shard_map/ppermute | solution.py:506
  116.7 4.7 %collective-permute-start.9 = (bf16[80,256]{1,0:T(8,128)(2,1)S(1)}, bf16[80,256]{1,0:T(8,128)(2,1)S(1)}, u32[]{:S(2)}, u32[]{:S(2)}) collective-permute-start(bf16[80,256]{1,0:T(8,128)(2,1)S(1)} %collective-permute-done.8.later_ref), channel_id=1, source_target_pairs={{0,32},{32,64},{64,96},{96,128},{128,160},{160,192},{192,224},{1,3... | collective-permute-start | bytes 122888 | tf_op jit(solution)/shard_map/ppermute | solution.py:506
  121.4 6.1 %collective-permute-start.10 = (bf16[80,256]{1,0:T(8,128)(2,1)S(1)}, bf16[80,256]{1,0:T(8,128)(2,1)S(1)}, u32[]{:S(2)}, u32[]{:S(2)}) collective-permute-start(bf16[80,256]{1,0:T(8,128)(2,1)S(1)} %double.2.later_ref), channel_id=1, source_target_pairs={{0,64},{32,96},{64,128},{96,160},{128,192},{160,224},{1,65},{33,97... | collective-permute-start | bytes 122888 | tf_op jit(solution)/shard_map/ppermute | solution.py:506
  127.5 16.2 %collective-permute-start.11 = (bf16[80,256]{1,0:T(8,128)(2,1)S(1)}, bf16[80,256]{1,0:T(8,128)(2,1)S(1)}, u32[]{:S(2)}, u32[]{:S(2)}) collective-permute-start(bf16[80,256]{1,0:T(8,128)(2,1)S(1)} %double.3.later_ref), channel_id=1, source_target_pairs={{0,128},{32,160},{64,192},{96,224},{1,129},{33,161},{65,193},{97,2... | collective-permute-start | bytes 122888 | tf_op jit(solution)/shard_map/ppermute | solution.py:506
  139.0 20.9 %collective-permute-start.24 = (bf16[256,512]{1,0:T(8,128)(2,1)}, bf16[256,512]{1,0:T(8,128)(2,1)}, u32[]{:S(2)}, u32[]{:S(2)}) collective-permute-start(bf16[256,512]{1,0:T(8,128)(2,1)} %get-tuple-element.49), channel_id=1, source_target_pairs={{0,1},{1,2},{2,3},{3,0},{4,5},{5,6},{6,7},{7,4},{8,9},{9,10},{10,1... | collective-permute-start | bytes 786440 | tf_op jit(solution)/shard_map/ppermute | solution.py:450
  139.0 21.0 %collective-permute-start.25 = (bf16[256,512]{1,0:T(8,128)(2,1)}, bf16[256,512]{1,0:T(8,128)(2,1)}, u32[]{:S(2)}, u32[]{:S(2)}) collective-permute-start(bf16[256,512]{1,0:T(8,128)(2,1)} %get-tuple-element.51), channel_id=1, source_target_pairs={{0,3},{1,0},{2,1},{3,2},{4,7},{5,4},{6,5},{7,6},{8,11},{9,8},{10,9... | collective-permute-start | bytes 786440 | tf_op jit(solution)/shard_map/ppermute | solution.py:451
  141.7 18.3 %collective-permute-start.26 = (bf16[256,512]{1,0:T(8,128)(2,1)}, bf16[256,512]{1,0:T(8,128)(2,1)}, u32[]{:S(2)}, u32[]{:S(2)}) collective-permute-start(bf16[256,512]{1,0:T(8,128)(2,1)} %get-tuple-element.48), channel_id=1, source_target_pairs={{0,2},{1,3},{2,0},{3,1},{4,6},{5,7},{6,4},{7,5},{8,10},{9,11},{10,... | collective-permute-start | bytes 786440 | tf_op jit(solution)/shard_map/ppermute | solution.py:452
  142.4 17.6 %collective-permute-start.22 = (bf16[512,256]{1,0:T(8,128)(2,1)}, bf16[512,256]{1,0:T(8,128)(2,1)}, u32[]{:S(2)}, u32[]{:S(2)}) collective-permute-start(bf16[512,256]{1,0:T(8,128)(2,1)} %slice.34), channel_id=1, source_target_pairs={{0,1},{1,2},{2,3},{3,0},{4,5},{5,6},{6,7},{7,4},{8,9},{9,10},{10,1... | collective-permute-start | bytes 786440 | tf_op jit(solution)/shard_map/ppermute | solution.py:348
  143.7 16.3 %collective-permute-start.23 = (bf16[512,256]{1,0:T(8,128)(2,1)}, bf16[512,256]{1,0:T(8,128)(2,1)}, u32[]{:S(2)}, u32[]{:S(2)}) collective-permute-start(bf16[512,256]{1,0:T(8,128)(2,1)} %slice.35), channel_id=1, source_target_pairs={{0,3},{1,0},{2,1},{3,2},{4,7},{5,4},{6,5},{7,6},{8,11},{9,8},{10,9... | collective-permute-start | bytes 786440 | tf_op jit(solution)/shard_map/ppermute | solution.py:349
  146.6 18.1 %all-to-all-start = ((bf16[8,64,256]{2,1,0:T(8,128)(2,1)}), bf16[8,64,256]{2,1,0:T(8,128)(2,1)S(1)}, u32[]{:S(2)}, u32[]{:S(2)}) async-start(bf16[8,64,256]{2,1,0:T(8,128)(2,1)} %enter.1), calls=%async_computation | async-start | bytes 524288 | tf_op jit(solution)/shard_map/all_to_all | solution.py:532
  153.7 16.4 %copy-start.2 = (bf16[384,512]{1,0:T(8,128)(2,1)S(1)}, bf16[384,512]{1,0:T(8,128)(2,1)}, u32[]{:S(2)}) copy-start(bf16[384,512]{1,0:T(8,128)(2,1)} %get-tuple-element.28.r_ref) | copy-start | bytes 1179652
  160.0 10.1 %copy-start = (f32[384,1024]{1,0:T(8,128)S(1)}, f32[384,1024]{1,0:T(8,128)}, u32[]{:S(2)}) copy-start(f32[384,1024]{1,0:T(8,128)} %within.1.y_ref) | copy-start | bytes 4718596
  160.0 1.2 copy-start.5
  164.7 33.6 %all-to-all-start.2 = ((bf16[64,16,512]{2,1,0:T(8,128)(2,1)}), bf16[64,16,512]{2,1,0:T(8,128)(2,1)S(1)}, u32[]{:S(2)}, u32[]{:S(2)}) async-start(bf16[64,16,512]{2,1,0:T(8,128)(2,1)} %bitcast.18), calls=%async_computation.2 | async-start | bytes 2097152 | tf_op jit(solution)/shard_map/all_to_all | solution.py:597
  170.1 2.2 %copy-start.1 = (bf16[1024,2048]{1,0:T(8,128)(2,1)S(1)}, bf16[1024,2048]{1,0:T(8,128)(2,1)}, u32[]{:S(2)}) copy-start(bf16[1024,2048]{1,0:T(8,128)(2,1)} %wo_ref.1) | copy-start | bytes 12582916
  172.3 1.1 copy-start.3
  173.4 0.7 copy-start.6
  174.2 21.6 %copy-start.8 = (f32[2048]{0:T(1024)S(1)}, f32[2048]{0:T(1024)}, u32[]{:S(2)}) copy-start(f32[2048]{0:T(1024)} %param.34) | copy-start | bytes 24580
  177.7 20.5 %copy-start.11 = (f32[256,2]{0,1:T(2,128)S(1)}, f32[256,2]{0,1:T(2,128)}, u32[]{:S(2)}) copy-start(f32[256,2]{0,1:T(2,128)} %param.38) | copy-start | bytes 6148
  177.8 20.5 %copy-start.12 = (s32[2,256]{1,0:T(2,128)S(1)}, s32[2,256]{1,0:T(2,128)}, u32[]{:S(2)}) copy-start(s32[2,256]{1,0:T(2,128)} %get-tuple-element.47.dest_ref) | copy-start | bytes 6148
  177.8 7.3 %collective-permute-start.12 = (bf16[48,2048]{1,0:T(8,128)(2,1)S(1)}, bf16[48,2048]{1,0:T(8,128)(2,1)S(1)}, u32[]{:S(2)}, u32[]{:S(2)}) collective-permute-start(bf16[48,2048]{1,0:T(8,128)(2,1)S(1)} %get-tuple-element.43), channel_id=1, source_target_pairs={{0,1},{1,2},{2,3},{3,0},{4,5},{5,6},{6,7},{7,4},{8,9},{9,10},{10,1... | collective-permute-start | bytes 589832 | tf_op jit(solution)/shard_map/ppermute | solution.py:576
  177.9 7.4 %collective-permute-start.14 = (bf16[48,2048]{1,0:T(8,128)(2,1)S(1)}, bf16[48,2048]{1,0:T(8,128)(2,1)S(1)}, u32[]{:S(2)}, u32[]{:S(2)}) collective-permute-start(bf16[48,2048]{1,0:T(8,128)(2,1)S(1)} %get-tuple-element.45), channel_id=1, source_target_pairs={{0,3},{1,0},{2,1},{3,2},{4,7},{5,4},{6,5},{7,6},{8,11},{9,8},{10,9... | collective-permute-start | bytes 589832 | tf_op jit(solution)/shard_map/ppermute | solution.py:577
  185.2 10.7 %collective-permute-start.13 = (bf16[96,2048]{1,0:T(8,128)(2,1)S(1)}, bf16[96,2048]{1,0:T(8,128)(2,1)S(1)}, u32[]{:S(2)}, u32[]{:S(2)}) collective-permute-start(bf16[96,2048]{1,0:T(8,128)(2,1)S(1)} %pad_maximum_fusion), channel_id=1, source_target_pairs={{0,1},{1,2},{2,3},{3,0},{4,5},{5,6},{6,7},{7,4},{8,9},{9,10},{10,1... | collective-permute-start | bytes 1179656 | tf_op jit(solution)/shard_map/ppermute | solution.py:581
  185.3 10.5 %collective-permute-start.15 = (bf16[96,2048]{1,0:T(8,128)(2,1)S(1)}, bf16[96,2048]{1,0:T(8,128)(2,1)S(1)}, u32[]{:S(2)}, u32[]{:S(2)}) collective-permute-start(bf16[96,2048]{1,0:T(8,128)(2,1)S(1)} %pad_maximum_fusion.1), channel_id=1, source_target_pairs={{0,3},{1,0},{2,1},{3,2},{4,7},{5,4},{6,5},{7,6},{8,11},{9,8},{10,9... | collective-permute-start | bytes 1179656 | tf_op jit(solution)/shard_map/ppermute | solution.py:582

commit v3 on v2

--- a/solution.py
+++ b/solution.py
@@ -205,34 +205,20 @@
     return pad[0:groups] + pad[groups : 2 * groups]
 
 
-def double_kernel(later_ref, earlier_ref, out_ref):
-    height, width = out_ref.shape
-    groups = 4
-    rows = (height - 16) // groups
-    base = groups * rows
-    later = unpack_logs(later_ref, groups, base)
-    for g in range(groups):
-        here = slice(g * rows, (g + 1) * rows)
-        grown = jnp.exp(later[g : g + 1]) * earlier_ref[here, :].astype(F32)
-        out_ref[here, :] = (grown + later_ref[here, :].astype(F32)).astype(BF16)
-    total = later + unpack_logs(earlier_ref, groups, base)
-    high = total.astype(BF16).astype(F32)
-    out_ref[base:, :] = jnp.concatenate(
-        [high, total - high, jnp.zeros((16 - 2 * groups, width), F32)], axis=0
-    ).astype(BF16)
-
-
-def enter_kernel(before_ref, later_ref, earlier_ref, out_ref):
-    height, _ = later_ref.shape
+def enter_kernel(zi_ref, before_ref, planes_ref, out_ref):
+    count, height, width = planes_ref.shape
     parts = before_ref.shape[0]
     groups = 4
     rows = (height - 16) // groups
     base = groups * rows
-    later = unpack_logs(later_ref, groups, base)
+    mine = zi_ref[0]
+    logs = [unpack_logs(planes_ref.at[k], groups, base) for k in range(count)]
     for g in range(groups):
         here = slice(g * rows, (g + 1) * rows)
-        grown = jnp.exp(later[g : g + 1]) * earlier_ref[here, :].astype(F32)
-        state = grown + later_ref[here, :].astype(F32)
+        state = jnp.zeros((rows, width), F32)
+        for k in range(count - 1):
+            new = jnp.exp(logs[k][g : g + 1]) * state + planes_ref[k, here, :].astype(F32)
+            state = jnp.where(k < mine, new, state)
         for p in range(parts):
             log = before_ref[p, base + g : base + g + 1, :]
             out_ref[p, here, :] = (before_ref[p, here, :] + jnp.exp(log) * state).astype(BF16)
@@ -316,59 +302,71 @@
     out_ref[...] = (dot_tn(high, back) + dot_tn(low, back)).astype(BF16)
 
 
-def hidden_kernel(me_ref, own, left, right, op0, op1, gate_ref, up_ref, out_ref):
-    me = me_ref[0]
-    size = own.shape[1]
-    opposite = jnp.where(pl.program_id(0) < pl.num_programs(0) // 2, op0[...], op1[...])
-
-    def product(w):
-        def rows(shift):
-            return pl.ds(pl.multiple_of(lax.rem(me + shift, 4) * size, size), size)
-
-        total = dot(own[...], w[rows(0), :]) + dot(left[...], w[rows(3), :])
-        return total + dot(right[...], w[rows(1), :]) + dot(opposite, w[rows(2), :])
-
-    out_ref[...] = (silu(product(gate_ref)) * product(up_ref)).astype(BF16)
-
-
-def result_kernel(me_ref, own, left, right, op0, op1, down_own, down_left, down_right, down_cross, out_ref):
-    opposite = jnp.where(pl.program_id(0) < pl.num_programs(0) // 2, op0[...], op1[...])
-    total = dot(own[...], down_own[...]) + dot(left[...], down_left[...])
-    total = total + dot(right[...], down_right[...]) + dot(opposite, down_cross[...])
-    out_ref[...] = total.astype(BF16)
-
-
-def ring_pieces(x, axis):
+def tp_rows(me, shift, size):
+    return pl.ds(pl.multiple_of(lax.rem(me + shift, 4) * size, size), size)
+
+
+def hidden_near_kernel(me_ref, own, left0, left1, right0, right1, gate_ref, up_ref, out_ref):
+    half, size = left0.shape
+    columns = gate_ref.shape[1]
+    for c, (left, right) in enumerate(((left0, right0), (left1, right1))):
+        here = slice(c * half, (c + 1) * half)
+        for k, w in enumerate((gate_ref, up_ref)):
+            total = dot(own[here, :], w[tp_rows(me_ref[0], 0, size), :])
+            total = total + dot(left[...], w[tp_rows(me_ref[0], 3, size), :])
+            total = total + dot(right[...], w[tp_rows(me_ref[0], 1, size), :])
+            out_ref[here, k * columns : (k + 1) * columns] = total
+
+
+def hidden_kernel(me_ref, near_ref, op0, op1, gate_ref, up_ref, out0_ref, out1_ref):
+    half, size = op0.shape
+    columns = gate_ref.shape[1]
+    for c, (op, out_ref) in enumerate(((op0, out0_ref), (op1, out1_ref))):
+        here = slice(c * half, (c + 1) * half)
+        rows = tp_rows(me_ref[0], 2, size)
+        gate = near_ref[here, :columns] + dot(op[...], gate_ref[rows, :])
+        up = near_ref[here, columns:] + dot(op[...], up_ref[rows, :])
+        out_ref[...] = (silu(gate) * up).astype(BF16)
+
+
+def result_near_kernel(own0, own1, left0, left1, right0, right1, down_own, down_left, down_right, out_ref):
+    half = own0.shape[0]
+    for c, (own, left, right) in enumerate(((own0, left0, right0), (own1, left1, right1))):
+        total = dot(own[...], down_own[...]) + dot(left[...], down_left[...])
+        out_ref[c * half : (c + 1) * half, :] = total + dot(right[...], down_right[...])
+
+
+def result_kernel(near_ref, op0, op1, down_ref, out_ref):
+    half = op0.shape[0]
+    for c, op in enumerate((op0, op1)):
+        here = slice(c * half, (c + 1) * half)
+        out_ref[here, :] = (near_ref[here, :] + dot(op[...], down_ref[...])).astype(BF16)
+
+
+def ring_step(x, axis, by):
     n = lax.axis_size(axis)
-    plus = [(i, (i + 1) % n) for i in range(n)]
-    minus = [(i, (i - 1) % n) for i in range(n)]
-    half = x.shape[0] // 2
-    left = lax.ppermute(x, axis, plus)
-    right = lax.ppermute(x, axis, minus)
-    op0 = lax.ppermute(left[:half], axis, plus)
-    op1 = lax.ppermute(right[half:], axis, minus)
-    return x, left, right, op0, op1
-
-
-def ring_call(kernel, me, pieces, weights, columns, tile):
-    rows = pieces[0].shape[0]
-    steps = rows // tile
-    smem = pl.BlockSpec(memory_space=pltpu.SMEM)
-    specs = [smem]
-    specs += [pl.BlockSpec((tile, p.shape[1]), lambda i: (i, 0)) for p in pieces[:3]]
-    specs.append(pl.BlockSpec((tile, pieces[3].shape[1]), lambda i: (jnp.minimum(i, steps // 2 - 1), 0)))
-    specs.append(pl.BlockSpec((tile, pieces[4].shape[1]), lambda i: (jnp.maximum(i - steps // 2, 0), 0)))
-    specs += [pl.BlockSpec(w.shape, lambda i: (0, 0)) for w in weights]
-    depth = sum(w.shape[0] for w in weights)
+    return lax.ppermute(x, axis, [(i, (i + by) % n) for i in range(n)])
+
+
+def ring(first, second, axis):
+    left0 = ring_step(first, axis, 1)
+    right1 = ring_step(second, axis, -1)
+    left1 = ring_step(second, axis, 1)
+    right0 = ring_step(first, axis, -1)
+    op0 = ring_step(left0, axis, 1)
+    op1 = ring_step(right1, axis, -1)
+    return left0, left1, right0, right1, op0, op1
+
+
+def expert_call(kernel, scalars, arrays, shapes, flops, grant=MID):
     return pl.pallas_call(
         kernel,
-        grid=(steps,),
-        in_specs=specs,
-        out_specs=pl.BlockSpec((tile, columns), lambda i: (i, 0)),
-        out_shape=jax.ShapeDtypeStruct((rows, columns), BF16),
-        compiler_params=params(MID),
-        cost_estimate=cost(2 * rows * depth * columns, rows * depth * 2),
-    )(me, *pieces, *weights)
+        in_specs=[pl.BlockSpec(memory_space=pltpu.SMEM)] * len(scalars) + vmem(len(arrays)),
+        out_specs=vmem(len(shapes)),
+        out_shape=shapes,
+        compiler_params=params(grant),
+        cost_estimate=cost(flops, 4 * MIB),
+    )(*scalars, *arrays)
 
 
 def per_device(
@@ -500,35 +498,19 @@
         cost_estimate=cost(1000000, MIB),
         name="plane",
     )(place, *blocks)
-    planes = lax.axis_size("ep_0")
-
-    def from_below(value, shift):
-        return lax.ppermute(value, "ep_0", [(i, i + shift) for i in range(planes - shift)])
-
-    later = from_below(total, 1)
-    shift = 1
-    while 2 * shift < planes:
-        earlier = from_below(later, shift)
-        later = pl.pallas_call(
-            double_kernel,
-            in_specs=vmem(2),
-            out_specs=vmem(1)[0],
-            out_shape=sds((height, width), BF16),
-            compiler_params=params(MID),
-            cost_estimate=cost(200000, MIB // 8),
-            name="double",
-        )(later, earlier)
-        shift *= 2
-    earlier = from_below(later, shift)
+    zs = lax.axis_size("ep_0")
+    planes = lax.all_to_all(
+        jnp.broadcast_to(total[None], (zs, height, width)), "ep_0", 0, 0, tiled=True
+    )
     entering = pl.pallas_call(
         enter_kernel,
-        in_specs=vmem(3),
+        in_specs=[smem] + vmem(2),
         out_specs=vmem(1)[0],
         out_shape=sds((parts, height - 16, width), BF16),
         compiler_params=params(MID),
         cost_estimate=cost(1000000, MIB),
         name="enter",
-    )(before, later, earlier)
+    )(lax.axis_index("ep_0").reshape(1).astype(jnp.int32), before, planes)
     entering = lax.all_to_all(entering, PLANE, 0, 0, tiled=True)
 
     y = pl.pallas_call(
@@ -590,10 +572,36 @@
         name="norm",
     )(own, up, dn, mixer_norm_scale[None, :])
 
-    pieces = ring_pieces(arrived, "tp")
-    hidden = ring_call(hidden_kernel, me, pieces, (expert_gate_matrix[0], expert_up_matrix[0]), ff, 512)
-    pieces = ring_pieces(hidden, "tp")
-    result = ring_call(result_kernel, me, pieces, (d_own, d_left, d_right, d_cross), quarter, 512)
+    gate_up = (expert_gate_matrix[0], expert_up_matrix[0])
+    half = slots // 2
+    work = 2 * slots * model * ff
+    l0, l1, r0, r1, o0, o1 = ring(arrived[:half], arrived[half:], "tp")
+    (near,) = expert_call(
+        hidden_near_kernel,
+        (me,),
+        (arrived, l0, l1, r0, r1, *gate_up),
+        (sds((slots, 2 * ff), F32),),
+        3 * work // 2,
+        BIG,
+    )
+    h0, h1 = expert_call(
+        hidden_kernel,
+        (me,),
+        (near, o0, o1, *gate_up),
+        (sds((half, ff), BF16), sds((half, ff), BF16)),
+        work // 2,
+    )
+    l0, l1, r0, r1, o0, o1 = ring(h0, h1, "tp")
+    (near,) = expert_call(
+        result_near_kernel,
+        (),
+        (h0, h1, l0, l1, r0, r1, d_own, d_left, d_right),
+        (sds((slots, quarter), F32),),
+        3 * work // 4,
+    )
+    (result,) = expert_call(
+        result_kernel, (), (near, o0, o1, d_cross), (sds((slots, quarter), BF16),), work // 4
+    )
     returned = lax.all_to_all(
         result.reshape(experts, CAP, quarter), EP, split_axis=0, concat_axis=0, tiled=True
     )

time: 201 us -> 189 us (0.940)
  waiting for transfers between devices: 47.8 us -> 29.1 us
  Pallas kernels: 29.3 us -> 34.3 us
  starting transfers between devices: 69.8 us -> 72.1 us
    ppermute x12, waiting for transfers between devices: 30.2 us -> 1.2 us  [ring_step(): return lax.ppermute(x, axis, [(i, (i + by) % n) for i in range(n)])]
    ppermute x12, starting transfers between devices: 32.3 us -> 16.2 us  [ring_step(): return lax.ppermute(x, axis, [(i, (i + by) % n) for i in range(n)])]
    ppermute x7, waiting for transfers between devices: 4.05 us -> 13.6 us  [per_device(): lax.ppermute(blocks[d], PLANE, [(i, i ^ d) for i in range(parts)])]
    all_to_all x1, starting transfers between devices: 7.06 us -> 14.6 us  [per_device(): entering = lax.all_to_all(entering, PLANE, 0, 0, tiled=True)]
    all_to_all x1, starting transfers between devices: 5.38 us -> 10.8 us  [per_device(): lax.all_to_all(result.reshape(experts, CAP, quarter), EP, split_axis=0, c...]
    pallas_call x5, Pallas kernels: 6.92 us -> 12 us  [the longest x4 11.2 us: expert_call(): pl.pallas_call(kernel, in_specs=[pl.BlockSpec(memory_space=pltpu.SMEM)] *...]
    all_to_all x0 -> x1, starting transfers between devices: none -> 4.09 us  [per_device(): lax.all_to_all(jnp.broadcast_to(total[None], (zs, height, width)), 'ep_0'...]
    unnamed x30 -> x32, local copies, waits for them, and re-layouts: 6.64 us -> 7.33 us
  transfers between devices with their start and end apart: 29 -> 30, of which waited for: 11 -> 10; matrix products, arithmetic and copies ran while one was open for 2% -> 1% of each run, Pallas kernels for 12% -> 16%
where the time goes in v3:
time: 189 us; the launch traced here: 188 us
  starting transfers between devices  72.1 us (38%)
  blocking collectives  41.5 us (22%)
  Pallas kernels  34.3 us (18%)
  waiting for transfers between devices  29.1 us (15%)
  local copies, waits for them, and re-layouts  9.99 us (5%)
    all_to_all x1, blocking collectives, per_device(): lax.all_to_all(outgoing.reshape(experts, CAP, quarter), EP, split_axis=0,...  41.5 us
    ppermute x12, starting transfers between devices, ring_step(): return lax.ppermute(x, axis, [(i, (i + by) % n) for i in range(n)])  16.2 us
    all_to_all x1, starting transfers between devices, per_device(): entering = lax.all_to_all(entering, PLANE, 0, 0, tiled=True)  14.6 us
    ppermute x7, waiting for transfers between devices, per_device(): lax.ppermute(blocks[d], PLANE, [(i, i ^ d) for i in range(parts)])  13.6 us
    ppermute x7, starting transfers between devices, per_device(): lax.ppermute(blocks[d], PLANE, [(i, i ^ d) for i in range(parts)])  13.5 us
    pallas_call x4, Pallas kernels, expert_call(): pl.pallas_call(kernel, in_specs=[pl.BlockSpec(memory_space=pltpu.SMEM)] *...  11.2 us
    all_to_all x1, starting transfers between devices, per_device(): lax.all_to_all(result.reshape(experts, CAP, quarter), EP, split_axis=0, c...  10.8 us
    ppermute x1, waiting for transfers between devices, per_device(): up = lax.ppermute(up, 'tp', plus)  7.51 us
  transfers between devices with their start and end apart: 30, of which 10 were waited for; matrix products, arithmetic and copies ran while one was open for 1% of the time, Pallas kernels for 16%

profile of v3, /device:TPU:1, one launch (start us, length us, event | category | flops | bytes accessed | tf_op | source)
XLA Modules:
  0.0 188.0 jit_solution(18320147133245223883)
XLA Ops:
  0.6 3.3 %dispatch.1 = (bf16[1024,512]{1,0:T(8,128)(2,1)}, s32[2,256]{1,0:T(2,128)}, bf16[16,2048]{1,0:T(8,128)(2,1)}) custom-call(s32[1]{0:T(128)} %bitcast.me_ref, bf16[256,2048]{1,0:T(8,128)(2,1)} %tok_ref.1, f32[1,2048]{1,0:T(1,128)} %bitcast.37, s32[2,256]{1,0:T(2,128)} %bitcast.38, bf16[384,1024]{1,0:T(8,128)(2,1)} %ch_ref.3, bf16[384,512]{1,0:T(8,128)(2,1)} %wr_ref.3, ...), custom_call_target="tpu_custom_call" | custom-call | flops 268435456 | bytes 4194304 | tf_op jit(solution)/shard_map/dispatch/pallas_call | solution.py:412
  4.0 41.5 %all_to_all.20 = bf16[64,16,512]{2,1,0:T(8,128)(2,1)S(1)} all-to-all(bf16[64,16,512]{2,1,0:T(8,128)(2,1)} %bitcast.36), channel_id=1, replica_groups=mesh['ep_0'=8,'ep_1'=4,'ep_2'=2,'tp'=4] {'ep_0','ep_1','ep_2'}, dimensions={0} | all-to-all | bytes 2097152 | tf_op jit(solution)/shard_map/all_to_all | solution.py:436
  45.4 1.0 copy-done.12
  46.4 1.1 fusion
  47.5 1.2 collective-permute-start.12
  48.7 1.5 collective-permute-start.15
  50.2 4.7 %collective-permute-start = (bf16[16,2048]{1,0:T(8,128)(2,1)S(1)}, bf16[16,2048]{1,0:T(8,128)(2,1)S(1)}, u32[]{:S(2)}, u32[]{:S(2)}) collective-permute-start(bf16[16,2048]{1,0:T(8,128)(2,1)S(1)} %copy-done.14), channel_id=1, source_target_pairs={{0,4},{4,8},{8,12},{12,16},{16,20},{20,24},{24,28},{28,32},{32,36}... | collective-permute-start | bytes 196616 | tf_op jit(solution)/shard_map/ppermute | solution.py:455
  54.9 2.7 %collective-permute-start.14 = (bf16[512,512]{1,0:T(8,128)(2,1)}, bf16[512,512]{1,0:T(8,128)(2,1)}, u32[]{:S(2)}, u32[]{:S(2)}) collective-permute-start(bf16[512,512]{1,0:T(8,128)(2,1)} %bitcast.13), channel_id=1, source_target_pairs={{0,3},{1,0},{2,1},{3,2},{4,7},{5,4},{6,5},{7,6},{8,11},{9,8},{10,9... | collective-permute-start | bytes 1572872 | tf_op jit(solution)/shard_map/ppermute | solution.py:348
  58.2 6.4 %conv.1 = (bf16[384,1024]{1,0:T(8,128)(2,1)}, bf16[384,512]{1,0:T(8,128)(2,1)}, bf16[384,512]{1,0:T(8,128)(2,1)}, f32[16,384]{1,0:T(8,128)}, f32[16,384]{1,0:T(8...) custom-call(s32[1]{0:T(128)} %bitcast.1.place_ref, ...), custom_call_target="tpu_custom_call" | custom-call | flops 805306368 | bytes 4194304 | tf_op jit(solution)/shard_map/conv/pallas_call | solution.py:459
  64.8 1.4 collective-permute-done.1.refs_1_
  66.2 1.2 collective-permute-start.2
  67.4 2.7 %collective-permute-start.17 = (bf16[512,512]{1,0:T(8,128)(2,1)}, bf16[512,512]{1,0:T(8,128)(2,1)S(1)}, u32[]{:S(2)}, u32[]{:S(2)}) collective-permute-start(bf16[512,512]{1,0:T(8,128)(2,1)} %collective-permute-done.15.right1), channel_id=1, source_target_pairs={{0,3},{1,0},{2,1},{3,2},{4,7},{5,4},{6,5},{7,6},{8,11},{9,8},{10,9... | collective-permute-start | bytes 1572872 | tf_op jit(solution)/shard_map/ppermute | solution.py:348
  70.1 1.6 collective-permute-start.3
  71.6 2.6 %collective-permute-done.3.refs_3_ = bf16[80,256]{1,0:T(8,128)(2,1)S(1)} collective-permute-done((bf16[80,256]{1,0:T(8,128)(2,1)}, bf16[80,256]{1,0:T(8,128)(2,1)S(1)}, u32[]{:S(2)}, u32[]{:S(2)}) %collective-permute-start.3) | collective-permute-done | bytes 40992 | tf_op jit(solution)/shard_map/ppermute | solution.py:490
  74.2 1.9 %collective-permute-start.4 = (bf16[80,256]{1,0:T(8,128)(2,1)}, bf16[80,256]{1,0:T(8,128)(2,1)S(1)}, u32[]{:S(2)}, u32[]{:S(2)}) collective-permute-start(bf16[80,256]{1,0:T(8,128)(2,1)} %get-tuple-element.37), channel_id=1, source_target_pairs={{0,16},{4,20},{8,24},{12,28},{16,0},{20,4},{24,8},{28,12},{1,17},{... | collective-permute-start | bytes 122888 | tf_op jit(solution)/shard_map/ppermute | solution.py:490
  76.1 2.7 %collective-permute-done.4.refs_4_ = bf16[80,256]{1,0:T(8,128)(2,1)S(1)} collective-permute-done((bf16[80,256]{1,0:T(8,128)(2,1)}, bf16[80,256]{1,0:T(8,128)(2,1)S(1)}, u32[]{:S(2)}, u32[]{:S(2)}) %collective-permute-start.4) | collective-permute-done | bytes 40992 | tf_op jit(solution)/shard_map/ppermute | solution.py:490
  78.8 3.6 %collective-permute-start.5 = (bf16[80,256]{1,0:T(8,128)(2,1)}, bf16[80,256]{1,0:T(8,128)(2,1)S(1)}, u32[]{:S(2)}, u32[]{:S(2)}) collective-permute-start(bf16[80,256]{1,0:T(8,128)(2,1)} %get-tuple-element.38), channel_id=1, source_target_pairs={{0,20},{4,16},{8,28},{12,24},{16,4},{20,0},{24,12},{28,8},{1,21},{... | collective-permute-start | bytes 122888 | tf_op jit(solution)/shard_map/ppermute | solution.py:490
  82.4 1.9 %collective-permute-done.5.refs_5_ = bf16[80,256]{1,0:T(8,128)(2,1)S(1)} collective-permute-done((bf16[80,256]{1,0:T(8,128)(2,1)}, bf16[80,256]{1,0:T(8,128)(2,1)S(1)}, u32[]{:S(2)}, u32[]{:S(2)}) %collective-permute-start.5) | collective-permute-done | bytes 40992 | tf_op jit(solution)/shard_map/ppermute | solution.py:490
  84.3 1.2 collective-permute-start.6
  85.5 3.1 %collective-permute-done.6.refs_6_ = bf16[80,256]{1,0:T(8,128)(2,1)S(1)} collective-permute-done((bf16[80,256]{1,0:T(8,128)(2,1)}, bf16[80,256]{1,0:T(8,128)(2,1)S(1)}, u32[]{:S(2)}, u32[]{:S(2)}) %collective-permute-start.6) | collective-permute-done | bytes 40992 | tf_op jit(solution)/shard_map/ppermute | solution.py:490
  88.6 3.9 %collective-permute-start.7 = (bf16[80,256]{1,0:T(8,128)(2,1)}, bf16[80,256]{1,0:T(8,128)(2,1)S(1)}, u32[]{:S(2)}, u32[]{:S(2)}) collective-permute-start(bf16[80,256]{1,0:T(8,128)(2,1)} %get-tuple-element.40), channel_id=1, source_target_pairs={{0,28},{4,24},{8,20},{12,16},{16,12},{20,8},{24,4},{28,0},{1,29},{... | collective-permute-start | bytes 122888 | tf_op jit(solution)/shard_map/ppermute | solution.py:490
  92.5 1.9 %collective-permute-done.7.refs_7_ = bf16[80,256]{1,0:T(8,128)(2,1)S(1)} collective-permute-done((bf16[80,256]{1,0:T(8,128)(2,1)}, bf16[80,256]{1,0:T(8,128)(2,1)S(1)}, u32[]{:S(2)}, u32[]{:S(2)}) %collective-permute-start.7) | collective-permute-done | bytes 40992 | tf_op jit(solution)/shard_map/ppermute | solution.py:490
  94.4 0.8 copy-done.8
  96.1 4.1 %all-to-all-start = ((bf16[8,80,256]{2,1,0:T(8,128)(2,1)}), bf16[8,80,256]{2,1,0:T(8,128)(2,1)S(1)}, u32[]{:S(2)}, u32[]{:S(2)}) async-start(bf16[8,80,256]{2,1,0:T(8,128)(2,1)} %broadcast_in_dim.25), calls=%async_computation | async-start | bytes 655360 | tf_op jit(solution)/shard_map/all_to_all | solution.py:502
  100.2 0.8 dynamic-slice_bitcast_fusion
  101.1 2.6 %collective-permute-start.23 = (bf16[256,512]{1,0:T(8,128)(2,1)S(1)}, bf16[256,512]{1,0:T(8,128)(2,1)S(1)}, u32[]{:S(2)}, u32[]{:S(2)}) collective-permute-start(bf16[256,512]{1,0:T(8,128)(2,1)S(1)} %get-tuple-element.55), channel_id=1, source_target_pairs={{0,3},{1,0},{2,1},{3,2},{4,7},{5,4},{6,5},{7,6},{8,11},{9,8},{10,9... | collective-permute-start | bytes 786440 | tf_op jit(solution)/shard_map/ppermute | solution.py:449
  103.7 5.8 %shard_map.212.near_ref = f32[1024,512]{1,0:T(8,128)} custom-call(s32[1]{0:T(128)} %bitcast.me_ref, bf16[1024,512]{1,0:T(8,128)(2,1)} %bitcast.35, bf16[512,512]{1,0:T(8,128)(2,1)} %collective-permute-done.12.left0, bf16[512,512]{1,0:T(8,128)(2,1)} %collective-permute-done.13.left1, bf16[512,512]{1,0:T(8,128)(2,1)} %collective-permute-done.14.right0, ...), custom_call_target="tpu_custom_call" | custom-call | flops 1610612736 | bytes 4194304 | tf_op jit(solution)/shard_map/pallas_call | solution.py:362
  109.5 1.6 copy-done
  111.9 2.7 %collective-permute-start.21 = (bf16[512,256]{1,0:T(8,128)(2,1)S(1)}, bf16[512,256]{1,0:T(8,128)(2,1)}, u32[]{:S(2)}, u32[]{:S(2)}) collective-permute-start(bf16[512,256]{1,0:T(8,128)(2,1)S(1)} %get-tuple-element.50.own1), channel_id=1, source_target_pairs={{0,3},{1,0},{2,1},{3,2},{4,7},{5,4},{6,5},{7,6},{8,11},{9,8},{10,9... | collective-permute-start | bytes 786440 | tf_op jit(solution)/shard_map/ppermute | solution.py:348
  114.6 2.7 %collective-permute-start.20 = (bf16[512,256]{1,0:T(8,128)(2,1)S(1)}, bf16[512,256]{1,0:T(8,128)(2,1)S(1)}, u32[]{:S(2)}, u32[]{:S(2)}) collective-permute-start(bf16[512,256]{1,0:T(8,128)(2,1)S(1)} %get-tuple-element.49.own0), channel_id=1, source_target_pairs={{0,3},{1,0},{2,1},{3,2},{4,7},{5,4},{6,5},{7,6},{8,11},{9,8},{10,9... | collective-permute-start | bytes 786440 | tf_op jit(solution)/shard_map/ppermute | solution.py:348
  117.3 1.2 collective-permute-done.18.left0
  118.4 2.7 %collective-permute-start.25 = (bf16[512,256]{1,0:T(8,128)(2,1)}, bf16[512,256]{1,0:T(8,128)(2,1)}, u32[]{:S(2)}, u32[]{:S(2)}) collective-permute-start(bf16[512,256]{1,0:T(8,128)(2,1)} %collective-permute-done.21.right1), channel_id=1, source_target_pairs={{0,3},{1,0},{2,1},{3,2},{4,7},{5,4},{6,5},{7,6},{8,11},{9,8},{10,9... | collective-permute-start | bytes 786440 | tf_op jit(solution)/shard_map/ppermute | solution.py:348
  121.1 0.8 enter.1
  122.0 14.6 %all-to-all-start.1 = ((bf16[8,64,256]{2,1,0:T(8,128)(2,1)}), bf16[8,64,256]{2,1,0:T(8,128)(2,1)S(1)}, u32[]{:S(2)}, u32[]{:S(2)}) async-start(bf16[8,64,256]{2,1,0:T(8,128)(2,1)} %enter.1), calls=%async_computation.1 | async-start | bytes 524288 | tf_op jit(solution)/shard_map/all_to_all | solution.py:514
  136.5 6.3 %within.1.y_ref = f32[384,1024]{1,0:T(8,128)} custom-call(bf16[384,1024]{1,0:T(8,128)(2,1)} %get-tuple-element.28.x_ref, bf16[384,512]{1,0:T(8,128)(2,1)} %get-tuple-element.29.w_ref, bf16[384,512]{1,0:T(8,128)(2,1)} %get-tuple-element.30.r_ref, f32[16,384]{1,0:T(8,128)} %get-tuple-element.31.cum_ref, f32[16,384]{1,0:T(8,128)} %get-tuple-element.32.step_ref, ...), custom_call_target="tpu_custom_call" | custom-call | flops 603979776 | bytes 4194304 | tf_op jit(solution)/shard_map/within/pallas_call | solution.py:516
  142.8 2.0 %shard_map.214.near_ref = f32[1024,512]{1,0:T(8,128)S(1)} custom-call(bf16[512,256]{1,0:T(8,128)(2,1)S(1)} %get-tuple-element.49.own0, bf16[512,256]{1,0:T(8,128)(2,1)S(1)} %get-tuple-element.50.own1, bf16[512,256]{1,0:T(8,128)(2,1)} %collective-permute-done.18.left0, bf16[512,256]{1,0:T(8,128)(2,1)S(1)} %collective-permute-done.19.left1, ...), custom_call_target="tpu_custom_call" | custom-call | flops 805306368 | bytes 4194304 | tf_op jit(solution)/shard_map/pallas_call | solution.py:362
  144.9 2.7 %shard_map.215 = bf16[1024,512]{1,0:T(8,128)(2,1)} custom-call(f32[1024,512]{1,0:T(8,128)S(1)} %shard_map.214.near_ref, bf16[512,256]{1,0:T(8,128)(2,1)} %collective-permute-done.24.op0, bf16[512,256]{1,0:T(8,128)(2,1)} %collective-permute-done.25.op1, bf16[256,512]{1,0:T(8,128)(2,1)} %collective-permute-done.26.down_ref), custom_call_target="tpu_custom_call" | custom-call | flops 268435456 | bytes 4194304 | tf_op jit(solution)/shard_map/pallas_call | solution.py:362
  147.5 10.8 %all-to-all-start.3 = ((bf16[64,16,512]{2,1,0:T(8,128)(2,1)}), bf16[64,16,512]{2,1,0:T(8,128)(2,1)S(1)}, u32[]{:S(2)}, u32[]{:S(2)}) async-start(bf16[64,16,512]{2,1,0:T(8,128)(2,1)} %bitcast.21), calls=%async_computation.3 | async-start | bytes 2097152 | tf_op jit(solution)/shard_map/all_to_all | solution.py:605
  158.3 2.2 %copy-done.2 = bf16[1024,2048]{1,0:T(8,128)(2,1)S(1)} copy-done((bf16[1024,2048]{1,0:T(8,128)(2,1)S(1)}, bf16[1024,2048]{1,0:T(8,128)(2,1)}, u32[]{:S(2)}) %copy-start.2) | copy-done | bytes 4194328
  160.5 1.1 copy-done.6
  161.6 3.6 %project.1 = (bf16[96,2048]{1,0:T(8,128)(2,1)S(1)}, bf16[96,2048]{1,0:T(8,128)(2,1)S(1)}, bf16[96,2048]{1,0:T(8,128)(2,1)S(1)}, bf16[48,2048]{1,0:T(8,128)(2,1)S(1)}, bf16[48,2048]{1,0:T(8,128)(2,1)S(1)}) custom-call(s32[1]{0:T(128)} %bitcast.me_ref, f32[384,1024]{1,0:T(8,128)S(1)} %copy-done.1, bf16[384,512]{1,0:T(8,128)(2,1)S(1)} %copy-done.5, ...), custom_call_target="tpu_custom_call" | custom-call | flops 1610612736 | bytes 6291456 | tf_op jit(solution)/shard_map/project/pallas_call | solution.py:539
  165.3 2.7 %collective-permute-start.10 = (bf16[48,2048]{1,0:T(8,128)(2,1)S(1)}, bf16[48,2048]{1,0:T(8,128)(2,1)S(1)}, u32[]{:S(2)}, u32[]{:S(2)}) collective-permute-start(bf16[48,2048]{1,0:T(8,128)(2,1)S(1)} %get-tuple-element.47), channel_id=1, source_target_pairs={{0,3},{1,0},{2,1},{3,2},{4,7},{5,4},{6,5},{7,6},{8,11},{9,8},{10,9... | collective-permute-start | bytes 589832 | tf_op jit(solution)/shard_map/ppermute | solution.py:559
  168.1 4.2 %collective-permute-done.8 = bf16[48,2048]{1,0:T(8,128)(2,1)S(1)} collective-permute-done((bf16[48,2048]{1,0:T(8,128)(2,1)S(1)}, bf16[48,2048]{1,0:T(8,128)(2,1)S(1)}, u32[]{:S(2)}, u32[]{:S(2)}) %collective-permute-start.8) | collective-permute-done | bytes 196640 | tf_op jit(solution)/shard_map/ppermute | solution.py:558
  172.6 2.7 %collective-permute-start.11 = (bf16[96,2048]{1,0:T(8,128)(2,1)S(1)}, bf16[96,2048]{1,0:T(8,128)(2,1)S(1)}, u32[]{:S(2)}, u32[]{:S(2)}) collective-permute-start(bf16[96,2048]{1,0:T(8,128)(2,1)S(1)} %pad_maximum_fusion.1), channel_id=1, source_target_pairs={{0,3},{1,0},{2,1},{3,2},{4,7},{5,4},{6,5},{7,6},{8,11},{9,8},{10,9... | collective-permute-start | bytes 1179656 | tf_op jit(solution)/shard_map/ppermute | solution.py:564
  175.3 7.5 %collective-permute-done.9.u_ref = bf16[96,2048]{1,0:T(8,128)(2,1)S(1)} collective-permute-done((bf16[96,2048]{1,0:T(8,128)(2,1)S(1)}, bf16[96,2048]{1,0:T(8,128)(2,1)S(1)}, u32[]{:S(2)}, u32[]{:S(2)}) %collective-permute-start.9) | collective-permute-done | bytes 393248 | tf_op jit(solution)/shard_map/ppermute | solution.py:563
  182.8 1.1 norm.1
  183.9 2.6 %all-to-all-done.3 = bf16[64,16,512]{2,1,0:T(8,128)(2,1)S(1)} async-done(((bf16[64,16,512]{2,1,0:T(8,128)(2,1)}), bf16[64,16,512]{2,1,0:T(8,128)(2,1)S(1)}, u32[]{:S(2)}, u32[]{:S(2)}) %all-to-all-start.3) | async-done | bytes 1048608 | tf_op jit(solution)/shard_map/all_to_all | solution.py:605
  186.5 1.5 combine.1
  (66 shorter events, 3.0 us)
Async XLA Ops:
  4.0 46.2 %copy-start.14 = (bf16[16,2048]{1,0:T(8,128)(2,1)S(1)}, bf16[16,2048]{1,0:T(8,128)(2,1)}, u32[]{:S(2)}) copy-start(bf16[16,2048]{1,0:T(8,128)(2,1)} %get-tuple-element.27) | copy-start | bytes 196612
  45.4 1.0 copy-start.12
  47.5 19.9 %collective-permute-start.12 = (bf16[512,512]{1,0:T(8,128)(2,1)}, bf16[512,512]{1,0:T(8,128)(2,1)}, u32[]{:S(2)}, u32[]{:S(2)}) collective-permute-start(bf16[512,512]{1,0:T(8,128)(2,1)} %bitcast.13), channel_id=1, source_target_pairs={{0,1},{1,2},{2,3},{3,0},{4,5},{5,6},{6,7},{7,4},{8,9},{9,10},{10,1... | collective-permute-start | bytes 1572872 | tf_op jit(solution)/shard_map/ppermute | solution.py:348
  48.7 18.7 %collective-permute-start.15 = (bf16[512,512]{1,0:T(8,128)(2,1)}, bf16[512,512]{1,0:T(8,128)(2,1)}, u32[]{:S(2)}, u32[]{:S(2)}) collective-permute-start(bf16[512,512]{1,0:T(8,128)(2,1)} %bitcast.14), channel_id=1, source_target_pairs={{0,3},{1,0},{2,1},{3,2},{4,7},{5,4},{6,5},{7,6},{8,11},{9,8},{10,9... | collective-permute-start | bytes 1572872 | tf_op jit(solution)/shard_map/ppermute | solution.py:348
  50.2 7.5 %collective-permute-start = (bf16[16,2048]{1,0:T(8,128)(2,1)S(1)}, bf16[16,2048]{1,0:T(8,128)(2,1)S(1)}, u32[]{:S(2)}, u32[]{:S(2)}) collective-permute-start(bf16[16,2048]{1,0:T(8,128)(2,1)S(1)} %copy-done.14), channel_id=1, source_target_pairs={{0,4},{4,8},{8,12},{12,16},{16,20},{20,24},{24,28},{28,32},{32,36}... | collective-permute-start | bytes 196616 | tf_op jit(solution)/shard_map/ppermute | solution.py:455
  54.9 46.2 %collective-permute-start.13 = (bf16[512,512]{1,0:T(8,128)(2,1)}, bf16[512,512]{1,0:T(8,128)(2,1)}, u32[]{:S(2)}, u32[]{:S(2)}) collective-permute-start(bf16[512,512]{1,0:T(8,128)(2,1)} %bitcast.14), channel_id=1, source_target_pairs={{0,1},{1,2},{2,3},{3,0},{4,5},{5,6},{6,7},{7,4},{8,9},{9,10},{10,1... | collective-permute-start | bytes 1572872 | tf_op jit(solution)/shard_map/ppermute | solution.py:348
  54.9 48.7 %collective-permute-start.14 = (bf16[512,512]{1,0:T(8,128)(2,1)}, bf16[512,512]{1,0:T(8,128)(2,1)}, u32[]{:S(2)}, u32[]{:S(2)}) collective-permute-start(bf16[512,512]{1,0:T(8,128)(2,1)} %bitcast.13), channel_id=1, source_target_pairs={{0,3},{1,0},{2,1},{3,2},{4,7},{5,4},{6,5},{7,6},{8,11},{9,8},{10,9... | collective-permute-start | bytes 1572872 | tf_op jit(solution)/shard_map/ppermute | solution.py:348
  57.6 0.6 copy-start.15
  58.2 41.9 %copy-start.13 = (bf16[1,256,2048]{2,1,0:T(8,128)(2,1)S(1)}, bf16[1,256,2048]{2,1,0:T(8,128)(2,1)}, u32[]{:S(2)}) copy-start(bf16[1,256,2048]{2,1,0:T(8,128)(2,1)} %param.41) | copy-start | bytes 3145732
  64.7 1.5 collective-permute-start.1
  66.2 3.9 %collective-permute-start.2 = (bf16[80,256]{1,0:T(8,128)(2,1)}, bf16[80,256]{1,0:T(8,128)(2,1)S(1)}, u32[]{:S(2)}, u32[]{:S(2)}) collective-permute-start(bf16[80,256]{1,0:T(8,128)(2,1)} %get-tuple-element.35), channel_id=1, source_target_pairs={{0,8},{4,12},{8,0},{12,4},{16,24},{20,28},{24,16},{28,20},{1,9},{5... | collective-permute-start | bytes 122888 | tf_op jit(solution)/shard_map/ppermute | solution.py:490
  67.4 42.1 %collective-permute-start.16 = (bf16[512,512]{1,0:T(8,128)(2,1)}, bf16[512,512]{1,0:T(8,128)(2,1)S(1)}, u32[]{:S(2)}, u32[]{:S(2)}) collective-permute-start(bf16[512,512]{1,0:T(8,128)(2,1)} %collective-permute-done.12.left0), channel_id=1, source_target_pairs={{0,1},{1,2},{2,3},{3,0},{4,5},{5,6},{6,7},{7,4},{8,9},{9,10},{10,1... | collective-permute-start | bytes 1572872 | tf_op jit(solution)/shard_map/ppermute | solution.py:348
  67.4 42.1 %collective-permute-start.17 = (bf16[512,512]{1,0:T(8,128)(2,1)}, bf16[512,512]{1,0:T(8,128)(2,1)S(1)}, u32[]{:S(2)}, u32[]{:S(2)}) collective-permute-start(bf16[512,512]{1,0:T(8,128)(2,1)} %collective-permute-done.15.right1), channel_id=1, source_target_pairs={{0,3},{1,0},{2,1},{3,2},{4,7},{5,4},{6,5},{7,6},{8,11},{9,8},{10,9... | collective-permute-start | bytes 1572872 | tf_op jit(solution)/shard_map/ppermute | solution.py:348
  70.1 4.2 %collective-permute-start.3 = (bf16[80,256]{1,0:T(8,128)(2,1)}, bf16[80,256]{1,0:T(8,128)(2,1)S(1)}, u32[]{:S(2)}, u32[]{:S(2)}) collective-permute-start(bf16[80,256]{1,0:T(8,128)(2,1)} %get-tuple-element.36), channel_id=1, source_target_pairs={{0,12},{4,8},{8,4},{12,0},{16,28},{20,24},{24,20},{28,16},{1,13},{... | collective-permute-start | bytes 122888 | tf_op jit(solution)/shard_map/ppermute | solution.py:490
  74.2 4.6 %collective-permute-start.4 = (bf16[80,256]{1,0:T(8,128)(2,1)}, bf16[80,256]{1,0:T(8,128)(2,1)S(1)}, u32[]{:S(2)}, u32[]{:S(2)}) collective-permute-start(bf16[80,256]{1,0:T(8,128)(2,1)} %get-tuple-element.37), channel_id=1, source_target_pairs={{0,16},{4,20},{8,24},{12,28},{16,0},{20,4},{24,8},{28,12},{1,17},{... | collective-permute-start | bytes 122888 | tf_op jit(solution)/shard_map/ppermute | solution.py:490
  78.8 5.5 %collective-permute-start.5 = (bf16[80,256]{1,0:T(8,128)(2,1)}, bf16[80,256]{1,0:T(8,128)(2,1)S(1)}, u32[]{:S(2)}, u32[]{:S(2)}) collective-permute-start(bf16[80,256]{1,0:T(8,128)(2,1)} %get-tuple-element.38), channel_id=1, source_target_pairs={{0,20},{4,16},{8,28},{12,24},{16,4},{20,0},{24,12},{28,8},{1,21},{... | collective-permute-start | bytes 122888 | tf_op jit(solution)/shard_map/ppermute | solution.py:490
  84.3 4.3 %collective-permute-start.6 = (bf16[80,256]{1,0:T(8,128)(2,1)}, bf16[80,256]{1,0:T(8,128)(2,1)S(1)}, u32[]{:S(2)}, u32[]{:S(2)}) collective-permute-start(bf16[80,256]{1,0:T(8,128)(2,1)} %get-tuple-element.39), channel_id=1, source_target_pairs={{0,24},{4,28},{8,16},{12,20},{16,8},{20,12},{24,0},{28,4},{1,25},{... | collective-permute-start | bytes 122888 | tf_op jit(solution)/shard_map/ppermute | solution.py:490
  88.6 5.8 %collective-permute-start.7 = (bf16[80,256]{1,0:T(8,128)(2,1)}, bf16[80,256]{1,0:T(8,128)(2,1)S(1)}, u32[]{:S(2)}, u32[]{:S(2)}) collective-permute-start(bf16[80,256]{1,0:T(8,128)(2,1)} %get-tuple-element.40), channel_id=1, source_target_pairs={{0,28},{4,24},{8,20},{12,16},{16,12},{20,8},{24,4},{28,0},{1,29},{... | collective-permute-start | bytes 122888 | tf_op jit(solution)/shard_map/ppermute | solution.py:490
  94.4 0.8 copy-start.8
  96.1 25.0 %all-to-all-start = ((bf16[8,80,256]{2,1,0:T(8,128)(2,1)}), bf16[8,80,256]{2,1,0:T(8,128)(2,1)S(1)}, u32[]{:S(2)}, u32[]{:S(2)}) async-start(bf16[8,80,256]{2,1,0:T(8,128)(2,1)} %broadcast_in_dim.25), calls=%async_computation | async-start | bytes 655360 | tf_op jit(solution)/shard_map/all_to_all | solution.py:502
  101.0 13.6 %collective-permute-start.22 = (bf16[256,512]{1,0:T(8,128)(2,1)S(1)}, bf16[256,512]{1,0:T(8,128)(2,1)S(1)}, u32[]{:S(2)}, u32[]{:S(2)}) collective-permute-start(bf16[256,512]{1,0:T(8,128)(2,1)S(1)} %get-tuple-element.53), channel_id=1, source_target_pairs={{0,1},{1,2},{2,3},{3,0},{4,5},{5,6},{6,7},{7,4},{8,9},{9,10},{10,1... | collective-permute-start | bytes 786440 | tf_op jit(solution)/shard_map/ppermute | solution.py:448
  101.1 16.2 %collective-permute-start.23 = (bf16[256,512]{1,0:T(8,128)(2,1)S(1)}, bf16[256,512]{1,0:T(8,128)(2,1)S(1)}, u32[]{:S(2)}, u32[]{:S(2)}) collective-permute-start(bf16[256,512]{1,0:T(8,128)(2,1)S(1)} %get-tuple-element.55), channel_id=1, source_target_pairs={{0,3},{1,0},{2,1},{3,2},{4,7},{5,4},{6,5},{7,6},{8,11},{9,8},{10,9... | collective-permute-start | bytes 786440 | tf_op jit(solution)/shard_map/ppermute | solution.py:449
  103.7 5.8 %copy-start.3 = (bf16[1,2048,256]{2,1,0:T(8,128)(2,1)S(1)}, bf16[1,2048,256]{2,1,0:T(8,128)(2,1)}, u32[]{:S(2)}) copy-start(bf16[1,2048,256]{2,1,0:T(8,128)(2,1)} %param.39) | copy-start | bytes 3145732
  103.7 5.8 %copy-start.4 = (bf16[1,2048,256]{2,1,0:T(8,128)(2,1)S(1)}, bf16[1,2048,256]{2,1,0:T(8,128)(2,1)}, u32[]{:S(2)}) copy-start(bf16[1,2048,256]{2,1,0:T(8,128)(2,1)} %param.40) | copy-start | bytes 3145732
  109.5 1.6 copy-start
  111.8 6.6 %collective-permute-start.18 = (bf16[512,256]{1,0:T(8,128)(2,1)S(1)}, bf16[512,256]{1,0:T(8,128)(2,1)}, u32[]{:S(2)}, u32[]{:S(2)}) collective-permute-start(bf16[512,256]{1,0:T(8,128)(2,1)S(1)} %get-tuple-element.49.own0), channel_id=1, source_target_pairs={{0,1},{1,2},{2,3},{3,0},{4,5},{5,6},{6,7},{7,4},{8,9},{9,10},{10,1... | collective-permute-start | bytes 786440 | tf_op jit(solution)/shard_map/ppermute | solution.py:348
  111.9 6.5 %collective-permute-start.21 = (bf16[512,256]{1,0:T(8,128)(2,1)S(1)}, bf16[512,256]{1,0:T(8,128)(2,1)}, u32[]{:S(2)}, u32[]{:S(2)}) collective-permute-start(bf16[512,256]{1,0:T(8,128)(2,1)S(1)} %get-tuple-element.50.own1), channel_id=1, source_target_pairs={{0,3},{1,0},{2,1},{3,2},{4,7},{5,4},{6,5},{7,6},{8,11},{9,8},{10,9... | collective-permute-start | bytes 786440 | tf_op jit(solution)/shard_map/ppermute | solution.py:348
  114.6 28.2 %collective-permute-start.19 = (bf16[512,256]{1,0:T(8,128)(2,1)S(1)}, bf16[512,256]{1,0:T(8,128)(2,1)S(1)}, u32[]{:S(2)}, u32[]{:S(2)}) collective-permute-start(bf16[512,256]{1,0:T(8,128)(2,1)S(1)} %get-tuple-element.50.own1), channel_id=1, source_target_pairs={{0,1},{1,2},{2,3},{3,0},{4,5},{5,6},{6,7},{7,4},{8,9},{9,10},{10,1... | collective-permute-start | bytes 786440 | tf_op jit(solution)/shard_map/ppermute | solution.py:348
  114.6 28.2 %collective-permute-start.20 = (bf16[512,256]{1,0:T(8,128)(2,1)S(1)}, bf16[512,256]{1,0:T(8,128)(2,1)S(1)}, u32[]{:S(2)}, u32[]{:S(2)}) collective-permute-start(bf16[512,256]{1,0:T(8,128)(2,1)S(1)} %get-tuple-element.49.own0), channel_id=1, source_target_pairs={{0,3},{1,0},{2,1},{3,2},{4,7},{5,4},{6,5},{7,6},{8,11},{9,8},{10,9... | collective-permute-start | bytes 786440 | tf_op jit(solution)/shard_map/ppermute | solution.py:348
  117.3 27.6 %collective-permute-start.26 = (bf16[256,512]{1,0:T(8,128)(2,1)}, bf16[256,512]{1,0:T(8,128)(2,1)}, u32[]{:S(2)}, u32[]{:S(2)}) collective-permute-start(bf16[256,512]{1,0:T(8,128)(2,1)} %get-tuple-element.52), channel_id=1, source_target_pairs={{0,2},{1,3},{2,0},{3,1},{4,6},{5,7},{6,4},{7,5},{8,10},{9,11},{10,... | collective-permute-start | bytes 786440 | tf_op jit(solution)/shard_map/ppermute | solution.py:450
  118.4 26.4 %collective-permute-start.24 = (bf16[512,256]{1,0:T(8,128)(2,1)}, bf16[512,256]{1,0:T(8,128)(2,1)}, u32[]{:S(2)}, u32[]{:S(2)}) collective-permute-start(bf16[512,256]{1,0:T(8,128)(2,1)} %collective-permute-done.18.left0), channel_id=1, source_target_pairs={{0,1},{1,2},{2,3},{3,0},{4,5},{5,6},{6,7},{7,4},{8,9},{9,10},{10,1... | collective-permute-start | bytes 786440 | tf_op jit(solution)/shard_map/ppermute | solution.py:348
  118.4 26.4 %collective-permute-start.25 = (bf16[512,256]{1,0:T(8,128)(2,1)}, bf16[512,256]{1,0:T(8,128)(2,1)}, u32[]{:S(2)}, u32[]{:S(2)}) collective-permute-start(bf16[512,256]{1,0:T(8,128)(2,1)} %collective-permute-done.21.right1), channel_id=1, source_target_pairs={{0,3},{1,0},{2,1},{3,2},{4,7},{5,4},{6,5},{7,6},{8,11},{9,8},{10,9... | collective-permute-start | bytes 786440 | tf_op jit(solution)/shard_map/ppermute | solution.py:348
  122.0 25.6 %all-to-all-start.1 = ((bf16[8,64,256]{2,1,0:T(8,128)(2,1)}), bf16[8,64,256]{2,1,0:T(8,128)(2,1)S(1)}, u32[]{:S(2)}, u32[]{:S(2)}) async-start(bf16[8,64,256]{2,1,0:T(8,128)(2,1)} %enter.1), calls=%async_computation.1 | async-start | bytes 524288 | tf_op jit(solution)/shard_map/all_to_all | solution.py:514
  144.8 13.5 %copy-start.1 = (f32[384,1024]{1,0:T(8,128)S(1)}, f32[384,1024]{1,0:T(8,128)}, u32[]{:S(2)}) copy-start(f32[384,1024]{1,0:T(8,128)} %within.1.y_ref) | copy-start | bytes 4718596
  144.8 13.5 %copy-start.5 = (bf16[384,512]{1,0:T(8,128)(2,1)S(1)}, bf16[384,512]{1,0:T(8,128)(2,1)}, u32[]{:S(2)}) copy-start(bf16[384,512]{1,0:T(8,128)(2,1)} %get-tuple-element.30.r_ref) | copy-start | bytes 1179652
  144.8 13.5 %copy-start.7 = (f32[16,384]{1,0:T(8,128)S(1)}, f32[16,384]{1,0:T(8,128)}, u32[]{:S(2)}) copy-start(f32[16,384]{1,0:T(8,128)} %get-tuple-element.31.cum_ref) | copy-start | bytes 73732
  147.5 38.9 %all-to-all-start.3 = ((bf16[64,16,512]{2,1,0:T(8,128)(2,1)}), bf16[64,16,512]{2,1,0:T(8,128)(2,1)S(1)}, u32[]{:S(2)}, u32[]{:S(2)}) async-start(bf16[64,16,512]{2,1,0:T(8,128)(2,1)} %bitcast.21), calls=%async_computation.3 | async-start | bytes 2097152 | tf_op jit(solution)/shard_map/all_to_all | solution.py:605
  158.3 2.2 %copy-start.2 = (bf16[1024,2048]{1,0:T(8,128)(2,1)S(1)}, bf16[1024,2048]{1,0:T(8,128)(2,1)}, u32[]{:S(2)}) copy-start(bf16[1024,2048]{1,0:T(8,128)(2,1)} %wo_ref.1) | copy-start | bytes 12582916
  160.5 1.1 copy-start.6
  165.2 17.6 %copy-start.9 = (f32[2048]{0:T(1024)S(1)}, f32[2048]{0:T(1024)}, u32[]{:S(2)}) copy-start(f32[2048]{0:T(1024)} %param.34) | copy-start | bytes 24580
  165.2 7.1 %collective-permute-start.8 = (bf16[48,2048]{1,0:T(8,128)(2,1)S(1)}, bf16[48,2048]{1,0:T(8,128)(2,1)S(1)}, u32[]{:S(2)}, u32[]{:S(2)}) collective-permute-start(bf16[48,2048]{1,0:T(8,128)(2,1)S(1)} %get-tuple-element.45), channel_id=1, source_target_pairs={{0,1},{1,2},{2,3},{3,0},{4,5},{5,6},{6,7},{7,4},{8,9},{9,10},{10,1... | collective-permute-start | bytes 589832 | tf_op jit(solution)/shard_map/ppermute | solution.py:558
  165.3 7.1 %collective-permute-start.10 = (bf16[48,2048]{1,0:T(8,128)(2,1)S(1)}, bf16[48,2048]{1,0:T(8,128)(2,1)S(1)}, u32[]{:S(2)}, u32[]{:S(2)}) collective-permute-start(bf16[48,2048]{1,0:T(8,128)(2,1)S(1)} %get-tuple-element.47), channel_id=1, source_target_pairs={{0,3},{1,0},{2,1},{3,2},{4,7},{5,4},{6,5},{7,6},{8,11},{9,8},{10,9... | collective-permute-start | bytes 589832 | tf_op jit(solution)/shard_map/ppermute | solution.py:559
  168.1 18.4 %copy-start.10 = (f32[256,2]{0,1:T(2,128)S(1)}, f32[256,2]{0,1:T(2,128)}, u32[]{:S(2)}) copy-start(f32[256,2]{0,1:T(2,128)} %param.38) | copy-start | bytes 6148
  168.1 18.4 %copy-start.11 = (s32[2,256]{1,0:T(2,128)S(1)}, s32[2,256]{1,0:T(2,128)}, u32[]{:S(2)}) copy-start(s32[2,256]{1,0:T(2,128)} %get-tuple-element.51.dest_ref) | copy-start | bytes 6148
  172.4 10.4 %collective-permute-start.9 = (bf16[96,2048]{1,0:T(8,128)(2,1)S(1)}, bf16[96,2048]{1,0:T(8,128)(2,1)S(1)}, u32[]{:S(2)}, u32[]{:S(2)}) collective-permute-start(bf16[96,2048]{1,0:T(8,128)(2,1)S(1)} %pad_maximum_fusion), channel_id=1, source_target_pairs={{0,1},{1,2},{2,3},{3,0},{4,5},{5,6},{6,7},{7,4},{8,9},{9,10},{10,1... | collective-permute-start | bytes 1179656 | tf_op jit(solution)/shard_map/ppermute | solution.py:563
  172.6 10.2 %collective-permute-start.11 = (bf16[96,2048]{1,0:T(8,128)(2,1)S(1)}, bf16[96,2048]{1,0:T(8,128)(2,1)S(1)}, u32[]{:S(2)}, u32[]{:S(2)}) collective-permute-start(bf16[96,2048]{1,0:T(8,128)(2,1)S(1)} %pad_maximum_fusion.1), channel_id=1, source_target_pairs={{0,3},{1,0},{2,1},{3,2},{4,7},{5,4},{6,5},{7,6},{8,11},{9,8},{10,9... | collective-permute-start | bytes 1179656 | tf_op jit(solution)/shard_map/ppermute | solution.py:564

commit v4 on v3

--- a/solution.py
+++ b/solution.py
@@ -263,7 +263,7 @@
 
 
 def dispatch_kernel(
-    me_ref, tok_ref, gain_ref, routes_ref, ch_ref, wr_ref, rd_ref, out_ref, dest_ref, edge_ref, normed_ref
+    me_ref, tok_ref, gain_ref, routes_ref, ch_ref, wr_ref, rd_ref, out_ref, dest_ref, edge_ref
 ):
     count = tok_ref.shape[0]
     slots, quarter = out_ref.shape
@@ -274,7 +274,8 @@
     edge_ref[:, nch + nw :] = rd_ref[...]
     v = tok_ref[...].astype(F32)
     mean = jnp.mean(v * v, axis=-1, keepdims=True)
-    normed_ref[...] = (v * lax.rsqrt(mean + EPS) * gain_ref[...]).astype(BF16)
+    lanes = pl.ds(pl.multiple_of(me_ref[0] * quarter, quarter), quarter)
+    normed = (tok_ref[:, lanes].astype(F32) * lax.rsqrt(mean + EPS) * gain_ref[:, lanes]).astype(BF16)
     ids = iota((experts, count), 0)
     is_first, is_second = ids == routes_ref[0:1, :], ids == routes_ref[1:2, :]
     named = jnp.where(is_first | is_second, 1.0, 0.0).astype(BF16)
@@ -286,8 +287,7 @@
     dest_ref[1:2, :] = dest1
     slot = iota((slots, count), 0)
     chosen = jnp.where((slot == dest0) | (slot == dest1), 1.0, 0.0).astype(BF16)
-    lanes = pl.ds(pl.multiple_of(me_ref[0] * quarter, quarter), quarter)
-    out_ref[...] = dot(chosen, normed_ref[:, lanes]).astype(BF16)
+    out_ref[...] = dot(chosen, normed).astype(BF16)
 
 
 def combine_kernel(back_ref, dest_ref, weight_ref, out_ref):
@@ -336,11 +336,28 @@
         out_ref[c * half : (c + 1) * half, :] = total + dot(right[...], down_right[...])
 
 
-def result_kernel(near_ref, op0, op1, down_ref, out_ref):
-    half = op0.shape[0]
-    for c, op in enumerate((op0, op1)):
-        here = slice(c * half, (c + 1) * half)
-        out_ref[here, :] = (near_ref[here, :] + dot(op[...], down_ref[...])).astype(BF16)
+def result_kernel(near_ref, op, down_ref, *rest):
+    rest[-1][...] = (near_ref[...] + dot(op[...], down_ref[...])).astype(BF16)
+
+
+def result_call(half, near, op, down, before):
+    rows, columns = op.shape[0], down.shape[1]
+    extra = () if before is None else (before,)
+    return pl.pallas_call(
+        result_kernel,
+        grid=(1,),
+        in_specs=[
+            pl.BlockSpec((rows, columns), lambda i: (half, 0)),
+            pl.BlockSpec(op.shape, lambda i: (0, 0)),
+            pl.BlockSpec(down.shape, lambda i: (0, 0)),
+        ]
+        + [pl.BlockSpec(memory_space=pl.ANY)] * len(extra),
+        out_specs=pl.BlockSpec((rows, columns), lambda i: (half, 0)),
+        out_shape=jax.ShapeDtypeStruct((2 * rows, columns), BF16),
+        input_output_aliases={3: 0} if extra else {},
+        compiler_params=params(MID),
+        cost_estimate=cost(2 * rows * op.shape[1] * columns, 2 * MIB),
+    )(near, op, down, *extra)
 
 
 def ring_step(x, axis, by):
@@ -420,7 +437,6 @@
             sds((2, tokens), jnp.int32),
             sds((16, channels + 2 * nw), BF16),
         ),
-        scratch_shapes=[pltpu.VMEM((tokens, model), BF16)],
         compiler_params=params(BIG),
         cost_estimate=cost(2 * slots * tokens * quarter, 4 * MIB),
         name="dispatch",
@@ -599,9 +615,8 @@
         (sds((slots, quarter), F32),),
         3 * work // 4,
     )
-    (result,) = expert_call(
-        result_kernel, (), (near, o0, o1, d_cross), (sds((slots, quarter), BF16),), work // 4
-    )
+    result = result_call(1, near, o1, d_cross, None)
+    result = result_call(0, near, o0, d_cross, result)
     returned = lax.all_to_all(
         result.reshape(experts, CAP, quarter), EP, split_axis=0, concat_axis=0, tiled=True
     )

time: 189 us -> 188 us (level)
  starting transfers between devices: 72.1 us -> 69.3 us
    pallas_call x0 -> x2, Pallas kernels: none -> 3.13 us  [result_call(): pl.pallas_call(result_kernel, grid=(1,), in_specs=[pl.BlockSpec((rows, co...]
    ppermute x12, starting transfers between devices: 16.2 us -> 13.8 us  [ring_step(): return lax.ppermute(x, axis, [(i, (i + by) % n) for i in range(n)])]
    pallas_call x4 -> x3, Pallas kernels: 11.2 us -> 9.39 us  [expert_call(): pl.pallas_call(kernel, in_specs=[pl.BlockSpec(memory_space=pltpu.SMEM)] *...]
    unnamed x32 -> x30, local copies, waits for them, and re-layouts: 7.33 us -> 7.31 us
  transfers between devices with their start and end apart: 30 -> 30, of which waited for: 10 -> 10; matrix products, arithmetic and copies ran while one was open for 1% -> 2% of each run, Pallas kernels for 16% -> 16%
where the time goes in v4:
time: 188 us; the launch traced here: 187 us
  starting transfers between devices  69.3 us (37%)
  blocking collectives  41.4 us (22%)
  Pallas kernels  35.3 us (19%)
  waiting for transfers between devices  29 us (15%)
  local copies, waits for them, and re-layouts  10.9 us (6%)
    all_to_all x1, blocking collectives, per_device(): lax.all_to_all(outgoing.reshape(experts, CAP, quarter), EP, split_axis=0,...  41.4 us
    ppermute x12, starting transfers between devices, ring_step(): return lax.ppermute(x, axis, [(i, (i + by) % n) for i in range(n)])  13.8 us
    all_to_all x1, starting transfers between devices, per_device(): entering = lax.all_to_all(entering, PLANE, 0, 0, tiled=True)  13.7 us
    ppermute x7, waiting for transfers between devices, per_device(): lax.ppermute(blocks[d], PLANE, [(i, i ^ d) for i in range(parts)])  13.6 us
    ppermute x7, starting transfers between devices, per_device(): lax.ppermute(blocks[d], PLANE, [(i, i ^ d) for i in range(parts)])  13.5 us
    all_to_all x1, starting transfers between devices, per_device(): lax.all_to_all(result.reshape(experts, CAP, quarter), EP, split_axis=0, c...  11 us
    pallas_call x3, Pallas kernels, expert_call(): pl.pallas_call(kernel, in_specs=[pl.BlockSpec(memory_space=pltpu.SMEM)] *...  9.39 us
    ppermute x1, waiting for transfers between devices, per_device(): up = lax.ppermute(up, 'tp', plus)  7.79 us
  transfers between devices with their start and end apart: 30, of which 10 were waited for; matrix products, arithmetic and copies ran while one was open for 2% of the time, Pallas kernels for 16%

profile of v4, /device:TPU:1, one launch (start us, length us, event | category | flops | bytes accessed | tf_op | source)
XLA Modules:
  0.0 186.9 jit_solution(3454685801715831509)
XLA Ops:
  0.6 3.0 %dispatch.1 = (bf16[1024,512]{1,0:T(8,128)(2,1)}, s32[2,256]{1,0:T(2,128)}, bf16[16,2048]{1,0:T(8,128)(2,1)}) custom-call(s32[1]{0:T(128)} %bitcast.me_ref, bf16[256,2048]{1,0:T(8,128)(2,1)} %tok_ref.1, f32[1,2048]{1,0:T(1,128)} %bitcast.39, s32[2,256]{1,0:T(2,128)} %bitcast.40, bf16[384,1024]{1,0:T(8,128)(2,1)} %ch_ref.3, bf16[384,512]{1,0:T(8,128)(2,1)} %wr_ref.3, ...), custom_call_target="tpu_custom_call" | custom-call | flops 268435456 | bytes 4194304 | tf_op jit(solution)/shard_map/dispatch/pallas_call | solution.py:429
  3.7 41.4 %all_to_all.20 = bf16[64,16,512]{2,1,0:T(8,128)(2,1)S(1)} all-to-all(bf16[64,16,512]{2,1,0:T(8,128)(2,1)} %bitcast.36), channel_id=1, replica_groups=mesh['ep_0'=8,'ep_1'=4,'ep_2'=2,'tp'=4] {'ep_0','ep_1','ep_2'}, dimensions={0} | all-to-all | bytes 2097152 | tf_op jit(solution)/shard_map/all_to_all | solution.py:452
  45.1 1.0 copy-done.12
  46.1 0.9 fusion
  46.9 1.2 collective-permute-start.12
  48.1 1.5 collective-permute-start.15
  49.6 4.7 %collective-permute-start = (bf16[16,2048]{1,0:T(8,128)(2,1)S(1)}, bf16[16,2048]{1,0:T(8,128)(2,1)S(1)}, u32[]{:S(2)}, u32[]{:S(2)}) collective-permute-start(bf16[16,2048]{1,0:T(8,128)(2,1)S(1)} %copy-done.13), channel_id=1, source_target_pairs={{0,4},{4,8},{8,12},{12,16},{16,20},{20,24},{24,28},{28,32},{32,36}... | collective-permute-start | bytes 196616 | tf_op jit(solution)/shard_map/ppermute | solution.py:471
  54.4 2.7 %collective-permute-start.14 = (bf16[512,512]{1,0:T(8,128)(2,1)}, bf16[512,512]{1,0:T(8,128)(2,1)}, u32[]{:S(2)}, u32[]{:S(2)}) collective-permute-start(bf16[512,512]{1,0:T(8,128)(2,1)} %bitcast.13), channel_id=1, source_target_pairs={{0,3},{1,0},{2,1},{3,2},{4,7},{5,4},{6,5},{7,6},{8,11},{9,8},{10,9... | collective-permute-start | bytes 1572872 | tf_op jit(solution)/shard_map/ppermute | solution.py:365
  57.7 6.4 %conv.1 = (bf16[384,1024]{1,0:T(8,128)(2,1)}, bf16[384,512]{1,0:T(8,128)(2,1)}, bf16[384,512]{1,0:T(8,128)(2,1)}, f32[16,384]{1,0:T(8,128)}, f32[16,384]{1,0:T(8...) custom-call(s32[1]{0:T(128)} %bitcast.1.place_ref, ...), custom_call_target="tpu_custom_call" | custom-call | flops 805306368 | bytes 4194304 | tf_op jit(solution)/shard_map/conv/pallas_call | solution.py:475
  64.1 1.4 collective-permute-done.1.refs_1_
  65.6 1.2 collective-permute-start.2
  66.8 2.7 %collective-permute-start.17 = (bf16[512,512]{1,0:T(8,128)(2,1)}, bf16[512,512]{1,0:T(8,128)(2,1)S(1)}, u32[]{:S(2)}, u32[]{:S(2)}) collective-permute-start(bf16[512,512]{1,0:T(8,128)(2,1)} %collective-permute-done.15.right1), channel_id=1, source_target_pairs={{0,3},{1,0},{2,1},{3,2},{4,7},{5,4},{6,5},{7,6},{8,11},{9,8},{10,9... | collective-permute-start | bytes 1572872 | tf_op jit(solution)/shard_map/ppermute | solution.py:365
  69.4 1.6 collective-permute-start.3
  71.0 2.6 %collective-permute-done.3.refs_3_ = bf16[80,256]{1,0:T(8,128)(2,1)S(1)} collective-permute-done((bf16[80,256]{1,0:T(8,128)(2,1)}, bf16[80,256]{1,0:T(8,128)(2,1)S(1)}, u32[]{:S(2)}, u32[]{:S(2)}) %collective-permute-start.3) | collective-permute-done | bytes 40992 | tf_op jit(solution)/shard_map/ppermute | solution.py:506
  73.6 1.9 %collective-permute-start.4 = (bf16[80,256]{1,0:T(8,128)(2,1)}, bf16[80,256]{1,0:T(8,128)(2,1)S(1)}, u32[]{:S(2)}, u32[]{:S(2)}) collective-permute-start(bf16[80,256]{1,0:T(8,128)(2,1)} %get-tuple-element.37), channel_id=1, source_target_pairs={{0,16},{4,20},{8,24},{12,28},{16,0},{20,4},{24,8},{28,12},{1,17},{... | collective-permute-start | bytes 122888 | tf_op jit(solution)/shard_map/ppermute | solution.py:506
  75.5 2.7 %collective-permute-done.4.refs_4_ = bf16[80,256]{1,0:T(8,128)(2,1)S(1)} collective-permute-done((bf16[80,256]{1,0:T(8,128)(2,1)}, bf16[80,256]{1,0:T(8,128)(2,1)S(1)}, u32[]{:S(2)}, u32[]{:S(2)}) %collective-permute-start.4) | collective-permute-done | bytes 40992 | tf_op jit(solution)/shard_map/ppermute | solution.py:506
  78.2 3.6 %collective-permute-start.5 = (bf16[80,256]{1,0:T(8,128)(2,1)}, bf16[80,256]{1,0:T(8,128)(2,1)S(1)}, u32[]{:S(2)}, u32[]{:S(2)}) collective-permute-start(bf16[80,256]{1,0:T(8,128)(2,1)} %get-tuple-element.38), channel_id=1, source_target_pairs={{0,20},{4,16},{8,28},{12,24},{16,4},{20,0},{24,12},{28,8},{1,21},{... | collective-permute-start | bytes 122888 | tf_op jit(solution)/shard_map/ppermute | solution.py:506
  81.8 1.9 %collective-permute-done.5.refs_5_ = bf16[80,256]{1,0:T(8,128)(2,1)S(1)} collective-permute-done((bf16[80,256]{1,0:T(8,128)(2,1)}, bf16[80,256]{1,0:T(8,128)(2,1)S(1)}, u32[]{:S(2)}, u32[]{:S(2)}) %collective-permute-start.5) | collective-permute-done | bytes 40992 | tf_op jit(solution)/shard_map/ppermute | solution.py:506
  83.7 1.2 collective-permute-start.6
  84.9 3.1 %collective-permute-done.6.refs_6_ = bf16[80,256]{1,0:T(8,128)(2,1)S(1)} collective-permute-done((bf16[80,256]{1,0:T(8,128)(2,1)}, bf16[80,256]{1,0:T(8,128)(2,1)S(1)}, u32[]{:S(2)}, u32[]{:S(2)}) %collective-permute-start.6) | collective-permute-done | bytes 40992 | tf_op jit(solution)/shard_map/ppermute | solution.py:506
  88.0 3.9 %collective-permute-start.7 = (bf16[80,256]{1,0:T(8,128)(2,1)}, bf16[80,256]{1,0:T(8,128)(2,1)S(1)}, u32[]{:S(2)}, u32[]{:S(2)}) collective-permute-start(bf16[80,256]{1,0:T(8,128)(2,1)} %get-tuple-element.40), channel_id=1, source_target_pairs={{0,28},{4,24},{8,20},{12,16},{16,12},{20,8},{24,4},{28,0},{1,29},{... | collective-permute-start | bytes 122888 | tf_op jit(solution)/shard_map/ppermute | solution.py:506
  91.9 1.9 %collective-permute-done.7.refs_7_ = bf16[80,256]{1,0:T(8,128)(2,1)S(1)} collective-permute-done((bf16[80,256]{1,0:T(8,128)(2,1)}, bf16[80,256]{1,0:T(8,128)(2,1)S(1)}, u32[]{:S(2)}, u32[]{:S(2)}) %collective-permute-start.7) | collective-permute-done | bytes 40992 | tf_op jit(solution)/shard_map/ppermute | solution.py:506
  95.4 4.1 %all-to-all-start = ((bf16[8,80,256]{2,1,0:T(8,128)(2,1)}), bf16[8,80,256]{2,1,0:T(8,128)(2,1)S(1)}, u32[]{:S(2)}, u32[]{:S(2)}) async-start(bf16[8,80,256]{2,1,0:T(8,128)(2,1)} %broadcast_in_dim.25), calls=%async_computation | async-start | bytes 655360 | tf_op jit(solution)/shard_map/all_to_all | solution.py:518
  99.5 2.0 %dynamic-slice_bitcast_fusion = (bf16[256,512]{1,0:T(8,128)(2,1)}, bf16[256,512]{1,0:T(8,128)(2,1)S(1)}, bf16[256,512]{1,0:T(8,128)(2,1)S(1)}, bf16[256,512]{1,0:T(8,128)(2,1)S(1)}) fusion(bf16[1,256,2048]{2,1,0:T(8,128)(2,1)} %param.41, s32[]{:T(128)S(6)} %select_n.15, s32[]{:T(128)S(6)} %select_n.13, s32[]{:T(128)S(6)} %select_n.12, s32[]{:T(128)S(6)} %select_n.14), kind=kLoop, calls=%fused_computation.4 | loop fusion | bytes 2097168 | tf_op jit(solution)/shard_map/dynamic_slice | solution.py:461
  101.6 2.6 %collective-permute-start.23 = (bf16[256,512]{1,0:T(8,128)(2,1)S(1)}, bf16[256,512]{1,0:T(8,128)(2,1)S(1)}, u32[]{:S(2)}, u32[]{:S(2)}) collective-permute-start(bf16[256,512]{1,0:T(8,128)(2,1)S(1)} %get-tuple-element.55), channel_id=1, source_target_pairs={{0,3},{1,0},{2,1},{3,2},{4,7},{5,4},{6,5},{7,6},{8,11},{9,8},{10,9... | collective-permute-start | bytes 786440 | tf_op jit(solution)/shard_map/ppermute | solution.py:465
  104.2 5.8 %shard_map.212.near_ref = f32[1024,512]{1,0:T(8,128)} custom-call(s32[1]{0:T(128)} %bitcast.me_ref, bf16[1024,512]{1,0:T(8,128)(2,1)} %bitcast.35, bf16[512,512]{1,0:T(8,128)(2,1)} %collective-permute-done.12.left0, bf16[512,512]{1,0:T(8,128)(2,1)} %collective-permute-done.13.left1, bf16[512,512]{1,0:T(8,128)(2,1)} %collective-permute-done.14.right0, ...), custom_call_target="tpu_custom_call" | custom-call | flops 1610612736 | bytes 4194304 | tf_op jit(solution)/shard_map/pallas_call | solution.py:379
  110.0 1.6 copy-done
  111.6 1.4 shard_map.213
  113.1 1.4 collective-permute-start.18
  114.5 2.7 %collective-permute-start.20 = (bf16[512,256]{1,0:T(8,128)(2,1)S(1)}, bf16[512,256]{1,0:T(8,128)(2,1)}, u32[]{:S(2)}, u32[]{:S(2)}) collective-permute-start(bf16[512,256]{1,0:T(8,128)(2,1)S(1)} %get-tuple-element.49.own0), channel_id=1, source_target_pairs={{0,3},{1,0},{2,1},{3,2},{4,7},{5,4},{6,5},{7,6},{8,11},{9,8},{10,9... | collective-permute-start | bytes 786440 | tf_op jit(solution)/shard_map/ppermute | solution.py:365
  117.2 1.4 collective-permute-done.21.right1
  118.6 1.2 collective-permute-start.26
  121.0 13.7 %all-to-all-start.1 = ((bf16[8,64,256]{2,1,0:T(8,128)(2,1)}), bf16[8,64,256]{2,1,0:T(8,128)(2,1)S(1)}, u32[]{:S(2)}, u32[]{:S(2)}) async-start(bf16[8,64,256]{2,1,0:T(8,128)(2,1)} %enter.1), calls=%async_computation.1 | async-start | bytes 524288 | tf_op jit(solution)/shard_map/all_to_all | solution.py:530
  134.7 6.2 %within.1.y_ref = f32[384,1024]{1,0:T(8,128)} custom-call(bf16[384,1024]{1,0:T(8,128)(2,1)} %get-tuple-element.28.x_ref, bf16[384,512]{1,0:T(8,128)(2,1)} %get-tuple-element.29.w_ref, bf16[384,512]{1,0:T(8,128)(2,1)} %get-tuple-element.30.r_ref, f32[16,384]{1,0:T(8,128)} %get-tuple-element.31.cum_ref, f32[16,384]{1,0:T(8,128)} %get-tuple-element.32.step_ref, ...), custom_call_target="tpu_custom_call" | custom-call | flops 603979776 | bytes 4194304 | tf_op jit(solution)/shard_map/within/pallas_call | solution.py:532
  140.9 2.2 %shard_map.214.near_ref = f32[1024,512]{1,0:T(8,128)S(1)} custom-call(bf16[512,256]{1,0:T(8,128)(2,1)S(1)} %get-tuple-element.49.own0, bf16[512,256]{1,0:T(8,128)(2,1)} %get-tuple-element.50.own1, bf16[512,256]{1,0:T(8,128)(2,1)S(1)} %collective-permute-done.18.left0, bf16[512,256]{1,0:T(8,128)(2,1)} %collective-permute-done.19.left1, ...), custom_call_target="tpu_custom_call" | custom-call | flops 805306368 | bytes 4194304 | tf_op jit(solution)/shard_map/pallas_call | solution.py:379
  143.1 1.1 shard_map.215.rest_0_
  144.2 2.0 %shard_map.216 = bf16[1024,512]{1,0:T(8,128)(2,1)} custom-call(f32[1024,512]{1,0:T(8,128)S(1)} %shard_map.214.near_ref, bf16[512,256]{1,0:T(8,128)(2,1)} %collective-permute-done.24.op, bf16[256,512]{1,0:T(8,128)(2,1)S(1)} %collective-permute-done.25.down_ref, bf16[1024,512]{1,0:T(8,128)(2,1)} %shard_map.215.rest_0_), custom_call_target="tpu_custom_call", output_to_operand_aliasing={{}: (3, {})} | custom-call | flops 134217728 | bytes 2097152 | tf_op jit(solution)/shard_map/pallas_call | solution.py:346
  146.2 11.0 %all-to-all-start.3 = ((bf16[64,16,512]{2,1,0:T(8,128)(2,1)}), bf16[64,16,512]{2,1,0:T(8,128)(2,1)S(1)}, u32[]{:S(2)}, u32[]{:S(2)}) async-start(bf16[64,16,512]{2,1,0:T(8,128)(2,1)} %bitcast.21), calls=%async_computation.3 | async-start | bytes 2097152 | tf_op jit(solution)/shard_map/all_to_all | solution.py:620
  157.3 2.2 %copy-done.2 = bf16[1024,2048]{1,0:T(8,128)(2,1)S(1)} copy-done((bf16[1024,2048]{1,0:T(8,128)(2,1)S(1)}, bf16[1024,2048]{1,0:T(8,128)(2,1)}, u32[]{:S(2)}) %copy-start.2) | copy-done | bytes 4194328
  159.4 1.1 copy-done.6
  160.6 3.6 %project.1 = (bf16[96,2048]{1,0:T(8,128)(2,1)S(1)}, bf16[96,2048]{1,0:T(8,128)(2,1)S(1)}, bf16[96,2048]{1,0:T(8,128)(2,1)S(1)}, bf16[48,2048]{1,0:T(8,128)(2,1)S(1)}, bf16[48,2048]{1,0:T(8,128)(2,1)S(1)}) custom-call(s32[1]{0:T(128)} %bitcast.me_ref, f32[384,1024]{1,0:T(8,128)S(1)} %copy-done.1, bf16[384,512]{1,0:T(8,128)(2,1)S(1)} %copy-done.5, ...), custom_call_target="tpu_custom_call" | custom-call | flops 1610612736 | bytes 6291456 | tf_op jit(solution)/shard_map/project/pallas_call | solution.py:555
  164.4 2.9 %collective-permute-start.10 = (bf16[48,2048]{1,0:T(8,128)(2,1)S(1)}, bf16[48,2048]{1,0:T(8,128)(2,1)S(1)}, u32[]{:S(2)}, u32[]{:S(2)}) collective-permute-start(bf16[48,2048]{1,0:T(8,128)(2,1)S(1)} %get-tuple-element.47), channel_id=1, source_target_pairs={{0,3},{1,0},{2,1},{3,2},{4,7},{5,4},{6,5},{7,6},{8,11},{9,8},{10,9... | collective-permute-start | bytes 589832 | tf_op jit(solution)/shard_map/ppermute | solution.py:575
  167.3 4.5 %collective-permute-done.8 = bf16[48,2048]{1,0:T(8,128)(2,1)S(1)} collective-permute-done((bf16[48,2048]{1,0:T(8,128)(2,1)S(1)}, bf16[48,2048]{1,0:T(8,128)(2,1)S(1)}, u32[]{:S(2)}, u32[]{:S(2)}) %collective-permute-start.8) | collective-permute-done | bytes 196640 | tf_op jit(solution)/shard_map/ppermute | solution.py:574
  172.1 2.7 %collective-permute-start.11 = (bf16[96,2048]{1,0:T(8,128)(2,1)S(1)}, bf16[96,2048]{1,0:T(8,128)(2,1)S(1)}, u32[]{:S(2)}, u32[]{:S(2)}) collective-permute-start(bf16[96,2048]{1,0:T(8,128)(2,1)S(1)} %pad_maximum_fusion.1), channel_id=1, source_target_pairs={{0,3},{1,0},{2,1},{3,2},{4,7},{5,4},{6,5},{7,6},{8,11},{9,8},{10,9... | collective-permute-start | bytes 1179656 | tf_op jit(solution)/shard_map/ppermute | solution.py:580
  174.8 7.8 %collective-permute-done.9.u_ref = bf16[96,2048]{1,0:T(8,128)(2,1)S(1)} collective-permute-done((bf16[96,2048]{1,0:T(8,128)(2,1)S(1)}, bf16[96,2048]{1,0:T(8,128)(2,1)S(1)}, u32[]{:S(2)}, u32[]{:S(2)}) %collective-permute-start.9) | collective-permute-done | bytes 393248 | tf_op jit(solution)/shard_map/ppermute | solution.py:579
  182.6 1.1 norm.1
  183.7 1.7 all-to-all-done.3
  185.4 1.5 combine.1
  (65 shorter events, 4.3 us)
Async XLA Ops:
  3.7 46.0 %copy-start.13 = (bf16[16,2048]{1,0:T(8,128)(2,1)S(1)}, bf16[16,2048]{1,0:T(8,128)(2,1)}, u32[]{:S(2)}) copy-start(bf16[16,2048]{1,0:T(8,128)(2,1)} %get-tuple-element.27) | copy-start | bytes 196612
  45.1 1.0 copy-start.12
  46.9 19.8 %collective-permute-start.12 = (bf16[512,512]{1,0:T(8,128)(2,1)}, bf16[512,512]{1,0:T(8,128)(2,1)}, u32[]{:S(2)}, u32[]{:S(2)}) collective-permute-start(bf16[512,512]{1,0:T(8,128)(2,1)} %bitcast.13), channel_id=1, source_target_pairs={{0,1},{1,2},{2,3},{3,0},{4,5},{5,6},{6,7},{7,4},{8,9},{9,10},{10,1... | collective-permute-start | bytes 1572872 | tf_op jit(solution)/shard_map/ppermute | solution.py:365
  48.1 18.6 %collective-permute-start.15 = (bf16[512,512]{1,0:T(8,128)(2,1)S(1)}, bf16[512,512]{1,0:T(8,128)(2,1)}, u32[]{:S(2)}, u32[]{:S(2)}) collective-permute-start(bf16[512,512]{1,0:T(8,128)(2,1)S(1)} %bitcast.37), channel_id=1, source_target_pairs={{0,3},{1,0},{2,1},{3,2},{4,7},{5,4},{6,5},{7,6},{8,11},{9,8},{10,9... | collective-permute-start | bytes 1572872 | tf_op jit(solution)/shard_map/ppermute | solution.py:365
  49.6 7.5 %collective-permute-start = (bf16[16,2048]{1,0:T(8,128)(2,1)S(1)}, bf16[16,2048]{1,0:T(8,128)(2,1)S(1)}, u32[]{:S(2)}, u32[]{:S(2)}) collective-permute-start(bf16[16,2048]{1,0:T(8,128)(2,1)S(1)} %copy-done.13), channel_id=1, source_target_pairs={{0,4},{4,8},{8,12},{12,16},{16,20},{20,24},{24,28},{28,32},{32,36}... | collective-permute-start | bytes 196616 | tf_op jit(solution)/shard_map/ppermute | solution.py:471
  54.3 47.3 %collective-permute-start.13 = (bf16[512,512]{1,0:T(8,128)(2,1)S(1)}, bf16[512,512]{1,0:T(8,128)(2,1)}, u32[]{:S(2)}, u32[]{:S(2)}) collective-permute-start(bf16[512,512]{1,0:T(8,128)(2,1)S(1)} %bitcast.38), channel_id=1, source_target_pairs={{0,1},{1,2},{2,3},{3,0},{4,5},{5,6},{6,7},{7,4},{8,9},{9,10},{10,1... | collective-permute-start | bytes 1572872 | tf_op jit(solution)/shard_map/ppermute | solution.py:365
  54.4 49.8 %collective-permute-start.14 = (bf16[512,512]{1,0:T(8,128)(2,1)}, bf16[512,512]{1,0:T(8,128)(2,1)}, u32[]{:S(2)}, u32[]{:S(2)}) collective-permute-start(bf16[512,512]{1,0:T(8,128)(2,1)} %bitcast.13), channel_id=1, source_target_pairs={{0,3},{1,0},{2,1},{3,2},{4,7},{5,4},{6,5},{7,6},{8,11},{9,8},{10,9... | collective-permute-start | bytes 1572872 | tf_op jit(solution)/shard_map/ppermute | solution.py:365
  57.1 0.6 copy-start.14
  64.1 1.5 collective-permute-start.1
  65.6 3.9 %collective-permute-start.2 = (bf16[80,256]{1,0:T(8,128)(2,1)}, bf16[80,256]{1,0:T(8,128)(2,1)S(1)}, u32[]{:S(2)}, u32[]{:S(2)}) collective-permute-start(bf16[80,256]{1,0:T(8,128)(2,1)} %get-tuple-element.35), channel_id=1, source_target_pairs={{0,8},{4,12},{8,0},{12,4},{16,24},{20,28},{24,16},{28,20},{1,9},{5... | collective-permute-start | bytes 122888 | tf_op jit(solution)/shard_map/ppermute | solution.py:506
  66.8 43.2 %collective-permute-start.16 = (bf16[512,512]{1,0:T(8,128)(2,1)}, bf16[512,512]{1,0:T(8,128)(2,1)S(1)}, u32[]{:S(2)}, u32[]{:S(2)}) collective-permute-start(bf16[512,512]{1,0:T(8,128)(2,1)} %collective-permute-done.12.left0), channel_id=1, source_target_pairs={{0,1},{1,2},{2,3},{3,0},{4,5},{5,6},{6,7},{7,4},{8,9},{9,10},{10,1... | collective-permute-start | bytes 1572872 | tf_op jit(solution)/shard_map/ppermute | solution.py:365
  66.8 43.2 %collective-permute-start.17 = (bf16[512,512]{1,0:T(8,128)(2,1)}, bf16[512,512]{1,0:T(8,128)(2,1)S(1)}, u32[]{:S(2)}, u32[]{:S(2)}) collective-permute-start(bf16[512,512]{1,0:T(8,128)(2,1)} %collective-permute-done.15.right1), channel_id=1, source_target_pairs={{0,3},{1,0},{2,1},{3,2},{4,7},{5,4},{6,5},{7,6},{8,11},{9,8},{10,9... | collective-permute-start | bytes 1572872 | tf_op jit(solution)/shard_map/ppermute | solution.py:365
  69.4 4.2 %collective-permute-start.3 = (bf16[80,256]{1,0:T(8,128)(2,1)}, bf16[80,256]{1,0:T(8,128)(2,1)S(1)}, u32[]{:S(2)}, u32[]{:S(2)}) collective-permute-start(bf16[80,256]{1,0:T(8,128)(2,1)} %get-tuple-element.36), channel_id=1, source_target_pairs={{0,12},{4,8},{8,4},{12,0},{16,28},{20,24},{24,20},{28,16},{1,13},{... | collective-permute-start | bytes 122888 | tf_op jit(solution)/shard_map/ppermute | solution.py:506
  73.6 4.6 %collective-permute-start.4 = (bf16[80,256]{1,0:T(8,128)(2,1)}, bf16[80,256]{1,0:T(8,128)(2,1)S(1)}, u32[]{:S(2)}, u32[]{:S(2)}) collective-permute-start(bf16[80,256]{1,0:T(8,128)(2,1)} %get-tuple-element.37), channel_id=1, source_target_pairs={{0,16},{4,20},{8,24},{12,28},{16,0},{20,4},{24,8},{28,12},{1,17},{... | collective-permute-start | bytes 122888 | tf_op jit(solution)/shard_map/ppermute | solution.py:506
  78.2 5.5 %collective-permute-start.5 = (bf16[80,256]{1,0:T(8,128)(2,1)}, bf16[80,256]{1,0:T(8,128)(2,1)S(1)}, u32[]{:S(2)}, u32[]{:S(2)}) collective-permute-start(bf16[80,256]{1,0:T(8,128)(2,1)} %get-tuple-element.38), channel_id=1, source_target_pairs={{0,20},{4,16},{8,28},{12,24},{16,4},{20,0},{24,12},{28,8},{1,21},{... | collective-permute-start | bytes 122888 | tf_op jit(solution)/shard_map/ppermute | solution.py:506
  83.7 4.3 %collective-permute-start.6 = (bf16[80,256]{1,0:T(8,128)(2,1)}, bf16[80,256]{1,0:T(8,128)(2,1)S(1)}, u32[]{:S(2)}, u32[]{:S(2)}) collective-permute-start(bf16[80,256]{1,0:T(8,128)(2,1)} %get-tuple-element.39), channel_id=1, source_target_pairs={{0,24},{4,28},{8,16},{12,20},{16,8},{20,12},{24,0},{28,4},{1,25},{... | collective-permute-start | bytes 122888 | tf_op jit(solution)/shard_map/ppermute | solution.py:506
  88.0 5.8 %collective-permute-start.7 = (bf16[80,256]{1,0:T(8,128)(2,1)}, bf16[80,256]{1,0:T(8,128)(2,1)S(1)}, u32[]{:S(2)}, u32[]{:S(2)}) collective-permute-start(bf16[80,256]{1,0:T(8,128)(2,1)} %get-tuple-element.40), channel_id=1, source_target_pairs={{0,28},{4,24},{8,20},{12,16},{16,12},{20,8},{24,4},{28,0},{1,29},{... | collective-permute-start | bytes 122888 | tf_op jit(solution)/shard_map/ppermute | solution.py:506
  93.8 0.8 copy-start.8
  95.4 24.7 %all-to-all-start = ((bf16[8,80,256]{2,1,0:T(8,128)(2,1)}), bf16[8,80,256]{2,1,0:T(8,128)(2,1)S(1)}, u32[]{:S(2)}, u32[]{:S(2)}) async-start(bf16[8,80,256]{2,1,0:T(8,128)(2,1)} %broadcast_in_dim.25), calls=%async_computation | async-start | bytes 655360 | tf_op jit(solution)/shard_map/all_to_all | solution.py:518
  101.5 13.0 %collective-permute-start.22 = (bf16[256,512]{1,0:T(8,128)(2,1)S(1)}, bf16[256,512]{1,0:T(8,128)(2,1)S(1)}, u32[]{:S(2)}, u32[]{:S(2)}) collective-permute-start(bf16[256,512]{1,0:T(8,128)(2,1)S(1)} %get-tuple-element.53), channel_id=1, source_target_pairs={{0,1},{1,2},{2,3},{3,0},{4,5},{5,6},{6,7},{7,4},{8,9},{9,10},{10,1... | collective-permute-start | bytes 786440 | tf_op jit(solution)/shard_map/ppermute | solution.py:464
  101.6 15.6 %collective-permute-start.23 = (bf16[256,512]{1,0:T(8,128)(2,1)S(1)}, bf16[256,512]{1,0:T(8,128)(2,1)S(1)}, u32[]{:S(2)}, u32[]{:S(2)}) collective-permute-start(bf16[256,512]{1,0:T(8,128)(2,1)S(1)} %get-tuple-element.55), channel_id=1, source_target_pairs={{0,3},{1,0},{2,1},{3,2},{4,7},{5,4},{6,5},{7,6},{8,11},{9,8},{10,9... | collective-permute-start | bytes 786440 | tf_op jit(solution)/shard_map/ppermute | solution.py:465
  104.2 5.8 %copy-start.3 = (bf16[1,2048,256]{2,1,0:T(8,128)(2,1)S(1)}, bf16[1,2048,256]{2,1,0:T(8,128)(2,1)}, u32[]{:S(2)}) copy-start(bf16[1,2048,256]{2,1,0:T(8,128)(2,1)} %param.39) | copy-start | bytes 3145732
  104.2 5.8 %copy-start.4 = (bf16[1,2048,256]{2,1,0:T(8,128)(2,1)S(1)}, bf16[1,2048,256]{2,1,0:T(8,128)(2,1)}, u32[]{:S(2)}) copy-start(bf16[1,2048,256]{2,1,0:T(8,128)(2,1)} %param.40) | copy-start | bytes 3145732
  110.0 1.6 copy-start
  113.0 5.5 %collective-permute-start.21 = (bf16[512,256]{1,0:T(8,128)(2,1)}, bf16[512,256]{1,0:T(8,128)(2,1)}, u32[]{:S(2)}, u32[]{:S(2)}) collective-permute-start(bf16[512,256]{1,0:T(8,128)(2,1)} %get-tuple-element.50.own1), channel_id=1, source_target_pairs={{0,3},{1,0},{2,1},{3,2},{4,7},{5,4},{6,5},{7,6},{8,11},{9,8},{10,9... | collective-permute-start | bytes 786440 | tf_op jit(solution)/shard_map/ppermute | solution.py:365
  113.1 6.8 %collective-permute-start.18 = (bf16[512,256]{1,0:T(8,128)(2,1)S(1)}, bf16[512,256]{1,0:T(8,128)(2,1)S(1)}, u32[]{:S(2)}, u32[]{:S(2)}) collective-permute-start(bf16[512,256]{1,0:T(8,128)(2,1)S(1)} %get-tuple-element.49.own0), channel_id=1, source_target_pairs={{0,1},{1,2},{2,3},{3,0},{4,5},{5,6},{6,7},{7,4},{8,9},{9,10},{10,1... | collective-permute-start | bytes 786440 | tf_op jit(solution)/shard_map/ppermute | solution.py:365
  114.5 26.4 %collective-permute-start.19 = (bf16[512,256]{1,0:T(8,128)(2,1)}, bf16[512,256]{1,0:T(8,128)(2,1)}, u32[]{:S(2)}, u32[]{:S(2)}) collective-permute-start(bf16[512,256]{1,0:T(8,128)(2,1)} %get-tuple-element.50.own1), channel_id=1, source_target_pairs={{0,1},{1,2},{2,3},{3,0},{4,5},{5,6},{6,7},{7,4},{8,9},{9,10},{10,1... | collective-permute-start | bytes 786440 | tf_op jit(solution)/shard_map/ppermute | solution.py:365
  114.5 26.4 %collective-permute-start.20 = (bf16[512,256]{1,0:T(8,128)(2,1)S(1)}, bf16[512,256]{1,0:T(8,128)(2,1)}, u32[]{:S(2)}, u32[]{:S(2)}) collective-permute-start(bf16[512,256]{1,0:T(8,128)(2,1)S(1)} %get-tuple-element.49.own0), channel_id=1, source_target_pairs={{0,3},{1,0},{2,1},{3,2},{4,7},{5,4},{6,5},{7,6},{8,11},{9,8},{10,9... | collective-permute-start | bytes 786440 | tf_op jit(solution)/shard_map/ppermute | solution.py:365
  117.2 25.9 %collective-permute-start.25 = (bf16[256,512]{1,0:T(8,128)(2,1)}, bf16[256,512]{1,0:T(8,128)(2,1)S(1)}, u32[]{:S(2)}, u32[]{:S(2)}) collective-permute-start(bf16[256,512]{1,0:T(8,128)(2,1)} %get-tuple-element.52), channel_id=1, source_target_pairs={{0,2},{1,3},{2,0},{3,1},{4,6},{5,7},{6,4},{7,5},{8,10},{9,11},{10,... | collective-permute-start | bytes 786440 | tf_op jit(solution)/shard_map/ppermute | solution.py:466
  118.6 24.5 %collective-permute-start.26 = (bf16[512,256]{1,0:T(8,128)(2,1)}, bf16[512,256]{1,0:T(8,128)(2,1)S(1)}, u32[]{:S(2)}, u32[]{:S(2)}) collective-permute-start(bf16[512,256]{1,0:T(8,128)(2,1)} %collective-permute-done.21.right1), channel_id=1, source_target_pairs={{0,3},{1,0},{2,1},{3,2},{4,7},{5,4},{6,5},{7,6},{8,11},{9,8},{10,9... | collective-permute-start | bytes 786440 | tf_op jit(solution)/shard_map/ppermute | solution.py:365
  119.8 24.4 %collective-permute-start.24 = (bf16[512,256]{1,0:T(8,128)(2,1)S(1)}, bf16[512,256]{1,0:T(8,128)(2,1)}, u32[]{:S(2)}, u32[]{:S(2)}) collective-permute-start(bf16[512,256]{1,0:T(8,128)(2,1)S(1)} %collective-permute-done.18.left0), channel_id=1, source_target_pairs={{0,1},{1,2},{2,3},{3,0},{4,5},{5,6},{6,7},{7,4},{8,9},{9,10},{10,1... | collective-permute-start | bytes 786440 | tf_op jit(solution)/shard_map/ppermute | solution.py:365
  121.0 25.2 %all-to-all-start.1 = ((bf16[8,64,256]{2,1,0:T(8,128)(2,1)}), bf16[8,64,256]{2,1,0:T(8,128)(2,1)S(1)}, u32[]{:S(2)}, u32[]{:S(2)}) async-start(bf16[8,64,256]{2,1,0:T(8,128)(2,1)} %enter.1), calls=%async_computation.1 | async-start | bytes 524288 | tf_op jit(solution)/shard_map/all_to_all | solution.py:530
  146.2 11.0 %copy-start.1 = (f32[384,1024]{1,0:T(8,128)S(1)}, f32[384,1024]{1,0:T(8,128)}, u32[]{:S(2)}) copy-start(f32[384,1024]{1,0:T(8,128)} %within.1.y_ref) | copy-start | bytes 4718596
  146.2 11.0 %copy-start.5 = (bf16[384,512]{1,0:T(8,128)(2,1)S(1)}, bf16[384,512]{1,0:T(8,128)(2,1)}, u32[]{:S(2)}) copy-start(bf16[384,512]{1,0:T(8,128)(2,1)} %get-tuple-element.30.r_ref) | copy-start | bytes 1179652
  146.2 11.0 %copy-start.7 = (f32[16,384]{1,0:T(8,128)S(1)}, f32[16,384]{1,0:T(8,128)}, u32[]{:S(2)}) copy-start(f32[16,384]{1,0:T(8,128)} %get-tuple-element.31.cum_ref) | copy-start | bytes 73732
  146.2 39.1 %all-to-all-start.3 = ((bf16[64,16,512]{2,1,0:T(8,128)(2,1)}), bf16[64,16,512]{2,1,0:T(8,128)(2,1)S(1)}, u32[]{:S(2)}, u32[]{:S(2)}) async-start(bf16[64,16,512]{2,1,0:T(8,128)(2,1)} %bitcast.21), calls=%async_computation.3 | async-start | bytes 2097152 | tf_op jit(solution)/shard_map/all_to_all | solution.py:620
  157.2 2.2 %copy-start.2 = (bf16[1024,2048]{1,0:T(8,128)(2,1)S(1)}, bf16[1024,2048]{1,0:T(8,128)(2,1)}, u32[]{:S(2)}) copy-start(bf16[1024,2048]{1,0:T(8,128)(2,1)} %wo_ref.1) | copy-start | bytes 12582916
  159.4 1.1 copy-start.6
  164.1 18.5 %copy-start.9 = (f32[2048]{0:T(1024)S(1)}, f32[2048]{0:T(1024)}, u32[]{:S(2)}) copy-start(f32[2048]{0:T(1024)} %param.34) | copy-start | bytes 24580
  164.2 7.6 %collective-permute-start.8 = (bf16[48,2048]{1,0:T(8,128)(2,1)S(1)}, bf16[48,2048]{1,0:T(8,128)(2,1)S(1)}, u32[]{:S(2)}, u32[]{:S(2)}) collective-permute-start(bf16[48,2048]{1,0:T(8,128)(2,1)S(1)} %get-tuple-element.45), channel_id=1, source_target_pairs={{0,1},{1,2},{2,3},{3,0},{4,5},{5,6},{6,7},{7,4},{8,9},{9,10},{10,1... | collective-permute-start | bytes 589832 | tf_op jit(solution)/shard_map/ppermute | solution.py:574
  164.4 7.6 %collective-permute-start.10 = (bf16[48,2048]{1,0:T(8,128)(2,1)S(1)}, bf16[48,2048]{1,0:T(8,128)(2,1)S(1)}, u32[]{:S(2)}, u32[]{:S(2)}) collective-permute-start(bf16[48,2048]{1,0:T(8,128)(2,1)S(1)} %get-tuple-element.47), channel_id=1, source_target_pairs={{0,3},{1,0},{2,1},{3,2},{4,7},{5,4},{6,5},{7,6},{8,11},{9,8},{10,9... | collective-permute-start | bytes 589832 | tf_op jit(solution)/shard_map/ppermute | solution.py:575
  167.3 18.1 %copy-start.10 = (f32[256,2]{0,1:T(2,128)S(1)}, f32[256,2]{0,1:T(2,128)}, u32[]{:S(2)}) copy-start(f32[256,2]{0,1:T(2,128)} %param.38) | copy-start | bytes 6148
  167.3 18.1 %copy-start.11 = (s32[2,256]{1,0:T(2,128)S(1)}, s32[2,256]{1,0:T(2,128)}, u32[]{:S(2)}) copy-start(s32[2,256]{1,0:T(2,128)} %get-tuple-element.51.dest_ref) | copy-start | bytes 6148
  171.9 10.7 %collective-permute-start.9 = (bf16[96,2048]{1,0:T(8,128)(2,1)S(1)}, bf16[96,2048]{1,0:T(8,128)(2,1)S(1)}, u32[]{:S(2)}, u32[]{:S(2)}) collective-permute-start(bf16[96,2048]{1,0:T(8,128)(2,1)S(1)} %pad_maximum_fusion), channel_id=1, source_target_pairs={{0,1},{1,2},{2,3},{3,0},{4,5},{5,6},{6,7},{7,4},{8,9},{9,10},{10,1... | collective-permute-start | bytes 1179656 | tf_op jit(solution)/shard_map/ppermute | solution.py:579
  172.1 10.5 %collective-permute-start.11 = (bf16[96,2048]{1,0:T(8,128)(2,1)S(1)}, bf16[96,2048]{1,0:T(8,128)(2,1)S(1)}, u32[]{:S(2)}, u32[]{:S(2)}) collective-permute-start(bf16[96,2048]{1,0:T(8,128)(2,1)S(1)} %pad_maximum_fusion.1), channel_id=1, source_target_pairs={{0,3},{1,0},{2,1},{3,2},{4,7},{5,4},{6,5},{7,6},{8,11},{9,8},{10,9... | collective-permute-start | bytes 1179656 | tf_op jit(solution)/shard_map/ppermute | solution.py:580
